TPU v7x, 32 devices: a whole 2x2x4 slice. The times are simulated.
32 devices in a mesh: sp: 16 (over z, y, x), tp: 2 (over core).
Axes of the slice: x: 2, y: 2, z: 4, core: 2. Of those that a mesh axis runs over, the one named last changes fastest.
Arguments:
- mid_rows: bfloat16 [4096, 2048], P(('sp', 'tp')), may hold values from -6 to 6
- cotangent: bfloat16 [4096, 2048], P(('sp', 'tp')), may hold values from -6 to 6
- routes: int32 [4096, 2], P(('sp', 'tp')), may hold values from 0 to 15, all different within a row; in each aligned block of 128 rows (0 to 127, 128 to 255, ...) at most 32 rows name the same one
- route_weight: float32 [4096, 2], P(('sp', 'tp')), may hold values from 0.3 to 2
- filtered: bfloat16 [4096, 2048], P('sp', 'tp'), may hold values from -30 to 30
- conv_taps: float32 [31, 2048], P(None, 'tp'), may hold values from -1 to 1
- norm_gain: float32 [2048], P('tp'), may hold values from 0.1 to 1.9
- out_weight: bfloat16 [2048, 2048], P('tp'), may hold values from -0.125 to 0.125
- gate_weight: bfloat16 [16, 2048, 1024], P('sp', None, 'tp'), may hold values from -0.125 to 0.125
- up_weight: bfloat16 [16, 2048, 1024], P('sp', None, 'tp'), may hold values from -0.125 to 0.125
- down_weight: bfloat16 [16, 1024, 2048], P('sp', 'tp'), may hold values from -0.1875 to 0.1875
Outputs:
- gate_grad: float32 [16, 2048, 1024], P('sp', None, 'tp')
- up_grad: float32 [16, 2048, 1024], P('sp', None, 'tp')
- down_grad: float32 [16, 1024, 2048], P('sp', 'tp')
- proj_grad: float32 [2048, 2048], P('sp', 'tp')
- input_grad: bfloat16 [4096, 2048], P('sp', 'tp')
Inputs may be any that keep to these rules, and one draw needn't show every extreme that they name: `routes`: each row names 2 different experts. In each aligned block of 128 rows no expert is named by more than 32 rows.
All inputs are finite; a program needn't handle non-finite values.
Results may differ from a plain program's by a relative error of at most 0.0075.
Values may be sent and summed in bfloat16 or wider, within the bound.
A program may use at most 128 MiB of HBM per device.

v0:
```python
import jax
import jax.numpy as jnp
from jax import lax
from jax.sharding import PartitionSpec as P

NORM_EPS = 1e-05


def extended(block, sides, width):
    for axis, dim in sides:
        count = lax.axis_size(axis)
        forward = [(i, i + 1) for i in range(count - 1)]
        backward = [(target, source) for source, target in forward]
        low = lax.ppermute(
            lax.slice_in_dim(block, block.shape[dim] - width, None, axis=dim), axis, forward
        )
        high = lax.ppermute(lax.slice_in_dim(block, 0, width, axis=dim), axis, backward)
        block = jnp.concatenate([low, block, high], axis=dim)
    return block


def silu_grad(pre_act):
    logistic = jax.nn.sigmoid(pre_act)
    return logistic * (1.0 + pre_act * (1.0 - logistic))


def slot_targets(routes, experts, capacity):
    token_count, per_token = routes.shape
    flattened = routes.reshape(token_count * per_token)
    one_hot = flattened[:, None] == jnp.arange(experts, dtype=jnp.int32)[None, :]
    route_ids = jnp.arange(token_count * per_token, dtype=jnp.int32)
    before = (route_ids[None, :] < route_ids[:, None]).astype(jnp.bfloat16)
    earlier = jnp.dot(before, one_hot.astype(jnp.bfloat16), preferred_element_type=jnp.float32)
    positions = jnp.sum(jnp.where(one_hot, earlier, 0.0), axis=1).astype(jnp.int32)
    return (flattened * capacity + positions).reshape(token_count, per_token)


def halving_orders(count):
    bits = count.bit_length() - 1
    turned = min(bits, 3)
    return [
        [(start + step) % turned for step in range(turned)] + list(range(turned, bits))
        for start in range(turned)
    ]


def column_groups(columns, groups):
    lanes = 128
    tiles = columns // lanes
    sizes = [tiles // groups + (1 if g < tiles % groups else 0) for g in range(groups)]
    starts = [sum(sizes[:g]) * lanes for g in range(groups)]
    return [(start, size * lanes) for start, size in zip(starts, sizes) if size]


def picked(block, place, dim):
    return lax.dynamic_index_in_dim(block, place, dim, keepdims=False)


def reduced_products(rows, columns, axis):
    count = lax.axis_size(axis)
    tokens, width = rows.shape
    bits = count.bit_length() - 1
    own = lax.axis_index(axis)
    product = transposed_product(rows, columns).astype(jnp.bfloat16)
    cut = product.reshape((2,) * bits + (width // count, columns.shape[1]))
    orders = halving_orders(count)
    groups = column_groups(columns.shape[1], len(orders))
    orders = orders[: len(groups)]
    totals = [lax.slice_in_dim(cut, start, start + size, axis=bits + 1) for start, size in groups]
    left = [list(range(bits - 1, -1, -1)) for _ in groups]
    for step in range(bits):
        outgoing, kept = [], []
        for total, order, dims in zip(totals, orders, left):
            mine = (own >> order[step]) & 1
            dim = dims.index(order[step])
            dims.pop(dim)
            outgoing.append(picked(total, 1 - mine, dim).astype(jnp.bfloat16))
            kept.append(picked(total, mine, dim).astype(jnp.float32))
        if step == 0:
            outgoing, rows = lax.optimization_barrier((outgoing, rows))
        arrived = [
            lax.ppermute(block, axis, [(i, i ^ (1 << order[step])) for i in range(count)])
            for block, order in zip(outgoing, orders)
        ]
        arrived = lax.optimization_barrier(arrived)
        totals = [own_part + got.astype(jnp.float32) for own_part, got in zip(kept, arrived)]
    return jnp.concatenate(totals, axis=1), rows


def row_product(rows, matrix, dim=0):
    return lax.dot_general(
        rows, matrix, (((1,), (dim,)), ((), ())), preferred_element_type=jnp.float32
    )


def transposed_product(left, right):
    return lax.dot_general(
        left, right, (((0,), (0,)), ((), ())), preferred_element_type=jnp.float32
    )


def from_partner(block, axis):
    count = lax.axis_size(axis)
    return [
        lax.ppermute(block, axis, [(i, (i + step) % count) for i in range(count)])
        for step in range(1, count)
    ]


def hidden_gradients(pre_gate, pre_up, routed, down_mat):
    gate_act = jax.nn.silu(pre_gate)
    hidden = (gate_act * pre_up).astype(jnp.bfloat16)
    hidden_grad = row_product(routed, down_mat, 1)
    gate_pre = (hidden_grad * pre_up * silu_grad(pre_gate)).astype(jnp.bfloat16)
    up_pre = (hidden_grad * gate_act).astype(jnp.bfloat16)
    return hidden, gate_pre, up_pre


def input_part(gate_pre, up_pre, gate_mat, up_mat):
    return (row_product(gate_pre, gate_mat, 1) + row_product(up_pre, up_mat, 1)).astype(
        jnp.bfloat16
    )


def expert_backward(got_in, got_cot, gate_mat, up_mat, down_mat, axis):
    count = lax.axis_size(axis)
    all_in = [got_in] + from_partner(got_in, axis)
    pre = [(row_product(rows, gate_mat), row_product(rows, up_mat)) for rows in all_in]
    pre, got_cot = lax.optimization_barrier((pre, got_cot))
    all_cot = [got_cot] + from_partner(got_cot, axis)
    grads = [hidden_gradients(g, u, c, down_mat) for (g, u), c in zip(pre, all_cot)]
    back = None
    for step in range(1, count):
        part = input_part(grads[step][1], grads[step][2], gate_mat, up_mat)
        arrived = lax.ppermute(part, axis, [(i, (i - step) % count) for i in range(count)])
        back = (arrived,) if back is None else back + (arrived,)
    back_rows = input_part(grads[0][1], grads[0][2], gate_mat, up_mat).astype(jnp.float32)
    for arrived in back or ():
        back_rows = back_rows + arrived.astype(jnp.float32)
    gate_part = sum(transposed_product(x, g[1]) for x, g in zip(all_in, grads))
    up_part = sum(transposed_product(x, g[2]) for x, g in zip(all_in, grads))
    down_part = sum(transposed_product(g[0], c) for g, c in zip(grads, all_cot))
    return gate_part, up_part, down_part, back_rows.astype(jnp.bfloat16)


def gathered_rows(block, axis):
    count = lax.axis_size(axis)
    own = lax.axis_index(axis)
    blocks = [block] + from_partner(block, axis)
    turned = jnp.concatenate(blocks, axis=0)
    result = turned
    for place in range(1, count):
        order = [blocks[(place - i) % count] for i in range(count)]
        result = jnp.where(own == place, jnp.concatenate(order, axis=0), result)
    first = [blocks[-i % count] for i in range(count)]
    return jnp.where(own == 0, jnp.concatenate(first, axis=0), result)


def per_device(
    mid_rows,
    cotangent,
    routes,
    route_weight,
    filtered,
    conv_taps,
    norm_gain,
    out_weight,
    gate_weight,
    up_weight,
    down_weight,
):
    sp_count = lax.axis_size("sp")
    token_count, model_width = mid_rows.shape
    per_token = routes.shape[1]
    local_experts = gate_weight.shape[0]
    experts = local_experts * sp_count
    capacity = 2 * token_count * per_token // sp_count
    values = filtered.astype(jnp.float32)
    channel_sum, squares = lax.psum(
        (jnp.sum(values, axis=1), jnp.sum(values * values, axis=1)), "tp"
    )
    half = sp_count // 2
    side = lax.axis_index("sp") // half
    target = slot_targets(routes, experts, capacity)
    slot_ids = jnp.arange(experts * capacity, dtype=jnp.int32)
    chosen = jnp.any(slot_ids[:, None, None] == target[None, :, :], axis=2).astype(jnp.bfloat16)

    def with_far(block):
        far = lax.ppermute(block, "sp", [(i, (i + half) % sp_count) for i in range(sp_count)])
        return jnp.concatenate([block, far], axis=0)

    both_target, both_weight = with_far(target), with_far(route_weight)
    expert = both_target // capacity - side * half * local_experts
    origin = jnp.concatenate(
        [jnp.full((token_count, 1), side), jnp.full((token_count, 1), 1 - side)], axis=0
    )
    place = (expert // local_experts * 2 + origin) * local_experts + expert % local_experts
    place = place * capacity + both_target % capacity
    place = jnp.where((expert >= 0) & (expert < half * local_experts), place, -1)
    holds = slot_ids[:, None, None] == place[None, :, :]
    sent = jnp.any(holds, axis=2).astype(jnp.bfloat16)
    route_scale = jnp.sum(jnp.where(holds, both_weight[None, :, :], 0.0), axis=(1, 2))

    def within_half(block):
        return lax.all_to_all(
            block.reshape(half, 2, local_experts, capacity, model_width),
            "sp",
            split_axis=0,
            concat_axis=0,
            axis_index_groups=[[s * half + i for i in range(half)] for s in range(2)],
            tiled=True,
        )

    both_mid = with_far(mid_rows)
    both_mid, near_cot = lax.optimization_barrier((both_mid, cotangent))
    both_cot = with_far(near_cot)
    inputs = jnp.dot(sent, both_mid, preferred_element_type=jnp.float32).astype(jnp.bfloat16)
    got_in = within_half(inputs)
    cot_rows = jnp.dot(sent, both_cot, preferred_element_type=jnp.float32)
    routed = (route_scale[:, None] * cot_rows).astype(jnp.bfloat16)
    got_cot = within_half(routed)
    by_expert = (sp_count, local_experts, capacity, model_width)
    parts = [
        expert_backward(
            got_in[:, :, e].reshape(sp_count * capacity, model_width),
            got_cot[:, :, e].reshape(sp_count * capacity, model_width),
            gate_weight[e],
            up_weight[e],
            down_weight[e],
            "tp",
        )
        for e in range(local_experts)
    ]
    gate_grad, up_grad, down_grad = (
        jnp.stack([part[i] for part in parts], axis=0) for i in range(3)
    )
    back_rows = jnp.stack(
        [
            part[3].reshape(half, 2, capacity, model_width).transpose(1, 0, 2, 3)
            for part in parts
        ],
        axis=2,
    ).reshape(by_expert)
    returned = lax.all_to_all(back_rows, "sp", split_axis=0, concat_axis=0, tiled=True)
    returned, gate_grad, up_grad, down_grad, channel_sum, squares = lax.optimization_barrier(
        (returned, gate_grad, up_grad, down_grad, channel_sum, squares)
    )
    back_all = returned.reshape(experts * capacity, model_width)
    route_sum = lax.dot_general(
        chosen, back_all, (((0,), (0,)), ((), ())), preferred_element_type=jnp.float32
    )
    mid_grad = (cotangent.astype(jnp.float32) + route_sum).astype(jnp.bfloat16)
    average = channel_sum / model_width
    variance = squares / model_width - average * average
    inv_scale = lax.rsqrt(variance + NORM_EPS)[:, None]
    normed = (values - average[:, None]) * inv_scale
    scaled = normed * norm_gain
    activated = jax.nn.silu(scaled).astype(jnp.bfloat16)
    grad_tokens = gathered_rows(mid_grad, "tp")
    proj_grad, grad_tokens = reduced_products(grad_tokens, activated, "sp")
    act_grad = lax.dot_general(
        grad_tokens, out_weight, (((1,), (1,)), ((), ())), preferred_element_type=jnp.float32
    )
    scaled_grad = act_grad * silu_grad(scaled) * norm_gain
    grad_total, corr_total = lax.psum(
        (jnp.sum(scaled_grad, axis=1), jnp.sum(scaled_grad * normed, axis=1)), "tp"
    )
    grad_mean = (grad_total / model_width)[:, None]
    grad_corr = (corr_total / model_width)[:, None]
    conv_grad = (inv_scale * (scaled_grad - grad_mean - normed * grad_corr)).astype(jnp.bfloat16)
    halo_width = conv_taps.shape[0] // 2
    padded = extended(conv_grad, (("sp", 0),), halo_width)
    seq_rows = conv_grad.shape[0]
    accumulated = jnp.zeros(conv_grad.shape, jnp.float32)
    for offset in range(conv_taps.shape[0]):
        lead = 2 * halo_width - offset
        accumulated = accumulated + conv_taps[offset] * padded[lead : lead + seq_rows]
    input_grad = accumulated.astype(jnp.bfloat16)
    return (gate_grad, up_grad, down_grad, proj_grad, input_grad)


def solution(mesh):
    in_specs = (
        P(("sp", "tp"), None),
        P(("sp", "tp"), None),
        P(("sp", "tp"), None),
        P(("sp", "tp"), None),
        P("sp", "tp"),
        P(None, "tp"),
        P("tp"),
        P("tp", None),
        P("sp", None, "tp"),
        P("sp", None, "tp"),
        P("sp", "tp", None),
    )
    out_specs = (
        P("sp", None, "tp"),
        P("sp", None, "tp"),
        P("sp", "tp", None),
        P("sp", "tp"),
        P("sp", "tp"),
    )
    return jax.shard_map(
        per_device, mesh=mesh, in_specs=in_specs, out_specs=out_specs, check_vma=False
    )
```

profile of v0, /device:TPU:0, one launch (start us, length us, event | category | flops | bytes accessed | tf_op | source)
XLA Modules:
  0.0 249.9 jit_solution(11022024559254988577)
XLA Ops:
  0.6 4.1 %collective-permute-start.1 = (bf16[128,2048]{1,0:T(8,128)(2,1)}, bf16[128,2048]{1,0:T(8,128)(2,1)S(1)}, u32[]{:S(2)}, u32[]{:S(2)}) collective-permute-start(bf16[128,2048]{1,0:T(8,128)(2,1)} %param.11), channel_id=1, source_target_pairs={{0,16},{2,18},{4,20},{6,22},{8,24},{10,26},{12,28},{14,30},{16,0},... | collective-permute-start | bytes 1572872 | tf_op jit(solution)/shard_map/ppermute | solution.py:189
  7.0 21.2 %collective-permute-done = s32[128,2]{0,1:T(2,128)S(1)} collective-permute-done((s32[128,2]{0,1:T(2,128)S(1)}, s32[128,2]{0,1:T(2,128)S(1)}, u32[]{:S(2)}, u32[]{:S(2)}) %collective-permute-start) | collective-permute-done | bytes 1056 | tf_op jit(solution)/shard_map/ppermute | solution.py:189
  31.6 4.5 %all-to-all-start = ((bf16[8,2,1,32,2048]{4,3,1,2,0:T(8,128)(2,1)}), bf16[8,2,1,32,2048]{4,3,1,2,0:T(8,128)(2,1)}, u32[]{:S(2)}, u32[]{:S(2)}) async-start(bf16[8,2,1,32,2048]{4,3,1,2,0:T(8,128)(2,1)} %bitcast.168), calls=%async_computation | async-start | bytes 4194304 | tf_op jit(solution)/shard_map/all_to_all | solution.py:205
  36.1 3.0 %collective-permute-start.4 = (bf16[128,2048]{1,0:T(8,128)(2,1)S(1)}, bf16[128,2048]{1,0:T(8,128)(2,1)S(1)}, u32[]{:S(2)}, u32[]{:S(2)}) collective-permute-start(bf16[128,2048]{1,0:T(8,128)(2,1)S(1)} %copy-done.21), channel_id=1, source_target_pairs={{0,16},{2,18},{4,20},{6,22},{8,24},{10,26},{12,28},{14,30},{16,0},... | collective-permute-start | bytes 1572872 | tf_op jit(solution)/shard_map/ppermute | solution.py:189
  39.2 30.7 %collective-permute-done.3 = f32[128,2]{0,1:T(2,128)S(1)} collective-permute-done((f32[128,2]{0,1:T(2,128)S(1)}, f32[128,2]{0,1:T(2,128)S(1)}, u32[]{:S(2)}, u32[]{:S(2)}) %collective-permute-start.3) | collective-permute-done | bytes 1056 | tf_op jit(solution)/shard_map/ppermute | solution.py:189
  72.1 11.4 %all-to-all-start.1 = ((bf16[8,2,1,32,2048]{4,3,1,2,0:T(8,128)(2,1)}), bf16[8,2,1,32,2048]{4,3,1,2,0:T(8,128)(2,1)}, u32[]{:S(2)}, u32[]{:S(2)}) async-start(bf16[8,2,1,32,2048]{4,3,1,2,0:T(8,128)(2,1)} %bitcast.172), calls=%async_computation.1 | async-start | bytes 4194304 | tf_op jit(solution)/shard_map/all_to_all | solution.py:205
  83.5 4.4 %fusion.9 = f32[512,512]{1,0:T(8,128)} fusion(bf16[512,2048]{1,0:T(8,128)(2,1)} %bitcast.2, bf16[1,2048,512]{2,1,0:T(8,128)(2,1)} %param.20), kind=kOutput, calls=%fused_computation.47 | convolution fusion | flops 1073741824 | bytes 5242880 | tf_op jit(solution)/shard_map/dot_general | solution.py:91
  88.0 4.0 %fusion.17 = f32[512,512]{1,0:T(8,128)} fusion(bf16[512,2048]{1,0:T(8,128)(2,1)} %bitcast.2, bf16[1,2048,512]{2,1,0:T(8,128)(2,1)S(1)} %copy-done), kind=kOutput, calls=%fused_computation.55 | convolution fusion | flops 1073741824 | bytes 5242880 | tf_op jit(solution)/shard_map/dot_general | solution.py:91
  92.0 2.3 fusion.7
  96.4 12.6 %all-to-all-done.1 = bf16[8,2,1,32,2048]{4,3,1,2,0:T(8,128)(2,1)} async-done(((bf16[8,2,1,32,2048]{4,3,1,2,0:T(8,128)(2,1)}), bf16[8,2,1,32,2048]{4,3,1,2,0:T(8,128)(2,1)}, u32[]{:S(2)}, u32[]{:S(2)}) %all-to-all-start.1) | async-done | bytes 2097184 | tf_op jit(solution)/shard_map/all_to_all | solution.py:205
  109.1 4.4 %collective-permute-done.5 = bf16[512,2048]{1,0:T(8,128)(2,1)S(1)} collective-permute-done((bf16[512,2048]{1,0:T(8,128)(2,1)}, bf16[512,2048]{1,0:T(8,128)(2,1)S(1)}, u32[]{:S(2)}, u32[]{:S(2)}) %collective-permute-start.5) | collective-permute-done | bytes 2097184 | tf_op jit(solution)/shard_map/ppermute | solution.py:105
  113.5 4.6 %multiply_convert_fusion.3 = (bf16[512,512]{1,0:T(8,128)(2,1)S(1)}, bf16[512,512]{1,0:T(8,128)(2,1)S(1)}) fusion(f32[512,512]{1,0:T(8,128)} %fusion.15, f32[512,512]{1,0:T(8,128)} %fusion.7, bf16[512,2048]{1,0:T(8,128)(2,1)S(1)} %collective-permute-done.5, bf16[1,512,2048]{2,1,0:T(8,128)(2,1)} %param.21), kind=kOutput, calls=%fused_computation.93 | convolution fusion | flops 1077149696 | bytes 7340032 | tf_op jit(solution)/shard_map/dot_general | solution.py:91
  122.1 3.3 %multiply_convert_fusion.5 = (bf16[512,512]{1,0:T(8,128)(2,1)S(1)}, bf16[512,512]{1,0:T(8,128)(2,1)S(1)}) fusion(f32[512,512]{1,0:T(8,128)S(1)} %copy-done.19, f32[512,512]{1,0:T(8,128)S(1)} %copy-done.17, bf16[512,2048]{1,0:T(8,128)(2,1)} %bitcast.7, bf16[1,512,2048]{2,1,0:T(8,128)(2,1)S(1)} %copy-done.26), kind=kOutput, calls=%fused_computation.97 | convolution fusion | flops 1077149696 | bytes 7340032 | tf_op jit(solution)/shard_map/dot_general | solution.py:91
  129.6 4.6 %all-to-all-start.2 = ((bf16[16,1,32,2048]{3,2,1,0:T(8,128)(2,1)}), bf16[16,1,32,2048]{3,2,1,0:T(8,128)(2,1)}, u32[]{:S(2)}, u32[]{:S(2)}) async-start(bf16[16,1,32,2048]{3,2,1,0:T(8,128)(2,1)} %bitcast.12), calls=%async_computation.2 | async-start | bytes 4194304 | tf_op jit(solution)/shard_map/all_to_all | solution.py:244
  134.4 2.7 %all-reduce.2 = (f32[256]{0:T(256)S(1)}, f32[256]{0:T(256)S(1)}) all-reduce(f32[256]{0:T(256)S(1)} %get-tuple-element.66, f32[256]{0:T(256)S(1)} %get-tuple-element.65), channel_id=1, replica_groups=mesh['sp'=16,'tp'=2] {'tp'}, use_global_device_ids=true, to_apply=%region_4.5 | all-reduce | flops 512 | bytes 4096 | tf_op jit(solution)/shard_map/psum | solution.py:179
  137.2 2.9 %fusion.103 = f32[2048,512]{1,0:T(8,128)S(1)} fusion(bf16[512,2048]{1,0:T(8,128)(2,1)} %bitcast.2, bf16[512,512]{1,0:T(8,128)(2,1)S(1)} %copy-done.15), kind=kOutput, calls=%fused_computation.225 | convolution fusion | flops 1073741824 | bytes 6815744 | tf_op jit(solution)/shard_map/dot_general | solution.py:97
  140.1 3.0 %fusion.102 = f32[2048,512]{1,0:T(8,128)S(1)} fusion(bf16[512,2048]{1,0:T(8,128)(2,1)} %bitcast.2, bf16[512,512]{1,0:T(8,128)(2,1)S(1)} %get-tuple-element.74), kind=kOutput, calls=%fused_computation.224 | convolution fusion | flops 1073741824 | bytes 6815744 | tf_op jit(solution)/shard_map/dot_general | solution.py:97
  143.2 3.1 %fusion.46 = f32[512,2048]{1,0:T(8,128)S(1)} fusion(bf16[512,2048]{1,0:T(8,128)(2,1)} %bitcast.7, f32[512,512]{1,0:T(8,128)S(1)} %copy-done.18, f32[512,512]{1,0:T(8,128)S(1)} %copy-done.20), kind=kOutput, calls=%fused_computation.112 | convolution fusion | flops 1075314688 | bytes 8388608 | tf_op jit(solution)/shard_map/dot_general | solution.py:97
  146.3 3.4 %add_bitcast_fusion.1 = f32[1,2048,512]{2,1,0:T(8,128)} fusion(f32[2048,512]{1,0:T(8,128)S(1)} %fusion.103, bf16[512,2048]{1,0:T(8,128)(2,1)S(1)} %copy-done.3, bf16[512,512]{1,0:T(8,128)(2,1)S(1)} %copy-done.11), kind=kOutput, calls=%fused_computation.1 | convolution fusion | flops 1074790400 | bytes 11010048 | tf_op jit(solution)/shard_map/dot_general | solution.py:97
  149.7 3.4 %add_bitcast_fusion.2 = f32[1,2048,512]{2,1,0:T(8,128)} fusion(f32[2048,512]{1,0:T(8,128)S(1)} %fusion.102, bf16[512,2048]{1,0:T(8,128)(2,1)S(1)} %copy-done.3, bf16[512,512]{1,0:T(8,128)(2,1)S(1)} %get-tuple-element.76), kind=kOutput, calls=%fused_computation.2 | convolution fusion | flops 1074790400 | bytes 11010048 | tf_op jit(solution)/shard_map/dot_general | solution.py:97
  153.2 3.4 %add_bitcast_fusion = f32[1,512,2048]{2,1,0:T(8,128)} fusion(f32[512,2048]{1,0:T(8,128)S(1)} %fusion.46, bf16[512,2048]{1,0:T(8,128)(2,1)S(1)} %copy-done.9, f32[512,512]{1,0:T(8,128)S(1)} %copy-done.6, f32[512,512]{1,0:T(8,128)S(1)} %copy-done.7), kind=kOutput, calls=%fused_computation | convolution fusion | flops 1076363264 | bytes 12582912 | tf_op jit(solution)/shard_map/dot_general | solution.py:97
  156.6 20.8 %all-to-all-done.2 = bf16[16,1,32,2048]{3,2,1,0:T(8,128)(2,1)} async-done(((bf16[16,1,32,2048]{3,2,1,0:T(8,128)(2,1)}), bf16[16,1,32,2048]{3,2,1,0:T(8,128)(2,1)}, u32[]{:S(2)}, u32[]{:S(2)}) %all-to-all-start.2) | async-done | bytes 2097184 | tf_op jit(solution)/shard_map/all_to_all | solution.py:244
  186.5 6.1 %collective-permute-start.10 = (bf16[2,2,2,128,256]{4,3,0,1,2:T(8,128)(2,1)}, bf16[2,2,2,128,256]{4,3,0,1,2:T(8,128)(2,1)}, u32[]{:S(2)}, u32[]{:S(2)}) collective-permute-start(bf16[2,2,2,128,256]{4,3,0,1,2:T(8,128)(2,1)} %bitcast.167), channel_id=1, source_target_pairs={{0,8},{2,10},{4,12},{6,14},{8,0},{10,2},{12,4},{14,6},{16,24},{18,... | collective-permute-start | bytes 1572872 | tf_op jit(solution)/shard_map/ppermute | solution.py:82
  194.3 2.5 %collective-permute-start.9 = (bf16[2,2,2,128,384]{4,3,0,2,1:T(8,128)(2,1)S(1)}, bf16[2,2,2,128,384]{4,3,0,2,1:T(8,128)(2,1)}, u32[]{:S(2)}, u32[]{:S(2)}) collective-permute-start(bf16[2,2,2,128,384]{4,3,0,2,1:T(8,128)(2,1)S(1)} %bitcast.173), channel_id=1, source_target_pairs={{0,4},{2,6},{4,0},{6,2},{8,12},{10,14},{12,8},{14,10},{16,20},{18,... | collective-permute-start | bytes 2359304 | tf_op jit(solution)/shard_map/ppermute | solution.py:82
  196.8 3.0 %fusion.97 = (f32[256]{0:T(256)S(1)}, f32[256]{0:T(256)S(1)}, f32[256,1024]{1,0:T(8,128)}) fusion(f32[256]{0:T(256)S(1)} %get-tuple-element.117, f32[256]{0:T(256)S(1)} %get-tuple-element.116, bf16[256,1024]{1,0:T(8,128)(2,1)S(1)} %copy-done.13, f32[1024]{0:T(1024)S(1)} %copy-done.27, bf16[256,2048]{1,0:T(8,128)(2,1)S(1)} %select_select_fusion, ...), kind=kOutput, calls=%fused_computation.219 | convolution fusion | flops 1077935616 | bytes 6823936 | tf_op jit(solution)/shard_map/dot_general | solution.py:261
  199.8 3.0 %all-reduce.1 = (f32[256]{0:T(256)S(1)}, f32[256]{0:T(256)}) all-reduce(f32[256]{0:T(256)S(1)} %get-tuple-element.64, f32[256]{0:T(256)S(1)} %get-tuple-element.63), channel_id=1, replica_groups=mesh['sp'=16,'tp'=2] {'tp'}, use_global_device_ids=true, to_apply=%region_11.12 | all-reduce | flops 512 | bytes 4096 | tf_op jit(solution)/shard_map/psum | solution.py:265
  205.2 7.1 %collective-permute-done.8 = bf16[2,2,2,128,384]{4,3,0,1,2:T(8,128)(2,1)} collective-permute-done((bf16[2,2,2,128,384]{4,3,0,1,2:T(8,128)(2,1)}, bf16[2,2,2,128,384]{4,3,0,1,2:T(8,128)(2,1)}, u32[]{:S(2)}, u32[]{:S(2)}) %collective-permute-start.8) | collective-permute-done | bytes 786464 | tf_op jit(solution)/shard_map/ppermute | solution.py:82
  221.2 5.8 %collective-permute-done.13 = bf16[2,2,128,256]{3,2,0,1:T(8,128)(2,1)S(1)} collective-permute-done((bf16[2,2,128,256]{3,2,0,1:T(8,128)(2,1)S(1)}, bf16[2,2,128,256]{3,2,0,1:T(8,128)(2,1)S(1)}, u32[]{:S(2)}, u32[]{:S(2)}) %collective-permute-start.13) | collective-permute-done | bytes 262176 | tf_op jit(solution)/shard_map/ppermute | solution.py:82
  231.6 4.5 %collective-permute-start.21 = (bf16[15,1024]{1,0:T(8,128)(2,1)S(1)}, bf16[15,1024]{1,0:T(8,128)(2,1)S(1)}, u32[]{:S(2)}, u32[]{:S(2)}) collective-permute-start(bf16[15,1024]{1,0:T(8,128)(2,1)S(1)} %get-tuple-element.84), channel_id=1, source_target_pairs={{0,2},{2,4},{4,6},{6,8},{8,10},{10,12},{12,14},{14,16},{16,18},{18... | collective-permute-start | bytes 92168 | tf_op jit(solution)/shard_map/ppermute | solution.py:14
  236.4 2.8 %collective-permute-start.19 = (bf16[128,256]{1,0:T(8,128)(2,1)S(1)}, bf16[128,256]{1,0:T(8,128)(2,1)S(1)}, u32[]{:S(2)}, u32[]{:S(2)}) collective-permute-start(bf16[128,256]{1,0:T(8,128)(2,1)S(1)} %fusion.90), channel_id=1, source_target_pairs={{0,16},{2,18},{4,20},{6,22},{8,24},{10,26},{12,28},{14,30},{16,0},... | collective-permute-start | bytes 196616 | tf_op jit(solution)/shard_map/ppermute | solution.py:82
  239.5 2.8 %collective-permute-start.17 = (bf16[128,384]{1,0:T(8,128)(2,1)S(1)}, bf16[128,384]{1,0:T(8,128)(2,1)S(1)}, u32[]{:S(2)}, u32[]{:S(2)}) collective-permute-start(bf16[128,384]{1,0:T(8,128)(2,1)S(1)} %fusion.88), channel_id=1, source_target_pairs={{0,16},{2,18},{4,20},{6,22},{8,24},{10,26},{12,28},{14,30},{16,0},... | collective-permute-start | bytes 294920 | tf_op jit(solution)/shard_map/ppermute | solution.py:82
  242.3 5.4 %add_convert_fusion.3 = bf16[256,1024]{1,0:T(8,128)(2,1)} fusion(bf16[256,1024]{1,0:T(8,128)(2,1)S(1)} %fusion.38, bf16[15,1024]{1,0:T(8,128)(2,1)S(1)} %collective-permute-done.21, bf16[15,1024]{1,0:T(8,128)(2,1)S(1)} %collective-permute-done.20, f32[1024]{0:T(1024)S(1)} %bitcast.184, f32[1024]{0:T(1024)S(1)} %bitcast.185, f32[1024]{0:T(1024)S(1)} %bitcast.187, ...), kind=kLoop, calls=%fused_computation.90 | loop fusion | flops 47972352 | bytes 1236992 | tf_op jit(solution)/shard_map/convert_element_type | solution.py:278
  (151 shorter events, 47.6 us)
Async XLA Ops:
  0.6 87.4 %copy-start = (bf16[1,2048,512]{2,1,0:T(8,128)(2,1)S(1)}, bf16[1,2048,512]{2,1,0:T(8,128)(2,1)}, u32[]{:S(2)}) copy-start(bf16[1,2048,512]{2,1,0:T(8,128)(2,1)} %param.19) | copy-start | bytes 6291460
  0.6 27.8 %collective-permute-start.1 = (bf16[128,2048]{1,0:T(8,128)(2,1)}, bf16[128,2048]{1,0:T(8,128)(2,1)S(1)}, u32[]{:S(2)}, u32[]{:S(2)}) collective-permute-start(bf16[128,2048]{1,0:T(8,128)(2,1)} %param.11), channel_id=1, source_target_pairs={{0,16},{2,18},{4,20},{6,22},{8,24},{10,26},{12,28},{14,30},{16,0},... | collective-permute-start | bytes 1572872 | tf_op jit(solution)/shard_map/ppermute | solution.py:189
  6.8 21.4 %collective-permute-start = (s32[128,2]{0,1:T(2,128)S(1)}, s32[128,2]{0,1:T(2,128)S(1)}, u32[]{:S(2)}, u32[]{:S(2)}) collective-permute-start(s32[128,2]{0,1:T(2,128)S(1)} %multiply_add_fusion), channel_id=1, source_target_pairs={{0,16},{2,18},{4,20},{6,22},{8,24},{10,26},{12,28},{14,30},{16,0},... | collective-permute-start | bytes 3080 | tf_op jit(solution)/shard_map/ppermute | solution.py:189
  31.6 7.5 %copy-start.24 = (f32[128,2]{0,1:T(2,128)S(1)}, f32[128,2]{0,1:T(2,128)}, u32[]{:S(2)}) copy-start(f32[128,2]{0,1:T(2,128)} %param.14) | copy-start | bytes 3076
  31.6 40.5 %all-to-all-start = ((bf16[8,2,1,32,2048]{4,3,1,2,0:T(8,128)(2,1)}), bf16[8,2,1,32,2048]{4,3,1,2,0:T(8,128)(2,1)}, u32[]{:S(2)}, u32[]{:S(2)}) async-start(bf16[8,2,1,32,2048]{4,3,1,2,0:T(8,128)(2,1)} %bitcast.168), calls=%async_computation | async-start | bytes 4194304 | tf_op jit(solution)/shard_map/all_to_all | solution.py:205
  36.1 34.0 %collective-permute-start.4 = (bf16[128,2048]{1,0:T(8,128)(2,1)S(1)}, bf16[128,2048]{1,0:T(8,128)(2,1)S(1)}, u32[]{:S(2)}, u32[]{:S(2)}) collective-permute-start(bf16[128,2048]{1,0:T(8,128)(2,1)S(1)} %copy-done.21), channel_id=1, source_target_pairs={{0,16},{2,18},{4,20},{6,22},{8,24},{10,26},{12,28},{14,30},{16,0},... | collective-permute-start | bytes 1572872 | tf_op jit(solution)/shard_map/ppermute | solution.py:189
  39.1 30.8 %collective-permute-start.3 = (f32[128,2]{0,1:T(2,128)S(1)}, f32[128,2]{0,1:T(2,128)S(1)}, u32[]{:S(2)}, u32[]{:S(2)}) collective-permute-start(f32[128,2]{0,1:T(2,128)S(1)} %copy-done.24), channel_id=1, source_target_pairs={{0,16},{2,18},{4,20},{6,22},{8,24},{10,26},{12,28},{14,30},{16,0},... | collective-permute-start | bytes 3080 | tf_op jit(solution)/shard_map/ppermute | solution.py:189
  72.1 36.9 %all-to-all-start.1 = ((bf16[8,2,1,32,2048]{4,3,1,2,0:T(8,128)(2,1)}), bf16[8,2,1,32,2048]{4,3,1,2,0:T(8,128)(2,1)}, u32[]{:S(2)}, u32[]{:S(2)}) async-start(bf16[8,2,1,32,2048]{4,3,1,2,0:T(8,128)(2,1)} %bitcast.172), calls=%async_computation.1 | async-start | bytes 4194304 | tf_op jit(solution)/shard_map/all_to_all | solution.py:205
  83.5 8.4 %collective-permute-start.2 = (bf16[512,2048]{1,0:T(8,128)(2,1)}, bf16[512,2048]{1,0:T(8,128)(2,1)S(1)}, u32[]{:S(2)}, u32[]{:S(2)}) collective-permute-start(bf16[512,2048]{1,0:T(8,128)(2,1)} %bitcast.2), channel_id=1, source_target_pairs={{0,1},{1,0},{2,3},{3,2},{4,5},{5,4},{6,7},{7,6},{8,9},{9,8},{10,11... | collective-permute-start | bytes 6291464 | tf_op jit(solution)/shard_map/ppermute | solution.py:105
  109.1 4.4 %collective-permute-start.5 = (bf16[512,2048]{1,0:T(8,128)(2,1)}, bf16[512,2048]{1,0:T(8,128)(2,1)S(1)}, u32[]{:S(2)}, u32[]{:S(2)}) collective-permute-start(bf16[512,2048]{1,0:T(8,128)(2,1)} %bitcast.7), channel_id=1, source_target_pairs={{0,1},{1,0},{2,3},{3,2},{4,5},{5,4},{6,7},{7,6},{8,9},{9,8},{10,11... | collective-permute-start | bytes 6291464 | tf_op jit(solution)/shard_map/ppermute | solution.py:105
  121.2 5.5 %collective-permute-start.6 = (bf16[512,2048]{1,0:T(8,128)(2,1)S(1)}, bf16[512,2048]{1,0:T(8,128)(2,1)S(1)}, u32[]{:S(2)}, u32[]{:S(2)}) collective-permute-start(bf16[512,2048]{1,0:T(8,128)(2,1)S(1)} %add_convert_fusion.1), channel_id=1, source_target_pairs={{0,1},{1,0},{2,3},{3,2},{4,5},{5,4},{6,7},{7,6},{8,9},{9,8},{10,11... | collective-permute-start | bytes 6291464 | tf_op jit(solution)/shard_map/ppermute | solution.py:135
  129.6 7.6 %copy-start.15 = (bf16[512,512]{1,0:T(8,128)(2,1)S(1)}, bf16[512,512]{1,0:T(8,128)(2,1)}, u32[]{:S(2)}) copy-start(bf16[512,512]{1,0:T(8,128)(2,1)} %copy-done.14) | copy-start | bytes 1572868
  129.6 47.8 %all-to-all-start.2 = ((bf16[16,1,32,2048]{3,2,1,0:T(8,128)(2,1)}), bf16[16,1,32,2048]{3,2,1,0:T(8,128)(2,1)}, u32[]{:S(2)}, u32[]{:S(2)}) async-start(bf16[16,1,32,2048]{3,2,1,0:T(8,128)(2,1)} %bitcast.12), calls=%async_computation.2 | async-start | bytes 4194304 | tf_op jit(solution)/shard_map/all_to_all | solution.py:244
  153.2 24.2 %copy-start.22 = (bf16[128,2048]{1,0:T(8,128)(2,1)S(1)}, bf16[128,2048]{1,0:T(8,128)(2,1)}, u32[]{:S(2)}) copy-start(bf16[128,2048]{1,0:T(8,128)(2,1)} %param.12) | copy-start | bytes 1572868
  156.6 23.0 %copy-start.23 = (f32[31,1024]{1,0:T(8,128)S(1)}, f32[31,1024]{1,0:T(8,128)}, u32[]{:S(2)}) copy-start(f32[31,1024]{1,0:T(8,128)} %param.16) | copy-start | bytes 380932
  179.5 2.0 collective-permute-start.7
  185.4 11.4 %copy-start.25 = (bf16[1024,2048]{1,0:T(8,128)(2,1)S(1)}, bf16[1024,2048]{1,0:T(8,128)(2,1)}, u32[]{:S(2)}) copy-start(bf16[1024,2048]{1,0:T(8,128)(2,1)} %param.18) | copy-start | bytes 12582916
  186.5 18.7 %collective-permute-start.10 = (bf16[2,2,2,128,256]{4,3,0,1,2:T(8,128)(2,1)}, bf16[2,2,2,128,256]{4,3,0,1,2:T(8,128)(2,1)}, u32[]{:S(2)}, u32[]{:S(2)}) collective-permute-start(bf16[2,2,2,128,256]{4,3,0,1,2:T(8,128)(2,1)} %bitcast.167), channel_id=1, source_target_pairs={{0,8},{2,10},{4,12},{6,14},{8,0},{10,2},{12,4},{14,6},{16,24},{18,... | collective-permute-start | bytes 1572872 | tf_op jit(solution)/shard_map/ppermute | solution.py:82
  192.6 19.6 %collective-permute-start.8 = (bf16[2,2,2,128,384]{4,3,0,1,2:T(8,128)(2,1)}, bf16[2,2,2,128,384]{4,3,0,1,2:T(8,128)(2,1)}, u32[]{:S(2)}, u32[]{:S(2)}) collective-permute-start(bf16[2,2,2,128,384]{4,3,0,1,2:T(8,128)(2,1)} %bitcast.166), channel_id=1, source_target_pairs={{0,2},{2,0},{4,6},{6,4},{8,10},{10,8},{12,14},{14,12},{16,18},{18,... | collective-permute-start | bytes 2359304 | tf_op jit(solution)/shard_map/ppermute | solution.py:82
  194.3 19.9 %collective-permute-start.9 = (bf16[2,2,2,128,384]{4,3,0,2,1:T(8,128)(2,1)S(1)}, bf16[2,2,2,128,384]{4,3,0,2,1:T(8,128)(2,1)}, u32[]{:S(2)}, u32[]{:S(2)}) collective-permute-start(bf16[2,2,2,128,384]{4,3,0,2,1:T(8,128)(2,1)S(1)} %bitcast.173), channel_id=1, source_target_pairs={{0,4},{2,6},{4,0},{6,2},{8,12},{10,14},{12,8},{14,10},{16,20},{18,... | collective-permute-start | bytes 2359304 | tf_op jit(solution)/shard_map/ppermute | solution.py:82
  215.5 11.4 %collective-permute-start.11 = (bf16[2,2,128,384]{3,2,0,1:T(8,128)(2,1)S(1)}, bf16[2,2,128,384]{3,2,0,1:T(8,128)(2,1)S(1)}, u32[]{:S(2)}, u32[]{:S(2)}) collective-permute-start(bf16[2,2,128,384]{3,2,0,1:T(8,128)(2,1)S(1)} %fusion.80), channel_id=1, source_target_pairs={{0,4},{2,6},{4,0},{6,2},{8,12},{10,14},{12,8},{14,10},{16,20},{18,... | collective-permute-start | bytes 1179656 | tf_op jit(solution)/shard_map/ppermute | solution.py:82
  218.7 9.5 %collective-permute-start.12 = (bf16[2,2,128,384]{3,2,0,1:T(8,128)(2,1)S(1)}, bf16[2,2,128,384]{3,2,0,1:T(8,128)(2,1)S(1)}, u32[]{:S(2)}, u32[]{:S(2)}) collective-permute-start(bf16[2,2,128,384]{3,2,0,1:T(8,128)(2,1)S(1)} %fusion.81), channel_id=1, source_target_pairs={{0,8},{2,10},{4,12},{6,14},{8,0},{10,2},{12,4},{14,6},{16,24},{18,... | collective-permute-start | bytes 1179656 | tf_op jit(solution)/shard_map/ppermute | solution.py:82
  220.3 6.7 %collective-permute-start.13 = (bf16[2,2,128,256]{3,2,0,1:T(8,128)(2,1)S(1)}, bf16[2,2,128,256]{3,2,0,1:T(8,128)(2,1)S(1)}, u32[]{:S(2)}, u32[]{:S(2)}) collective-permute-start(bf16[2,2,128,256]{3,2,0,1:T(8,128)(2,1)S(1)} %fusion.82), channel_id=1, source_target_pairs={{0,2},{2,0},{4,6},{6,4},{8,10},{10,8},{12,14},{14,12},{16,18},{18,... | collective-permute-start | bytes 786440 | tf_op jit(solution)/shard_map/ppermute | solution.py:82
  228.5 7.7 %collective-permute-start.16 = (bf16[2,128,256]{2,1,0:T(8,128)(2,1)S(1)}, bf16[2,128,256]{2,1,0:T(8,128)(2,1)S(1)}, u32[]{:S(2)}, u32[]{:S(2)}) collective-permute-start(bf16[2,128,256]{2,1,0:T(8,128)(2,1)S(1)} %fusion.87), channel_id=1, source_target_pairs={{0,4},{2,6},{4,0},{6,2},{8,12},{10,14},{12,8},{14,10},{16,20},{18,... | collective-permute-start | bytes 393224 | tf_op jit(solution)/shard_map/ppermute | solution.py:82
  229.2 7.0 %collective-permute-start.15 = (bf16[2,128,384]{2,1,0:T(8,128)(2,1)S(1)}, bf16[2,128,384]{2,1,0:T(8,128)(2,1)S(1)}, u32[]{:S(2)}, u32[]{:S(2)}) collective-permute-start(bf16[2,128,384]{2,1,0:T(8,128)(2,1)S(1)} %fusion.84), channel_id=1, source_target_pairs={{0,2},{2,0},{4,6},{6,4},{8,10},{10,8},{12,14},{14,12},{16,18},{18,... | collective-permute-start | bytes 589832 | tf_op jit(solution)/shard_map/ppermute | solution.py:82
  229.8 6.5 %collective-permute-start.14 = (bf16[2,128,384]{2,1,0:T(8,128)(2,1)S(1)}, bf16[2,128,384]{2,1,0:T(8,128)(2,1)S(1)}, u32[]{:S(2)}, u32[]{:S(2)}) collective-permute-start(bf16[2,128,384]{2,1,0:T(8,128)(2,1)S(1)} %fusion.83), channel_id=1, source_target_pairs={{0,8},{2,10},{4,12},{6,14},{8,0},{10,2},{12,4},{14,6},{16,24},{18,... | collective-permute-start | bytes 589832 | tf_op jit(solution)/shard_map/ppermute | solution.py:82
  230.3 11.9 %collective-permute-start.20 = (bf16[15,1024]{1,0:T(8,128)(2,1)S(1)}, bf16[15,1024]{1,0:T(8,128)(2,1)S(1)}, u32[]{:S(2)}, u32[]{:S(2)}) collective-permute-start(bf16[15,1024]{1,0:T(8,128)(2,1)S(1)} %get-tuple-element.83), channel_id=1, source_target_pairs={{2,0},{4,2},{6,4},{8,6},{10,8},{12,10},{14,12},{16,14},{18,16},{20... | collective-permute-start | bytes 92168 | tf_op jit(solution)/shard_map/ppermute | solution.py:17
  231.6 10.6 %collective-permute-start.21 = (bf16[15,1024]{1,0:T(8,128)(2,1)S(1)}, bf16[15,1024]{1,0:T(8,128)(2,1)S(1)}, u32[]{:S(2)}, u32[]{:S(2)}) collective-permute-start(bf16[15,1024]{1,0:T(8,128)(2,1)S(1)} %get-tuple-element.84), channel_id=1, source_target_pairs={{0,2},{2,4},{4,6},{6,8},{8,10},{10,12},{12,14},{14,16},{16,18},{18... | collective-permute-start | bytes 92168 | tf_op jit(solution)/shard_map/ppermute | solution.py:14
  236.3 13.6 %copy-start.1 = (bf16[1,2048,512]{2,1,0:T(8,128)(2,1)S(1)}, bf16[1,2048,512]{2,1,0:T(8,128)(2,1)}, u32[]{:S(2)}) copy-start(bf16[1,2048,512]{2,1,0:T(8,128)(2,1)} %param.19) | copy-start | bytes 6291460
  236.4 11.3 %collective-permute-start.19 = (bf16[128,256]{1,0:T(8,128)(2,1)S(1)}, bf16[128,256]{1,0:T(8,128)(2,1)S(1)}, u32[]{:S(2)}, u32[]{:S(2)}) collective-permute-start(bf16[128,256]{1,0:T(8,128)(2,1)S(1)} %fusion.90), channel_id=1, source_target_pairs={{0,16},{2,18},{4,20},{6,22},{8,24},{10,26},{12,28},{14,30},{16,0},... | collective-permute-start | bytes 196616 | tf_op jit(solution)/shard_map/ppermute | solution.py:82
  239.3 8.6 %collective-permute-start.18 = (bf16[128,384]{1,0:T(8,128)(2,1)S(1)}, bf16[128,384]{1,0:T(8,128)(2,1)S(1)}, u32[]{:S(2)}, u32[]{:S(2)}) collective-permute-start(bf16[128,384]{1,0:T(8,128)(2,1)S(1)} %fusion.89), channel_id=1, source_target_pairs={{0,16},{2,18},{4,20},{6,22},{8,24},{10,26},{12,28},{14,30},{16,0},... | collective-permute-start | bytes 294920 | tf_op jit(solution)/shard_map/ppermute | solution.py:82
  239.5 9.5 %collective-permute-start.17 = (bf16[128,384]{1,0:T(8,128)(2,1)S(1)}, bf16[128,384]{1,0:T(8,128)(2,1)S(1)}, u32[]{:S(2)}, u32[]{:S(2)}) collective-permute-start(bf16[128,384]{1,0:T(8,128)(2,1)S(1)} %fusion.88), channel_id=1, source_target_pairs={{0,16},{2,18},{4,20},{6,22},{8,24},{10,26},{12,28},{14,30},{16,0},... | collective-permute-start | bytes 294920 | tf_op jit(solution)/shard_map/ppermute | solution.py:82
  (21 other events, 63.4 us)
where the time goes:
time: 251 us; the launch traced here: 250 us
  waiting for transfers between devices  111 us (44%)
  matrix products  56.3 us (22%)
  starting transfers between devices  54.5 us (22%)
  other arithmetic  14.2 us (6%)
  local copies, waits for them, and re-layouts  7.4 us (3%)
  blocking collectives  5.69 us (2%)
    ppermute x4, waiting for transfers between devices, with_far(): lax.ppermute(block, 'sp', [(i, (i + half) % sp_count) for i in range(sp_c...  52 us
    dot_general x10, matrix products, row_product(): lax.dot_general(rows, matrix, (((1,), (dim,)), ((), ())), preferred_eleme...  25.9 us
    dot_general x7, matrix products, transposed_product(): lax.dot_general(left, right, (((0,), (0,)), ((), ())), preferred_element_...  20.9 us
    all_to_all x1, waiting for transfers between devices, per_device(): lax.all_to_all(back_rows, 'sp', split_axis=0, concat_axis=0, tiled=True)  20.8 us
    ppermute x12, starting transfers between devices, reduced_products(): lax.ppermute(block, axis, [(i, i ^ 1 << order[step]) for i in range(count)])  20.6 us
    ppermute x12, waiting for transfers between devices, reduced_products(): lax.ppermute(block, axis, [(i, i ^ 1 << order[step]) for i in range(count)])  19 us
    all_to_all x2, starting transfers between devices, within_half(): lax.all_to_all(block.reshape(half, 2, local_experts, capacity, model_widt...  15.9 us
    all_to_all x2, waiting for transfers between devices, within_half(): lax.all_to_all(block.reshape(half, 2, local_experts, capacity, model_widt...  12.6 us
  transfers between devices with their start and end apart: 25, of which 13 were waited for; matrix products, arithmetic and copies ran while one was open for 22% of the time, Pallas kernels for 0%

commit v1 on v0

v1 whole, which is shorter than its diff:
```python
import functools

import jax
import jax.numpy as jnp
from jax import lax
from jax.experimental import pallas as pl
from jax.experimental.pallas import tpu as pltpu
from jax.sharding import PartitionSpec as P

MESH = pl.DeviceIdType.MESH
NORM_EPS = 1e-05


def extended(block, sides, width):
    for axis, dim in sides:
        count = lax.axis_size(axis)
        forward = [(i, i + 1) for i in range(count - 1)]
        backward = [(target, source) for source, target in forward]
        low = lax.ppermute(
            lax.slice_in_dim(block, block.shape[dim] - width, None, axis=dim), axis, forward
        )
        high = lax.ppermute(lax.slice_in_dim(block, 0, width, axis=dim), axis, backward)
        block = jnp.concatenate([low, block, high], axis=dim)
    return block


def silu_grad(pre_act):
    logistic = jax.nn.sigmoid(pre_act)
    return logistic * (1.0 + pre_act * (1.0 - logistic))


def slot_targets(routes, experts, capacity):
    token_count, per_token = routes.shape
    flattened = routes.reshape(token_count * per_token)
    one_hot = flattened[:, None] == jnp.arange(experts, dtype=jnp.int32)[None, :]
    route_ids = jnp.arange(token_count * per_token, dtype=jnp.int32)
    before = (route_ids[None, :] < route_ids[:, None]).astype(jnp.bfloat16)
    earlier = jnp.dot(before, one_hot.astype(jnp.bfloat16), preferred_element_type=jnp.float32)
    positions = jnp.sum(jnp.where(one_hot, earlier, 0.0), axis=1).astype(jnp.int32)
    return (flattened * capacity + positions).reshape(token_count, per_token)


def halving_orders(count):
    bits = count.bit_length() - 1
    turned = min(bits, 3)
    return [
        [(start + step) % turned for step in range(turned)] + list(range(turned, bits))
        for start in range(turned)
    ]


def column_groups(columns, groups):
    lanes = 128
    tiles = columns // lanes
    sizes = [tiles // groups + (1 if g < tiles % groups else 0) for g in range(groups)]
    starts = [sum(sizes[:g]) * lanes for g in range(groups)]
    return [(start, size * lanes) for start, size in zip(starts, sizes) if size]


def picked(block, place, dim):
    return lax.dynamic_index_in_dim(block, place, dim, keepdims=False)


def reduced_products(rows, columns, axis):
    count = lax.axis_size(axis)
    tokens, width = rows.shape
    bits = count.bit_length() - 1
    own = lax.axis_index(axis)
    product = transposed_product(rows, columns).astype(jnp.bfloat16)
    cut = product.reshape((2,) * bits + (width // count, columns.shape[1]))
    orders = halving_orders(count)
    groups = column_groups(columns.shape[1], len(orders))
    orders = orders[: len(groups)]
    totals = [lax.slice_in_dim(cut, start, start + size, axis=bits + 1) for start, size in groups]
    left = [list(range(bits - 1, -1, -1)) for _ in groups]
    for step in range(bits):
        outgoing, kept = [], []
        for total, order, dims in zip(totals, orders, left):
            mine = (own >> order[step]) & 1
            dim = dims.index(order[step])
            dims.pop(dim)
            outgoing.append(picked(total, 1 - mine, dim).astype(jnp.bfloat16))
            kept.append(picked(total, mine, dim).astype(jnp.float32))
        if step == 0:
            outgoing, rows = lax.optimization_barrier((outgoing, rows))
        arrived = [
            lax.ppermute(block, axis, [(i, i ^ (1 << order[step])) for i in range(count)])
            for block, order in zip(outgoing, orders)
        ]
        arrived = lax.optimization_barrier(arrived)
        totals = [own_part + got.astype(jnp.float32) for own_part, got in zip(kept, arrived)]
    return jnp.concatenate(totals, axis=1), rows


def row_product(rows, matrix, dim=0):
    return lax.dot_general(
        rows, matrix, (((1,), (dim,)), ((), ())), preferred_element_type=jnp.float32
    )


def transposed_product(left, right):
    return lax.dot_general(
        left, right, (((0,), (0,)), ((), ())), preferred_element_type=jnp.float32
    )


def line_extent(count):
    bits = count.bit_length() - 1
    return 1 << -(-bits // 3)


def chunk_orders(extent):
    orders = []
    for own in range(extent):
        toward = [i for i in range(own + 1, extent)] if 2 * own < extent - 1 else [i for i in range(own - 1, -1, -1)]
        back = [i for i in range(extent) if i != own and i not in toward]
        back.sort(key=lambda i: abs(i - own))
        if own in (0, extent - 1):
            order = toward
        else:
            order = toward[:1] + back + toward[1:]
        orders.append([own] + order)
    return orders


def relay_orders(extent):
    return [
        sorted(
            (i for i in range(extent) if i != own),
            key=lambda i: (own if i > own else extent - 1 - own, abs(i - own)),
        )
        for own in range(extent)
    ]


def looked_up(table, row, column):
    value = jnp.int32(0)
    for i, entries in enumerate(table):
        for k, entry in enumerate(entries):
            value = value + jnp.where((row == i) & (column == k), entry, 0)
    return value


def routed_kernel(
    extent,
    plane,
    capacity,
    mid_hbm,
    cot_hbm,
    meta,
    gate_hbm,
    up_hbm,
    down_hbm,
    tokens_out,
    inputs_out,
    routed_out,
    hidden_out,
    gate_pre_out,
    up_pre_out,
    tok,
    metas,
    picks,
    rows,
    gate,
    up,
    down,
    pre_gate,
    pre_up,
    hidden,
    gate_pre,
    up_pre,
    part_own,
    part_sent,
    part_got,
    ret_sent,
    ret_got,
    line_sent,
    line_got,
    total,
    tokens,
    load_sem,
    meta_sems,
    tok_send,
    tok_recv,
    row_send,
    row_recv,
    swap_send,
    swap_recv,
    part_sems,
    ret_send,
    ret_recv,
    line_send,
    line_recv,
    out_sems,
    token_sems,
):
    sp, tp = lax.axis_index("sp"), lax.axis_index("tp")
    z, p = sp // plane, sp % plane
    slots = plane * capacity
    token_count, width = tok.shape[2], tok.shape[3]
    other = 1 - tp
    step = min(512, width)
    columns = width // step
    orders, relays = chunk_orders(extent), relay_orders(extent)
    load_from = [mid_hbm, cot_hbm]

    def remote(src, dst, send, recv, to_sp, to_tp):
        return pltpu.make_async_remote_copy(
            src_ref=src,
            dst_ref=dst,
            send_sem=send,
            recv_sem=recv,
            device_id=(to_sp, to_tp),
            device_id_type=MESH,
        )

    loads = [
        pltpu.make_async_copy(mid_hbm, tok.at[0, z], load_sem.at[0]),
        pltpu.make_async_copy(cot_hbm, tok.at[1, z], load_sem.at[1]),
        pltpu.make_async_copy(gate_hbm, gate, load_sem.at[2]),
        pltpu.make_async_copy(up_hbm, up, load_sem.at[3]),
        pltpu.make_async_copy(down_hbm, down, load_sem.at[4]),
    ]
    for load in loads:
        load.start()
    metas[z] = meta[...]

    barrier = pltpu.get_barrier_semaphore()

    def greet(to_sp, to_tp):
        pl.semaphore_signal(barrier, inc=1, device_id=(to_sp, to_tp), device_id_type=MESH)

    def line_peer(i):
        return lax.rem(z + i, extent)

    def plane_peer(i):
        return lax.rem(p + i, plane)

    for i in range(1, extent):
        greet(line_peer(i) * plane + p, tp)

    @pl.loop(1, plane)
    def _(i):
        greet(z * plane + plane_peer(i), tp)

    greet(sp, other)
    pl.semaphore_wait(barrier, extent - 1 + plane - 1 + 1)

    def meta_copy(to_z, from_z):
        return remote(
            meta, metas.at[from_z], meta_sems.at[0, to_z], meta_sems.at[1, from_z], to_z * plane + p, tp
        )

    def tok_copy(t, origin, up_way):
        to_z = z + 1 if up_way else z - 1
        return remote(
            tok.at[t, origin],
            tok.at[t, origin],
            tok_send.at[t, origin, int(up_way)],
            tok_recv.at[t, origin],
            to_z * plane + p,
            tp,
        )

    def forwards(origin, up_way):
        if up_way:
            return (origin <= z) & (z < extent - 1)
        return (origin >= z) & (z > 0)

    def row_copy(t, origin, q):
        return remote(
            picks.at[t, origin, q],
            rows.at[t, origin, 0, p],
            row_send.at[t, origin, q],
            row_recv.at[t, origin, p],
            z * plane + q,
            tp,
        )

    def row_arrival(t, origin, q):
        return remote(
            picks.at[t, origin, q],
            rows.at[t, origin, 0, q],
            row_send.at[t, origin, q],
            row_recv.at[t, origin, q],
            z * plane + q,
            tp,
        )

    def swap_copy(t, origin):
        return remote(
            rows.at[t, origin, 0],
            rows.at[t, origin, 1],
            swap_send.at[t, origin],
            swap_recv.at[t, origin],
            sp,
            other,
        )

    def part_copy(origin):
        return remote(
            part_sent.at[origin],
            part_got.at[origin],
            part_sems.at[0, origin],
            part_sems.at[1, origin],
            sp,
            other,
        )

    def ret_copy(origin, q):
        return remote(
            ret_sent.at[origin, q],
            ret_got.at[origin, p],
            ret_send.at[origin, q],
            ret_recv.at[origin, p],
            z * plane + q,
            tp,
        )

    def ret_arrival(origin, q):
        return remote(
            ret_sent.at[origin, q],
            ret_got.at[origin, q],
            ret_send.at[origin, q],
            ret_recv.at[origin, q],
            z * plane + q,
            tp,
        )

    def band(j):
        return pl.ds(j * step, step)

    def line_copy(home, j):
        to_z = jnp.where(home > z, z + 1, z - 1)
        slot = jnp.where((home < z) & (to_z == home), extent, home)
        return remote(
            line_sent.at[home, :, band(j)],
            line_got.at[slot, :, band(j)],
            line_send.at[home, j],
            line_recv.at[slot, j],
            to_z * plane + p,
            tp,
        )

    def line_arrival(slot, j):
        return remote(
            line_sent.at[0, :, band(j)],
            line_got.at[slot, :, band(j)],
            line_send.at[0, j],
            line_recv.at[slot, j],
            z * plane + p,
            other,
        )

    def has_inflow(home):
        return ((home > z) & (z > 0)) | ((home < z) & (z < extent - 1))

    def hits(origin):
        slot = lax.broadcasted_iota(jnp.int32, (slots, token_count), 0) + z * slots
        slot = slot.astype(jnp.float32)
        return [slot == metas[origin, pl.ds(k, 1), :] for k in range(TOPK_ROWS)]

    def chooser(origin):
        first, second = hits(origin)
        return jnp.where(first | second, 1.0, 0.0).astype(jnp.bfloat16)

    def scale_of(origin):
        first, second = hits(origin)
        weighted = jnp.where(first, metas[origin, pl.ds(TOPK_ROWS, 1), :], 0.0) + jnp.where(
            second, metas[origin, pl.ds(TOPK_ROWS + 1, 1), :], 0.0
        )
        return jnp.sum(weighted, axis=1, keepdims=True)

    def arrive(t, k):
        origin = looked_up(orders, z, k)

        @pl.when(k > 0)
        def _():
            tok_copy(t, origin, True).wait_recv()
            if t == 0:
                meta_copy(origin, origin).wait_recv()

        for up_way in (False, True):

            @pl.when(forwards(origin, up_way))
            def _():
                tok_copy(t, origin, up_way).start()

        select = chooser(origin)
        if t == 1:
            scale = scale_of(origin)
        for j in range(columns):
            picked = jnp.dot(
                select, tok[t, origin, :, band(j)], preferred_element_type=jnp.float32
            )
            if t == 1:
                picked = scale * picked
            picks[t, origin, :, :, band(j)] = picked.astype(jnp.bfloat16).reshape(
                plane, capacity, step
            )

        @pl.loop(1, plane)
        def _(i):
            row_copy(t, origin, plane_peer(i)).start()

        rows[t, origin, 0, p] = picks[t, origin, p]

    def swap(t, k):
        origin = looked_up(orders, z, k)

        @pl.loop(1, plane)
        def _(i):
            row_arrival(t, origin, plane_peer(i)).wait_recv()

        swap_copy(t, origin).start()

    def expert_rows(t, origin):
        return rows[t, origin].reshape(2 * slots, width)

    half = gate.shape[1]
    tile = min(256, half)

    def first_products(k):
        origin = looked_up(orders, z, k)

        @pl.when(k == 0)
        def _():
            loads[2].wait()
            loads[3].wait()

        swap_copy(0, origin).wait_recv()

        @pl.loop(0, half // tile)
        def _(n):
            cut = pl.ds(pl.multiple_of(n * tile, tile), tile)
            block = expert_rows(0, origin)
            pre_gate[:, cut] = jnp.dot(block, gate[:, cut], preferred_element_type=jnp.float32)
            pre_up[:, cut] = jnp.dot(block, up[:, cut], preferred_element_type=jnp.float32)

    def products(k):
        origin = looked_up(orders, z, k)

        @pl.when(k == 0)
        def _():
            loads[4].wait()

        swap_copy(1, origin).wait_recv()

        @pl.loop(0, half // tile)
        def _(n):
            cut = pl.ds(pl.multiple_of(n * tile, tile), tile)
            hidden_grad = lax.dot_general(
                expert_rows(1, origin),
                down[cut, :],
                (((1,), (1,)), ((), ())),
                preferred_element_type=jnp.float32,
            )
            g, u = pre_gate[:, cut], pre_up[:, cut]
            logistic = jax.nn.sigmoid(g)
            gate_act = g * logistic
            hidden[origin, :, cut] = (gate_act * u).astype(jnp.bfloat16)
            gate_pre[origin, :, cut] = (
                hidden_grad * u * (logistic * (1.0 + g * (1.0 - logistic)))
            ).astype(jnp.bfloat16)
            up_pre[origin, :, cut] = (hidden_grad * gate_act).astype(jnp.bfloat16)

        wide = min(256, width)

        @pl.loop(0, width // wide)
        def _(n):
            cut = pl.ds(pl.multiple_of(n * wide, wide), wide)
            part = lax.dot_general(
                gate_pre[origin],
                gate[cut, :],
                (((1,), (1,)), ((), ())),
                preferred_element_type=jnp.float32,
            ) + lax.dot_general(
                up_pre[origin],
                up[cut, :],
                (((1,), (1,)), ((), ())),
                preferred_element_type=jnp.float32,
            )
            part = part.astype(jnp.bfloat16).reshape(2, plane, capacity, wide)
            part_own[:, :, cut] = part[0]
            part_sent[origin, :, :, cut] = part[1]

        part_copy(origin).start()
        for out in results(origin):
            out.start()

    def results(origin):
        pairs = [
            (rows.at[0, origin], inputs_out.at[origin]),
            (rows.at[1, origin], routed_out.at[origin]),
            (hidden.at[origin], hidden_out.at[origin]),
            (gate_pre.at[origin], gate_pre_out.at[origin]),
            (up_pre.at[origin], up_pre_out.at[origin]),
        ]
        return [
            pltpu.make_async_copy(src, dst, out_sems.at[i, origin])
            for i, (src, dst) in enumerate(pairs)
        ]

    def send_back(k):
        origin = looked_up(orders, z, k)
        part_copy(origin).wait_recv()
        for j in range(columns):
            both = part_own[:, :, band(j)].astype(jnp.float32) + part_got[
                origin, :, :, band(j)
            ].astype(jnp.float32)
            ret_sent[origin, :, :, band(j)] = both.astype(jnp.bfloat16)

        @pl.loop(1, plane)
        def _(i):
            ret_copy(origin, plane_peer(i)).start()

        ret_got[origin, p] = ret_sent[origin, p]

    def combine(k):
        origin = looked_up(orders, z, k)

        @pl.loop(1, plane)
        def _(i):
            ret_arrival(origin, plane_peer(i)).wait_recv()

        select = chooser(origin)
        for j in range(columns):
            back = ret_got[origin, :, :, band(j)].reshape(slots, step)
            added = lax.dot_general(
                select, back, (((0,), (0,)), ((), ())), preferred_element_type=jnp.float32
            )

            @pl.when(origin == z)
            def _():
                total[:, band(j)] = added

            @pl.when(origin != z)
            def _():
                line_sent[origin, :, band(j)] = added.astype(jnp.bfloat16)

            @pl.when((origin != z) & jnp.logical_not(has_inflow(origin)))
            def _():
                line_copy(origin, j).start()

    for load in loads[:2]:
        load.wait()
    for i in range(1, extent):
        meta_copy(line_peer(i), z).start()

    arrive(0, 0)

    @pl.loop(0, extent)
    def _(k):
        arrive(1, k)
        swap(0, k)
        first_products(k)

        @pl.when(k > 0)
        def _():
            combine(k - 1)

        swap(1, k)

        @pl.when(k < extent - 1)
        def _():
            arrive(0, k + 1)

        products(k)
        send_back(k)

    combine(extent - 1)

    @pl.loop(0, extent - 1)
    def _(k):
        home = looked_up(relays, z, k)

        @pl.when(has_inflow(home))
        def _():
            for j in range(columns):
                line_arrival(home, j).wait_recv()
                line_sent[home, :, band(j)] = (
                    line_sent[home, :, band(j)].astype(jnp.float32)
                    + line_got[home, :, band(j)].astype(jnp.float32)
                ).astype(jnp.bfloat16)
                line_copy(home, j).start()

    for j in range(columns):
        for slot, there in ((z, z > 0), (extent, z < extent - 1)):

            @pl.when(there)
            def _():
                line_arrival(slot, j).wait_recv()
                total[:, band(j)] = total[:, band(j)] + line_got[slot, :, band(j)].astype(
                    jnp.float32
                )

        tokens[tp, :, band(j)] = (
            tok[1, z, :, band(j)].astype(jnp.float32) + total[:, band(j)]
        ).astype(jnp.bfloat16)
    token_swap = remote(
        tokens.at[tp], tokens.at[tp], token_sems.at[0], token_sems.at[1], sp, other
    )
    token_swap.start()

    for i in range(1, extent):
        meta_copy(line_peer(i), z).wait_send()

    @pl.loop(0, extent)
    def _(origin):
        for t in range(2):
            for up_way in (False, True):

                @pl.when(forwards(origin, up_way))
                def _():
                    tok_copy(t, origin, up_way).wait_send()

            @pl.loop(1, plane)
            def _(i):
                row_copy(t, origin, plane_peer(i)).wait_send()

            swap_copy(t, origin).wait_send()
        part_copy(origin).wait_send()

        @pl.loop(1, plane)
        def _(i):
            ret_copy(origin, plane_peer(i)).wait_send()

        @pl.when(origin != z)
        def _():
            for j in range(columns):
                line_copy(origin, j).wait_send()

        for out in results(origin):
            out.wait()

    token_swap.wait()
    last = pltpu.make_async_copy(tokens, tokens_out, load_sem.at[0])
    last.start()
    last.wait()


TOPK_ROWS = 2


def routed_backward(mid_rows, cotangent, meta, gate_mat, up_mat, down_mat, capacity):
    sp_count = lax.axis_size("sp")
    extent = line_extent(sp_count)
    plane = sp_count // extent
    token_count, width = mid_rows.shape
    half = gate_mat.shape[1]
    slots = plane * capacity
    kind = jnp.bfloat16
    any_space = pl.BlockSpec(memory_space=pl.ANY)
    dma = pltpu.SemaphoreType.DMA
    columns = width // min(512, width)
    rows_shape = (extent, 2, plane, capacity, width)
    small_shape = (extent, 2 * slots, half)
    out = pl.pallas_call(
        functools.partial(routed_kernel, extent, plane, capacity),
        out_shape=[
            jax.ShapeDtypeStruct((2, token_count, width), kind),
            jax.ShapeDtypeStruct(rows_shape, kind),
            jax.ShapeDtypeStruct(rows_shape, kind),
            jax.ShapeDtypeStruct(small_shape, kind),
            jax.ShapeDtypeStruct(small_shape, kind),
            jax.ShapeDtypeStruct(small_shape, kind),
        ],
        in_specs=[any_space, any_space, pl.BlockSpec(memory_space=pltpu.VMEM)] + [any_space] * 3,
        out_specs=[any_space] * 6,
        scratch_shapes=[
            pltpu.VMEM((2, extent, token_count, width), kind),
            pltpu.VMEM((extent,) + meta.shape, jnp.float32),
            pltpu.VMEM((2, extent, plane, capacity, width), kind),
            pltpu.VMEM((2,) + rows_shape, kind),
            pltpu.VMEM(gate_mat.shape, kind),
            pltpu.VMEM(up_mat.shape, kind),
            pltpu.VMEM(down_mat.shape, kind),
            pltpu.VMEM((2 * slots, half), jnp.float32),
            pltpu.VMEM((2 * slots, half), jnp.float32),
            pltpu.VMEM(small_shape, kind),
            pltpu.VMEM(small_shape, kind),
            pltpu.VMEM(small_shape, kind),
            pltpu.VMEM((plane, capacity, width), kind),
            pltpu.VMEM((extent, plane, capacity, width), kind),
            pltpu.VMEM((extent, plane, capacity, width), kind),
            pltpu.VMEM((extent, plane, capacity, width), kind),
            pltpu.VMEM((extent, plane, capacity, width), kind),
            pltpu.VMEM((extent, token_count, width), kind),
            pltpu.VMEM((extent + 1, token_count, width), kind),
            pltpu.VMEM((token_count, width), jnp.float32),
            pltpu.VMEM((2, token_count, width), kind),
            dma((5,)),
            dma((2, extent)),
            dma((2, extent, 2)),
            dma((2, extent)),
            dma((2, extent, plane)),
            dma((2, extent, plane)),
            dma((2, extent)),
            dma((2, extent)),
            dma((2, extent)),
            dma((extent, plane)),
            dma((extent, plane)),
            dma((extent, columns)),
            dma((extent + 1, columns)),
            dma((5, extent)),
            dma((2,)),
        ],
        compiler_params=pltpu.CompilerParams(
            collective_id=0, has_side_effects=True, vmem_limit_bytes=62 * 1024 * 1024
        ),
    )(mid_rows, cotangent, meta, gate_mat, up_mat, down_mat)
    tokens, inputs, routed, hidden, gate_pre, up_pre = out
    every = 2 * slots * extent
    return (
        tokens.reshape(2 * token_count, width),
        inputs.reshape(every, width),
        routed.reshape(every, width),
        hidden.reshape(every, half),
        gate_pre.reshape(every, half),
        up_pre.reshape(every, half),
    )


def per_device(
    mid_rows,
    cotangent,
    routes,
    route_weight,
    filtered,
    conv_taps,
    norm_gain,
    out_weight,
    gate_weight,
    up_weight,
    down_weight,
):
    sp_count = lax.axis_size("sp")
    token_count, model_width = mid_rows.shape
    per_token = routes.shape[1]
    local_experts = gate_weight.shape[0]
    experts = local_experts * sp_count
    capacity = 2 * token_count * per_token // sp_count
    values = filtered.astype(jnp.float32)
    channel_sum, squares = lax.psum(
        (jnp.sum(values, axis=1), jnp.sum(values * values, axis=1)), "tp"
    )
    target = slot_targets(routes, experts, capacity).astype(jnp.float32)
    meta = jnp.concatenate([target.T, route_weight.T], axis=0)
    meta = jnp.pad(meta, ((0, 8 - meta.shape[0]), (0, 0)))
    grad_tokens, inputs, routed, hidden, gate_pre, up_pre = routed_backward(
        mid_rows, cotangent, meta, gate_weight[0], up_weight[0], down_weight[0], capacity
    )
    gate_grad = transposed_product(inputs, gate_pre)[None]
    up_grad = transposed_product(inputs, up_pre)[None]
    down_grad = transposed_product(hidden, routed)[None]
    average = channel_sum / model_width
    variance = squares / model_width - average * average
    inv_scale = lax.rsqrt(variance + NORM_EPS)[:, None]
    normed = (values - average[:, None]) * inv_scale
    scaled = normed * norm_gain
    activated = jax.nn.silu(scaled).astype(jnp.bfloat16)
    proj_grad, grad_tokens = reduced_products(grad_tokens, activated, "sp")
    act_grad = lax.dot_general(
        grad_tokens, out_weight, (((1,), (1,)), ((), ())), preferred_element_type=jnp.float32
    )
    scaled_grad = act_grad * silu_grad(scaled) * norm_gain
    grad_total, corr_total = lax.psum(
        (jnp.sum(scaled_grad, axis=1), jnp.sum(scaled_grad * normed, axis=1)), "tp"
    )
    grad_mean = (grad_total / model_width)[:, None]
    grad_corr = (corr_total / model_width)[:, None]
    conv_grad = (inv_scale * (scaled_grad - grad_mean - normed * grad_corr)).astype(jnp.bfloat16)
    halo_width = conv_taps.shape[0] // 2
    padded = extended(conv_grad, (("sp", 0),), halo_width)
    seq_rows = conv_grad.shape[0]
    accumulated = jnp.zeros(conv_grad.shape, jnp.float32)
    for offset in range(conv_taps.shape[0]):
        lead = 2 * halo_width - offset
        accumulated = accumulated + conv_taps[offset] * padded[lead : lead + seq_rows]
    input_grad = accumulated.astype(jnp.bfloat16)
    return (gate_grad, up_grad, down_grad, proj_grad, input_grad)


def solution(mesh):
    in_specs = (
        P(("sp", "tp"), None),
        P(("sp", "tp"), None),
        P(("sp", "tp"), None),
        P(("sp", "tp"), None),
        P("sp", "tp"),
        P(None, "tp"),
        P("tp"),
        P("tp", None),
        P("sp", None, "tp"),
        P("sp", None, "tp"),
        P("sp", "tp", None),
    )
    out_specs = (
        P("sp", None, "tp"),
        P("sp", None, "tp"),
        P("sp", "tp", None),
        P("sp", "tp"),
        P("sp", "tp"),
    )
    return jax.shard_map(
        per_device, mesh=mesh, in_specs=in_specs, out_specs=out_specs, check_vma=False
    )
```

time: 251 us -> 229 us (0.912)
  Pallas kernels: 0 us -> 136 us
  waiting for transfers between devices: 111 us -> 12 us
  matrix products: 56.3 us -> 23.3 us
  starting transfers between devices: 54.5 us -> 21.5 us
  local copies, waits for them, and re-layouts: 7.4 us -> 14.3 us
    pallas_call x0 -> x1, Pallas kernels: none -> 136 us  [routed_backward(): pl.pallas_call(functools.partial(routed_kernel, extent, plane, capacity),...]
    ppermute x8 -> x0, waiting for transfers between devices: 58.1 us -> none  [the longest x4 52 us: with_far(): lax.ppermute(block, 'sp', [(i, (i + half) % sp_count) for i in range(sp_c...]
    all_to_all x3 -> x0, waiting for transfers between devices: 33.4 us -> none  [the longest x1 20.8 us: per_device(): lax.all_to_all(back_rows, 'sp', split_axis=0, concat_axis=0, tiled=True)]
    dot_general x13 -> x0, matrix products: 32.1 us -> none  [the longest x10 25.9 us: row_product(): lax.dot_general(rows, matrix, (((1,), (dim,)), ((), ())), preferred_eleme...]
    all_to_all x3 -> x0, starting transfers between devices: 20.4 us -> none  [the longest x2 15.9 us: within_half(): lax.all_to_all(block.reshape(half, 2, local_experts, capacity, model_widt...]
    ppermute x8 -> x0, starting transfers between devices: 7.61 us -> none  [the longest x4 7.34 us: with_far(): lax.ppermute(block, 'sp', [(i, (i + half) % sp_count) for i in range(sp_c...]
    ppermute x12, waiting for transfers between devices: 19 us -> 12 us  [reduced_products(): lax.ppermute(block, axis, [(i, i ^ 1 << order[step]) for i in range(count)])]
    ppermute x12, starting transfers between devices: 20.6 us -> 15.1 us  [reduced_products(): lax.ppermute(block, axis, [(i, i ^ 1 << order[step]) for i in range(count)])]
  transfers between devices with their start and end apart: 25 -> 14, of which waited for: 13 -> 7; matrix products, arithmetic and copies ran while one was open for 22% -> 14% of each run, Pallas kernels for 0% -> 0%
where the time goes in v1:
time: 229 us; the launch traced here: 228 us
  Pallas kernels  136 us (59%)
  matrix products  23.3 us (10%)
  starting transfers between devices  21.5 us (9%)
  other arithmetic  14.7 us (6%)
  local copies, waits for them, and re-layouts  14.3 us (6%)
  waiting for transfers between devices  12 us (5%)
  blocking collectives  5.11 us (2%)
    pallas_call x1, Pallas kernels, routed_backward(): pl.pallas_call(functools.partial(routed_kernel, extent, plane, capacity),...  136 us
    dot_general x4, matrix products, transposed_product(): lax.dot_general(left, right, (((0,), (0,)), ((), ())), preferred_element_...  18.8 us
    ppermute x12, starting transfers between devices, reduced_products(): lax.ppermute(block, axis, [(i, i ^ 1 << order[step]) for i in range(count)])  15.1 us
    ppermute x12, waiting for transfers between devices, reduced_products(): lax.ppermute(block, axis, [(i, i ^ 1 << order[step]) for i in range(count)])  12 us
    convert_element_type x1, other arithmetic, per_device(): input_grad = accumulated.astype(jnp.bfloat16)  7.3 us
    ppermute x1, starting transfers between devices, extended(): lax.ppermute(lax.slice_in_dim(block, block.shape[dim] - width, None, axis...  5.16 us
  transfers between devices with their start and end apart: 14, of which 7 were waited for; matrix products, arithmetic and copies ran while one was open for 14% of the time, Pallas kernels for 0%

profile of v1, /device:TPU:0, one launch (start us, length us, event | category | flops | bytes accessed | tf_op | source)
XLA Modules:
  0.0 227.9 jit_solution(1981143042612907685)
XLA Ops:
  0.7 1.3 convert_reduce_fusion
  4.1 2.6 %all-reduce.2 = (f32[256]{0:T(256)S(1)}, f32[256]{0:T(256)S(1)}) all-reduce(f32[256]{0:T(256)S(1)} %get-tuple-element.52, f32[256]{0:T(256)S(1)} %get-tuple-element.51), channel_id=1, replica_groups=mesh['sp'=16,'tp'=2] {'tp'}, use_global_device_ids=true, to_apply=%region_4.5 | all-reduce | flops 512 | bytes 4096 | tf_op jit(solution)/shard_map/psum | solution.py:744
  6.7 1.3 select_maximum_fusion.meta
  7.9 135.9 %shard_map.146 = (bf16[2,128,2048]{2,1,0:T(8,128)(2,1)}, bf16[4,2,4,32,2048]{4,3,2,1,0:T(8,128)(2,1)}, bf16[4,2,4,32,2048]{4,3,2,1,0:T(8,128)(2,1)}, bf16[4,256,...) custom-call(bf16[128,2048]{1,0:T(8,128)(2,1)} %mid_hbm.1, ...), custom_call_target="tpu_custom_call" | custom-call | tf_op jit(solution)/shard_map/pallas_call | solution.py:658
  143.9 2.8 %convolution_convert_fusion = bf16[2048,1024]{1,0:T(8,128)(2,1)S(1)} fusion(bf16[256,2048]{1,0:T(8,128)(2,1)} %bitcast.165, bf16[256,1024]{1,0:T(8,128)(2,1)S(1)} %copy-done.8, f32[1024]{0:T(1024)S(1)} %copy-done.13, f32[256]{0:T(256)S(1)} %get-tuple-element.99, f32[256]{0:T(256)S(1)} %get-tuple-element.98), kind=kOutput, calls=%fused_computation | convolution fusion | flops 1078198272 | bytes 5773312 | tf_op jit(solution)/shard_map/dot_general | solution.py:102
  147.3 1.1 slice.296
  148.4 1.1 constant_dynamic-slice_fusion.1
  150.5 1.1 constant_dynamic-slice_fusion.5
  153.5 4.3 %fusion.64 = (f32[256]{0:T(256)S(1)}, f32[256]{0:T(256)S(1)}, f32[256,1024]{1,0:T(8,128)S(1)}) fusion(f32[256]{0:T(256)S(1)} %get-tuple-element.99, f32[256]{0:T(256)S(1)} %get-tuple-element.98, bf16[256,1024]{1,0:T(8,128)(2,1)S(1)} %copy-done.9, f32[1024]{0:T(1024)S(1)} %copy-done.13, bf16[256,2048]{1,0:T(8,128)(2,1)} %bitcast.166, ...), kind=kOutput, calls=%fused_computation.163 | convolution fusion | flops 1077935616 | bytes 6823936 | tf_op jit(solution)/shard_map/dot_general | solution.py:763
  157.8 2.5 %all-reduce.1 = (f32[256]{0:T(256)S(1)}, f32[256]{0:T(256)S(1)}) all-reduce(f32[256]{0:T(256)S(1)} %get-tuple-element.50, f32[256]{0:T(256)S(1)} %get-tuple-element.49), channel_id=1, replica_groups=mesh['sp'=16,'tp'=2] {'tp'}, use_global_device_ids=true, to_apply=%region_8.9 | all-reduce | flops 512 | bytes 4096 | tf_op jit(solution)/shard_map/psum | solution.py:767
  162.1 1.3 collective-permute-start.12
  163.4 5.2 %collective-permute-start.13 = (bf16[15,1024]{1,0:T(8,128)(2,1)}, bf16[15,1024]{1,0:T(8,128)(2,1)}, u32[]{:S(2)}, u32[]{:S(2)}) collective-permute-start(bf16[15,1024]{1,0:T(8,128)(2,1)} %get-tuple-element.66), channel_id=1, source_target_pairs={{0,2},{2,4},{4,6},{6,8},{8,10},{10,12},{12,14},{14,16},{16,18},{18... | collective-permute-start | bytes 92168 | tf_op jit(solution)/shard_map/ppermute | solution.py:19
  169.6 1.7 collective-permute-start.1
  171.3 7.0 %convolution_bitcast_fusion.1 = f32[1,2048,512]{2,1,0:T(8,128)} fusion(bf16[1024,2048]{1,0:T(8,128)(2,1)} %bitcast.161, bf16[1024,512]{1,0:T(8,128)(2,1)} %bitcast.164), kind=kOutput, calls=%fused_computation.2 | convolution fusion | flops 2147483648 | bytes 9437184 | tf_op jit(solution)/shard_map/dot_general | solution.py:102
  178.4 4.5 %convolution_bitcast_fusion.2 = f32[1,2048,512]{2,1,0:T(8,128)} fusion(bf16[1024,2048]{1,0:T(8,128)(2,1)S(1)} %bitcast.162, bf16[1024,512]{1,0:T(8,128)(2,1)S(1)} %bitcast.163), kind=kOutput, calls=%fused_computation.3 | convolution fusion | flops 2147483648 | bytes 9437184 | tf_op jit(solution)/shard_map/dot_general | solution.py:102
  182.8 1.8 collective-permute-done.2
  184.6 3.7 %collective-permute-done = bf16[2,2,2,128,384]{4,3,0,1,2:T(8,128)(2,1)S(1)} collective-permute-done((bf16[2,2,2,128,384]{4,3,0,1,2:T(8,128)(2,1)}, bf16[2,2,2,128,384]{4,3,0,1,2:T(8,128)(2,1)S(1)}, u32[]{:S(2)}, u32[]{:S(2)}) %collective-permute-start) | collective-permute-done | bytes 786464 | tf_op jit(solution)/shard_map/ppermute | solution.py:87
  192.5 1.1 collective-permute-start.3
  193.6 4.4 %convolution_bitcast_fusion = f32[1,512,2048]{2,1,0:T(8,128)} fusion(bf16[1024,512]{1,0:T(8,128)(2,1)S(1)} %bitcast.122, bf16[1024,2048]{1,0:T(8,128)(2,1)S(1)} %bitcast.119), kind=kOutput, calls=%fused_computation.1 | convolution fusion | flops 2147483648 | bytes 9437184 | tf_op jit(solution)/shard_map/dot_general | solution.py:102
  198.1 1.4 fusion.67
  199.4 1.6 collective-permute-done.4
  201.0 1.2 collective-permute-done.3
  202.2 1.2 bitcast_add_fusion.2
  203.4 1.4 collective-permute-start.8
  205.0 1.3 collective-permute-start.7
  206.3 1.1 bitcast_add_fusion.1
  207.4 1.8 collective-permute-start.6
  209.2 1.1 fusion.68
  210.7 3.1 %collective-permute-done.6 = bf16[2,128,384]{2,1,0:T(8,128)(2,1)S(1)} collective-permute-done((bf16[2,128,384]{2,1,0:T(8,128)(2,1)S(1)}, bf16[2,128,384]{2,1,0:T(8,128)(2,1)S(1)}, u32[]{:S(2)}, u32[]{:S(2)}) %collective-permute-start.6) | collective-permute-done | bytes 196640 | tf_op jit(solution)/shard_map/ppermute | solution.py:87
  213.9 2.5 %collective-permute-start.11 = (bf16[128,256]{1,0:T(8,128)(2,1)S(1)}, bf16[128,256]{1,0:T(8,128)(2,1)S(1)}, u32[]{:S(2)}, u32[]{:S(2)}) collective-permute-start(bf16[128,256]{1,0:T(8,128)(2,1)S(1)} %fusion.61), channel_id=1, source_target_pairs={{0,16},{2,18},{4,20},{6,22},{8,24},{10,26},{12,28},{14,30},{16,0},... | collective-permute-start | bytes 196616 | tf_op jit(solution)/shard_map/ppermute | solution.py:87
  217.1 2.5 %collective-permute-start.9 = (bf16[128,384]{1,0:T(8,128)(2,1)S(1)}, bf16[128,384]{1,0:T(8,128)(2,1)S(1)}, u32[]{:S(2)}, u32[]{:S(2)}) collective-permute-start(bf16[128,384]{1,0:T(8,128)(2,1)S(1)} %fusion.59), channel_id=1, source_target_pairs={{0,16},{2,18},{4,20},{6,22},{8,24},{10,26},{12,28},{14,30},{16,0},... | collective-permute-start | bytes 294920 | tf_op jit(solution)/shard_map/ppermute | solution.py:87
  219.6 7.3 %add_convert_fusion = bf16[256,1024]{1,0:T(8,128)(2,1)} fusion(bf16[256,1024]{1,0:T(8,128)(2,1)S(1)} %copy-done.6, bf16[15,1024]{1,0:T(8,128)(2,1)} %collective-permute-done.13, bf16[15,1024]{1,0:T(8,128)(2,1)} %collective-permute-done.12, f32[1024]{0:T(1024)S(1)} %bitcast.158, f32[1024]{0:T(1024)S(1)} %bitcast.159, f32[1024]{0:T(1024)S(1)} %bitcast.130, ...), kind=kLoop, calls=%fused_computation.60 | loop fusion | flops 47972352 | bytes 1236992 | tf_op jit(solution)/shard_map/convert_element_type | solution.py:780
  (77 shorter events, 14.7 us)
Async XLA Ops:
  0.6 143.3 %copy-start.8 = (bf16[256,1024]{1,0:T(8,128)(2,1)S(1)}, bf16[256,1024]{1,0:T(8,128)(2,1)}, u32[]{:S(2)}) copy-start(bf16[256,1024]{1,0:T(8,128)(2,1)} %param.15) | copy-start | bytes 1572868
  0.6 143.3 %copy-start.13 = (f32[1024]{0:T(1024)S(1)}, f32[1024]{0:T(1024)}, u32[]{:S(2)}) copy-start(f32[1024]{0:T(1024)} %param.17) | copy-start | bytes 12292
  149.5 3.0 %copy-start.1 = (bf16[2,2,2,2,128,256]{5,4,3,2,1,0:T(8,128)(2,1)S(1)}, bf16[2,2,2,2,128,256]{5,4,3,2,1,0:T(8,128)(2,1)}, u32[]{:S(2)}) copy-start(bf16[2,2,2,2,128,256]{5,4,3,2,1,0:T(8,128)(2,1)} %slice.296) | copy-start | bytes 3145732
  150.5 3.0 %copy-start.9 = (bf16[256,1024]{1,0:T(8,128)(2,1)S(1)}, bf16[256,1024]{1,0:T(8,128)(2,1)}, u32[]{:S(2)}) copy-start(bf16[256,1024]{1,0:T(8,128)(2,1)} %param.15) | copy-start | bytes 1572868
  153.5 16.1 %copy-start.10 = (bf16[2,2,1,2,128,384]{5,4,0,3,1,2:T(8,128)(2,1)S(1)}, bf16[2,2,1,2,128,384]{5,4,0,3,1,2:T(8,128)(2,1)}, u32[]{:S(2)}) copy-start(bf16[2,2,1,2,128,384]{5,4,0,3,1,2:T(8,128)(2,1)} %copy.45) | copy-start | bytes 2359300
  160.7 0.8 copy-start.5
  162.1 57.5 %collective-permute-start.12 = (bf16[15,1024]{1,0:T(8,128)(2,1)}, bf16[15,1024]{1,0:T(8,128)(2,1)}, u32[]{:S(2)}, u32[]{:S(2)}) collective-permute-start(bf16[15,1024]{1,0:T(8,128)(2,1)} %get-tuple-element.65), channel_id=1, source_target_pairs={{2,0},{4,2},{6,4},{8,6},{10,8},{12,10},{14,12},{16,14},{18,16},{20... | collective-permute-start | bytes 92168 | tf_op jit(solution)/shard_map/ppermute | solution.py:22
  163.4 56.2 %collective-permute-start.13 = (bf16[15,1024]{1,0:T(8,128)(2,1)}, bf16[15,1024]{1,0:T(8,128)(2,1)}, u32[]{:S(2)}, u32[]{:S(2)}) collective-permute-start(bf16[15,1024]{1,0:T(8,128)(2,1)} %get-tuple-element.66), channel_id=1, source_target_pairs={{0,2},{2,4},{4,6},{6,8},{8,10},{10,12},{12,14},{14,16},{16,18},{18... | collective-permute-start | bytes 92168 | tf_op jit(solution)/shard_map/ppermute | solution.py:19
  168.6 19.7 %collective-permute-start = (bf16[2,2,2,128,384]{4,3,0,1,2:T(8,128)(2,1)}, bf16[2,2,2,128,384]{4,3,0,1,2:T(8,128)(2,1)S(1)}, u32[]{:S(2)}, u32[]{:S(2)}) collective-permute-start(bf16[2,2,2,128,384]{4,3,0,1,2:T(8,128)(2,1)} %bitcast.127), channel_id=1, source_target_pairs={{0,2},{2,0},{4,6},{6,4},{8,10},{10,8},{12,14},{14,12},{16,18},{18,... | collective-permute-start | bytes 2359304 | tf_op jit(solution)/shard_map/ppermute | solution.py:87
  169.6 18.9 %collective-permute-start.1 = (bf16[2,2,2,128,384]{4,3,0,2,1:T(8,128)(2,1)S(1)}, bf16[2,2,2,128,384]{4,3,0,2,1:T(8,128)(2,1)S(1)}, u32[]{:S(2)}, u32[]{:S(2)}) collective-permute-start(bf16[2,2,2,128,384]{4,3,0,2,1:T(8,128)(2,1)S(1)} %bitcast.126), channel_id=1, source_target_pairs={{0,4},{2,6},{4,0},{6,2},{8,12},{10,14},{12,8},{14,10},{16,20},{18,... | collective-permute-start | bytes 2359304 | tf_op jit(solution)/shard_map/ppermute | solution.py:87
  171.3 13.3 %collective-permute-start.2 = (bf16[2,2,2,128,256]{4,3,0,1,2:T(8,128)(2,1)}, bf16[2,2,2,128,256]{4,3,0,1,2:T(8,128)(2,1)S(1)}, u32[]{:S(2)}, u32[]{:S(2)}) collective-permute-start(bf16[2,2,2,128,256]{4,3,0,1,2:T(8,128)(2,1)} %bitcast.128), channel_id=1, source_target_pairs={{0,8},{2,10},{4,12},{6,14},{8,0},{10,2},{12,4},{14,6},{16,24},{18,... | collective-permute-start | bytes 1572872 | tf_op jit(solution)/shard_map/ppermute | solution.py:87
  171.3 7.0 %copy-start.11 = (bf16[4,2,4,32,2048]{4,3,2,1,0:T(8,128)(2,1)S(1)}, bf16[4,2,4,32,2048]{4,3,2,1,0:T(8,128)(2,1)}, u32[]{:S(2)}) copy-start(bf16[4,2,4,32,2048]{4,3,2,1,0:T(8,128)(2,1)} %get-tuple-element.27) | copy-start | bytes 12582916
  171.3 7.0 %copy-start.12 = (bf16[4,256,512]{2,1,0:T(8,128)(2,1)S(1)}, bf16[4,256,512]{2,1,0:T(8,128)(2,1)}, u32[]{:S(2)}) copy-start(bf16[4,256,512]{2,1,0:T(8,128)(2,1)} %get-tuple-element.28) | copy-start | bytes 3145732
  178.4 12.1 %copy-start.3 = (bf16[2,2,1,2,128,384]{5,4,3,2,1,0:T(8,128)(2,1)S(1)}, bf16[2,2,1,2,128,384]{5,4,3,2,1,0:T(8,128)(2,1)}, u32[]{:S(2)}) copy-start(bf16[2,2,1,2,128,384]{5,4,3,2,1,0:T(8,128)(2,1)} %get-tuple-element.59) | copy-start | bytes 2359300
  182.8 8.7 %copy-start.4 = (bf16[2,2,2,1,128,384]{5,4,3,2,1,0:T(8,128)(2,1)S(1)}, bf16[2,2,2,1,128,384]{5,4,3,2,1,0:T(8,128)(2,1)}, u32[]{:S(2)}) copy-start(bf16[2,2,2,1,128,384]{5,4,3,2,1,0:T(8,128)(2,1)} %get-tuple-element.61) | copy-start | bytes 2359300
  188.7 1.8 copy-start.2
  188.7 4.9 %copy-start = (bf16[4,2,4,32,2048]{4,3,2,1,0:T(8,128)(2,1)S(1)}, bf16[4,2,4,32,2048]{4,3,2,1,0:T(8,128)(2,1)}, u32[]{:S(2)}) copy-start(bf16[4,2,4,32,2048]{4,3,2,1,0:T(8,128)(2,1)} %get-tuple-element.31) | copy-start | bytes 12582916
  188.7 4.9 %copy-start.7 = (bf16[4,256,512]{2,1,0:T(8,128)(2,1)S(1)}, bf16[4,256,512]{2,1,0:T(8,128)(2,1)}, u32[]{:S(2)}) copy-start(bf16[4,256,512]{2,1,0:T(8,128)(2,1)} %get-tuple-element.30) | copy-start | bytes 3145732
  189.5 10.0 %collective-permute-start.5 = (bf16[2,2,128,256]{3,2,0,1:T(8,128)(2,1)}, bf16[2,2,128,256]{3,2,0,1:T(8,128)(2,1)}, u32[]{:S(2)}, u32[]{:S(2)}) collective-permute-start(bf16[2,2,128,256]{3,2,0,1:T(8,128)(2,1)} %fusion.55), channel_id=1, source_target_pairs={{0,2},{2,0},{4,6},{6,4},{8,10},{10,8},{12,14},{14,12},{16,18},{18,... | collective-permute-start | bytes 786440 | tf_op jit(solution)/shard_map/ppermute | solution.py:87
  191.4 9.6 %collective-permute-start.4 = (bf16[2,2,128,384]{3,2,0,1:T(8,128)(2,1)}, bf16[2,2,128,384]{3,2,0,1:T(8,128)(2,1)S(1)}, u32[]{:S(2)}, u32[]{:S(2)}) collective-permute-start(bf16[2,2,128,384]{3,2,0,1:T(8,128)(2,1)} %fusion.54), channel_id=1, source_target_pairs={{0,8},{2,10},{4,12},{6,14},{8,0},{10,2},{12,4},{14,6},{16,24},{18,... | collective-permute-start | bytes 1179656 | tf_op jit(solution)/shard_map/ppermute | solution.py:87
  192.5 9.7 %collective-permute-start.3 = (bf16[2,2,128,384]{3,2,0,1:T(8,128)(2,1)}, bf16[2,2,128,384]{3,2,0,1:T(8,128)(2,1)}, u32[]{:S(2)}, u32[]{:S(2)}) collective-permute-start(bf16[2,2,128,384]{3,2,0,1:T(8,128)(2,1)} %fusion.53), channel_id=1, source_target_pairs={{0,4},{2,6},{4,0},{6,2},{8,12},{10,14},{12,8},{14,10},{16,20},{18,... | collective-permute-start | bytes 1179656 | tf_op jit(solution)/shard_map/ppermute | solution.py:87
  203.4 16.2 %copy-start.6 = (bf16[256,1024]{1,0:T(8,128)(2,1)S(1)}, bf16[256,1024]{1,0:T(8,128)(2,1)}, u32[]{:S(2)}) copy-start(bf16[256,1024]{1,0:T(8,128)(2,1)} %copy-done.5) | copy-start | bytes 1572868
  203.4 6.9 %collective-permute-start.8 = (bf16[2,128,256]{2,1,0:T(8,128)(2,1)S(1)}, bf16[2,128,256]{2,1,0:T(8,128)(2,1)S(1)}, u32[]{:S(2)}, u32[]{:S(2)}) collective-permute-start(bf16[2,128,256]{2,1,0:T(8,128)(2,1)S(1)} %fusion.58), channel_id=1, source_target_pairs={{0,4},{2,6},{4,0},{6,2},{8,12},{10,14},{12,8},{14,10},{16,20},{18,... | collective-permute-start | bytes 393224 | tf_op jit(solution)/shard_map/ppermute | solution.py:87
  205.0 5.7 %collective-permute-start.7 = (bf16[2,128,384]{2,1,0:T(8,128)(2,1)S(1)}, bf16[2,128,384]{2,1,0:T(8,128)(2,1)S(1)}, u32[]{:S(2)}, u32[]{:S(2)}) collective-permute-start(bf16[2,128,384]{2,1,0:T(8,128)(2,1)S(1)} %fusion.57), channel_id=1, source_target_pairs={{0,2},{2,0},{4,6},{6,4},{8,10},{10,8},{12,14},{14,12},{16,18},{18,... | collective-permute-start | bytes 589832 | tf_op jit(solution)/shard_map/ppermute | solution.py:87
  207.4 6.4 %collective-permute-start.6 = (bf16[2,128,384]{2,1,0:T(8,128)(2,1)S(1)}, bf16[2,128,384]{2,1,0:T(8,128)(2,1)S(1)}, u32[]{:S(2)}, u32[]{:S(2)}) collective-permute-start(bf16[2,128,384]{2,1,0:T(8,128)(2,1)S(1)} %fusion.56), channel_id=1, source_target_pairs={{0,8},{2,10},{4,12},{6,14},{8,0},{10,2},{12,4},{14,6},{16,24},{18,... | collective-permute-start | bytes 589832 | tf_op jit(solution)/shard_map/ppermute | solution.py:87
  213.9 13.0 %collective-permute-start.11 = (bf16[128,256]{1,0:T(8,128)(2,1)S(1)}, bf16[128,256]{1,0:T(8,128)(2,1)S(1)}, u32[]{:S(2)}, u32[]{:S(2)}) collective-permute-start(bf16[128,256]{1,0:T(8,128)(2,1)S(1)} %fusion.61), channel_id=1, source_target_pairs={{0,16},{2,18},{4,20},{6,22},{8,24},{10,26},{12,28},{14,30},{16,0},... | collective-permute-start | bytes 196616 | tf_op jit(solution)/shard_map/ppermute | solution.py:87
  216.5 10.5 %collective-permute-start.10 = (bf16[128,384]{1,0:T(8,128)(2,1)S(1)}, bf16[128,384]{1,0:T(8,128)(2,1)S(1)}, u32[]{:S(2)}, u32[]{:S(2)}) collective-permute-start(bf16[128,384]{1,0:T(8,128)(2,1)S(1)} %fusion.60), channel_id=1, source_target_pairs={{0,16},{2,18},{4,20},{6,22},{8,24},{10,26},{12,28},{14,30},{16,0},... | collective-permute-start | bytes 294920 | tf_op jit(solution)/shard_map/ppermute | solution.py:87
  217.1 9.8 %collective-permute-start.9 = (bf16[128,384]{1,0:T(8,128)(2,1)S(1)}, bf16[128,384]{1,0:T(8,128)(2,1)S(1)}, u32[]{:S(2)}, u32[]{:S(2)}) collective-permute-start(bf16[128,384]{1,0:T(8,128)(2,1)S(1)} %fusion.59), channel_id=1, source_target_pairs={{0,16},{2,18},{4,20},{6,22},{8,24},{10,26},{12,28},{14,30},{16,0},... | collective-permute-start | bytes 294920 | tf_op jit(solution)/shard_map/ppermute | solution.py:87

commit v2 on v1

--- a/solution.py
+++ b/solution.py
@@ -1,4 +1,5 @@
 import functools
+import math
 
 import jax
 import jax.numpy as jnp
@@ -9,24 +10,7 @@
 
 MESH = pl.DeviceIdType.MESH
 NORM_EPS = 1e-05
-
-
-def extended(block, sides, width):
-    for axis, dim in sides:
-        count = lax.axis_size(axis)
-        forward = [(i, i + 1) for i in range(count - 1)]
-        backward = [(target, source) for source, target in forward]
-        low = lax.ppermute(
-            lax.slice_in_dim(block, block.shape[dim] - width, None, axis=dim), axis, forward
-        )
-        high = lax.ppermute(lax.slice_in_dim(block, 0, width, axis=dim), axis, backward)
-        block = jnp.concatenate([low, block, high], axis=dim)
-    return block
-
-
-def silu_grad(pre_act):
-    logistic = jax.nn.sigmoid(pre_act)
-    return logistic * (1.0 + pre_act * (1.0 - logistic))
+SPARE = 4 << 20
 
 
 def slot_targets(routes, experts, capacity):
@@ -38,64 +22,6 @@
     earlier = jnp.dot(before, one_hot.astype(jnp.bfloat16), preferred_element_type=jnp.float32)
     positions = jnp.sum(jnp.where(one_hot, earlier, 0.0), axis=1).astype(jnp.int32)
     return (flattened * capacity + positions).reshape(token_count, per_token)
-
-
-def halving_orders(count):
-    bits = count.bit_length() - 1
-    turned = min(bits, 3)
-    return [
-        [(start + step) % turned for step in range(turned)] + list(range(turned, bits))
-        for start in range(turned)
-    ]
-
-
-def column_groups(columns, groups):
-    lanes = 128
-    tiles = columns // lanes
-    sizes = [tiles // groups + (1 if g < tiles % groups else 0) for g in range(groups)]
-    starts = [sum(sizes[:g]) * lanes for g in range(groups)]
-    return [(start, size * lanes) for start, size in zip(starts, sizes) if size]
-
-
-def picked(block, place, dim):
-    return lax.dynamic_index_in_dim(block, place, dim, keepdims=False)
-
-
-def reduced_products(rows, columns, axis):
-    count = lax.axis_size(axis)
-    tokens, width = rows.shape
-    bits = count.bit_length() - 1
-    own = lax.axis_index(axis)
-    product = transposed_product(rows, columns).astype(jnp.bfloat16)
-    cut = product.reshape((2,) * bits + (width // count, columns.shape[1]))
-    orders = halving_orders(count)
-    groups = column_groups(columns.shape[1], len(orders))
-    orders = orders[: len(groups)]
-    totals = [lax.slice_in_dim(cut, start, start + size, axis=bits + 1) for start, size in groups]
-    left = [list(range(bits - 1, -1, -1)) for _ in groups]
-    for step in range(bits):
-        outgoing, kept = [], []
-        for total, order, dims in zip(totals, orders, left):
-            mine = (own >> order[step]) & 1
-            dim = dims.index(order[step])
-            dims.pop(dim)
-            outgoing.append(picked(total, 1 - mine, dim).astype(jnp.bfloat16))
-            kept.append(picked(total, mine, dim).astype(jnp.float32))
-        if step == 0:
-            outgoing, rows = lax.optimization_barrier((outgoing, rows))
-        arrived = [
-            lax.ppermute(block, axis, [(i, i ^ (1 << order[step])) for i in range(count)])
-            for block, order in zip(outgoing, orders)
-        ]
-        arrived = lax.optimization_barrier(arrived)
-        totals = [own_part + got.astype(jnp.float32) for own_part, got in zip(kept, arrived)]
-    return jnp.concatenate(totals, axis=1), rows
-
-
-def row_product(rows, matrix, dim=0):
-    return lax.dot_general(
-        rows, matrix, (((1,), (dim,)), ((), ())), preferred_element_type=jnp.float32
-    )
 
 
 def transposed_product(left, right):
@@ -133,6 +59,23 @@
     ]
 
 
+def sum_orders(extent):
+    return [
+        sorted((i for i in range(extent) if i != own), key=lambda i: -abs(i - own)) + [own]
+        for own in range(extent)
+    ]
+
+
+def sum_relays(extent):
+    return [
+        sorted(
+            (i for i in range(extent) if i != own),
+            key=lambda i: (own if i > own else extent - 1 - own, -abs(i - own)),
+        )
+        for own in range(extent)
+    ]
+
+
 def looked_up(table, row, column):
     value = jnp.int32(0)
     for i, entries in enumerate(table):
@@ -151,7 +94,12 @@
     gate_hbm,
     up_hbm,
     down_hbm,
-    tokens_out,
+    filtered_hbm,
+    out_weight_hbm,
+    taps,
+    gain,
+    proj_out,
+    input_out,
     inputs_out,
     routed_out,
     hidden_out,
@@ -169,7 +117,6 @@
     hidden,
     gate_pre,
     up_pre,
-    part_own,
     part_sent,
     part_got,
     ret_sent,
@@ -193,16 +140,35 @@
     line_recv,
     out_sems,
     token_sems,
+    values,
+    out_weight,
+    stats,
+    normed,
+    inverse,
+    active,
+    blocks,
+    sums_sent,
+    sums_got,
+    sums_own,
+    padded,
+    spread,
+    stat_sems,
+    active_send,
+    active_recv,
+    block_send,
+    block_recv,
+    sums_send,
+    sums_recv,
+    halo_sems,
 ):
     sp, tp = lax.axis_index("sp"), lax.axis_index("tp")
     z, p = sp // plane, sp % plane
     slots = plane * capacity
     token_count, width = tok.shape[2], tok.shape[3]
     other = 1 - tp
-    step = min(512, width)
-    columns = width // step
+    step = width // extent
+    columns = extent
     orders, relays = chunk_orders(extent), relay_orders(extent)
-    load_from = [mid_hbm, cot_hbm]
 
     def remote(src, dst, send, recv, to_sp, to_tp):
         return pltpu.make_async_remote_copy(
@@ -220,6 +186,8 @@
         pltpu.make_async_copy(gate_hbm, gate, load_sem.at[2]),
         pltpu.make_async_copy(up_hbm, up, load_sem.at[3]),
         pltpu.make_async_copy(down_hbm, down, load_sem.at[4]),
+        pltpu.make_async_copy(filtered_hbm, values, load_sem.at[5]),
+        pltpu.make_async_copy(out_weight_hbm, out_weight, load_sem.at[6]),
     ]
     for load in loads:
         load.start()
@@ -242,9 +210,21 @@
     @pl.loop(1, plane)
     def _(i):
         greet(z * plane + plane_peer(i), tp)
+        greet(z * plane + plane_peer(i), other)
 
     greet(sp, other)
-    pl.semaphore_wait(barrier, extent - 1 + plane - 1 + 1)
+    last_sp = extent * plane - 1
+
+    @pl.when(sp > 0)
+    def _():
+        greet(sp - 1, tp)
+
+    @pl.when(sp < last_sp)
+    def _():
+        greet(sp + 1, tp)
+
+    ends = jnp.where(sp > 0, 1, 0) + jnp.where(sp < last_sp, 1, 0)
+    pl.semaphore_wait(barrier, extent - 1 + 2 * (plane - 1) + 1 + ends)
 
     def meta_copy(to_z, from_z):
         return remote(
@@ -481,7 +461,7 @@
                 preferred_element_type=jnp.float32,
             )
             part = part.astype(jnp.bfloat16).reshape(2, plane, capacity, wide)
-            part_own[:, :, cut] = part[0]
+            ret_sent[origin, :, :, cut] = part[0]
             part_sent[origin, :, :, cut] = part[1]
 
         part_copy(origin).start()
@@ -505,7 +485,7 @@
         origin = looked_up(orders, z, k)
         part_copy(origin).wait_recv()
         for j in range(columns):
-            both = part_own[:, :, band(j)].astype(jnp.float32) + part_got[
+            both = ret_sent[origin, :, :, band(j)].astype(jnp.float32) + part_got[
                 origin, :, :, band(j)
             ].astype(jnp.float32)
             ret_sent[origin, :, :, band(j)] = both.astype(jnp.bfloat16)
@@ -547,7 +527,64 @@
     for i in range(1, extent):
         meta_copy(line_peer(i), z).start()
 
+    local = values.shape[1]
+    strip = min(256, local)
+    strips = local // strip
+    row_count = values.shape[0]
+
+    def strip_at(n):
+        return pl.ds(pl.multiple_of(n * strip, strip), strip)
+
+    def stat_copy(i):
+        return remote(
+            stats.at[i, 0], stats.at[i, 1], stat_sems.at[0, i], stat_sems.at[1, i], sp, other
+        )
+
+    def paired(i, first, second):
+        lane = lax.broadcasted_iota(jnp.int32, (row_count, stats.shape[3]), 1)
+        stats[i, 0] = jnp.where(lane == 0, first, second)
+        stat_copy(i).start()
+
+    def both_sums(i):
+        stat_copy(i).wait_recv()
+        merged = (stats[i, 0] + stats[i, 1]) / width
+        return merged[:, 0:1], merged[:, 1:2]
+
+    def active_copy(q):
+        return remote(
+            active.at[p], active.at[p], active_send.at[q], active_recv.at[p], z * plane + q, tp
+        )
+
+    def active_arrival(q):
+        return remote(
+            active.at[q], active.at[q], active_send.at[q], active_recv.at[q], z * plane + q, tp
+        )
+
+    def prepare():
+        loads[5].wait()
+        sums = jnp.zeros((row_count, 1), jnp.float32)
+        squares = jnp.zeros((row_count, 1), jnp.float32)
+        for n in range(strips):
+            block = values[:, n * strip : (n + 1) * strip].astype(jnp.float32)
+            sums = sums + jnp.sum(block, axis=1, keepdims=True)
+            squares = squares + jnp.sum(block * block, axis=1, keepdims=True)
+        paired(0, sums, squares)
+        average, second = both_sums(0)
+        scale = lax.rsqrt(second - average * average + NORM_EPS)
+        inverse[...] = jnp.broadcast_to(scale, inverse.shape)
+        for n in range(strips):
+            cut = slice(n * strip, (n + 1) * strip)
+            flat = (values[:, cut].astype(jnp.float32) - average) * scale
+            normed[:, cut] = flat
+            scaled = flat * gain[:, cut]
+            active[p, :, cut] = (scaled * jax.nn.sigmoid(scaled)).astype(jnp.bfloat16)
+
+        @pl.loop(1, plane)
+        def _(i):
+            active_copy(plane_peer(i)).start()
+
     arrive(0, 0)
+    prepare()
 
     @pl.loop(0, extent)
     def _(k):
@@ -584,6 +621,53 @@
                 ).astype(jnp.bfloat16)
                 line_copy(home, j).start()
 
+    own_block = width // (extent * plane)
+    lanes = blocks.shape[4]
+
+    def block_at(j, q):
+        start = (j * plane + q) * own_block
+        return pl.ds(pl.multiple_of(start // lanes * lanes, lanes), lanes)
+
+    def token_copy(j):
+        return remote(
+            tokens.at[tp, :, band(j)],
+            tokens.at[tp, :, band(j)],
+            token_sems.at[0, j],
+            token_sems.at[1, j],
+            sp,
+            other,
+        )
+
+    def token_arrival(j):
+        return remote(
+            tokens.at[other, :, band(j)],
+            tokens.at[other, :, band(j)],
+            token_sems.at[0, j],
+            token_sems.at[1, j],
+            sp,
+            other,
+        )
+
+    def block_copy(j, q, to_tp):
+        return remote(
+            tokens.at[tp, :, block_at(j, q)],
+            blocks.at[j, p, tp],
+            block_send.at[j, q, to_tp],
+            block_recv.at[j, p, tp],
+            z * plane + q,
+            to_tp,
+        )
+
+    def block_arrival(j, q, from_tp):
+        return remote(
+            tokens.at[tp, :, block_at(j, q)],
+            blocks.at[j, q, from_tp],
+            block_send.at[j, q, from_tp],
+            block_recv.at[j, q, from_tp],
+            z * plane + q,
+            from_tp,
+        )
+
     for j in range(columns):
         for slot, there in ((z, z > 0), (extent, z < extent - 1)):
 
@@ -597,10 +681,220 @@
         tokens[tp, :, band(j)] = (
             tok[1, z, :, band(j)].astype(jnp.float32) + total[:, band(j)]
         ).astype(jnp.bfloat16)
-    token_swap = remote(
-        tokens.at[tp], tokens.at[tp], token_sems.at[0], token_sems.at[1], sp, other
-    )
-    token_swap.start()
+
+        @pl.loop(1, plane)
+        def _(i):
+            for to_tp in range(2):
+                block_copy(j, plane_peer(i), to_tp).start()
+
+        token_copy(j).start()
+
+    pieces = 2
+    piece = local // pieces
+
+    def piece_at(h):
+        return pl.ds(h * piece, piece)
+
+    def sums_copy(j, h):
+        to_z = jnp.where(j > z, z + 1, z - 1)
+        slot = jnp.where((j < z) & (to_z == j), extent, j)
+        return remote(
+            sums_sent.at[j, :, piece_at(h)],
+            sums_got.at[slot, :, piece_at(h)],
+            sums_send.at[j, h],
+            sums_recv.at[slot, h],
+            to_z * plane + p,
+            tp,
+        )
+
+    def sums_arrival(slot, h):
+        return remote(
+            sums_sent.at[0, :, piece_at(h)],
+            sums_got.at[slot, :, piece_at(h)],
+            sums_send.at[0, h],
+            sums_recv.at[slot, h],
+            sp,
+            other,
+        )
+
+    @pl.loop(1, plane)
+    def _(i):
+        active_arrival(plane_peer(i)).wait_recv()
+
+    @pl.loop(0, extent)
+    def _(k):
+        j = looked_up(sum_orders(extent), z, k)
+
+        @pl.loop(1, plane)
+        def _(i):
+            for from_tp in range(2):
+                block_arrival(j, plane_peer(i), from_tp).wait_recv()
+
+        token_arrival(j).wait_recv()
+        for half_at in range(2):
+            blocks[j, p, half_at] = tokens[half_at, :, block_at(j, p)]
+        for n in range(strips):
+            cut = slice(n * strip, (n + 1) * strip)
+            spread[:lanes, cut] = lax.dot_general(
+                blocks[j].reshape(plane * row_count, lanes),
+                active[:, :, cut].reshape(plane * row_count, strip),
+                (((0,), (0,)), ((), ())),
+                preferred_element_type=jnp.float32,
+            )
+        start = lax.rem((j * plane + p) * own_block, lanes)
+        mine = spread[pl.ds(pl.multiple_of(start, own_block), own_block), :]
+
+        @pl.when(j == z)
+        def _():
+            sums_own[...] = mine
+
+        @pl.when(j != z)
+        def _():
+            sums_sent[j] = mine.astype(jnp.bfloat16)
+
+        @pl.when((j != z) & jnp.logical_not(has_inflow(j)))
+        def _():
+            for h in range(pieces):
+                sums_copy(j, h).start()
+
+    def relay(k):
+        j = looked_up(sum_relays(extent), z, k)
+
+        @pl.when(has_inflow(j))
+        def _():
+            for h in range(pieces):
+                sums_arrival(j, h).wait_recv()
+                sums_sent[j, :, piece_at(h)] = (
+                    sums_sent[j, :, piece_at(h)].astype(jnp.float32)
+                    + sums_got[j, :, piece_at(h)].astype(jnp.float32)
+                ).astype(jnp.bfloat16)
+                sums_copy(j, h).start()
+
+    loads[6].wait()
+    grad_sum = jnp.zeros((row_count, 1), jnp.float32)
+    grad_corr = jnp.zeros((row_count, 1), jnp.float32)
+    for n in range(strips):
+        cut = slice(n * strip, (n + 1) * strip)
+        act_grad = lax.dot_general(
+            tokens[...].reshape(row_count, width),
+            out_weight[cut, :],
+            (((1,), (1,)), ((), ())),
+            preferred_element_type=jnp.float32,
+        )
+        flat = normed[:, cut]
+        weight = gain[:, cut]
+        scaled = flat * weight
+        logistic = jax.nn.sigmoid(scaled)
+        slope = act_grad * (logistic * (1.0 + scaled * (1.0 - logistic))) * weight
+        spread[:row_count, cut] = slope
+        grad_sum = grad_sum + jnp.sum(slope, axis=1, keepdims=True)
+        grad_corr = grad_corr + jnp.sum(slope * flat, axis=1, keepdims=True)
+    paired(1, grad_sum, grad_corr)
+    near_relays = max(0, extent - 1 - 1)
+    for k in range(near_relays):
+        relay(k)
+    mean, corr = both_sums(1)
+    edge = (padded.shape[0] - row_count) // 2
+    scale = inverse[:, 0:1]
+    for n in range(strips):
+        cut = slice(n * strip, (n + 1) * strip)
+        padded[edge : edge + row_count, cut] = (
+            scale * (spread[:row_count, cut] - mean - normed[:, cut] * corr)
+        ).astype(jnp.bfloat16)
+
+    def halo_copy(up_way):
+        if up_way:
+            src, dst, to = row_count, 0, sp + 1
+        else:
+            src, dst, to = edge, edge + row_count, sp - 1
+        return remote(
+            padded.at[pl.ds(src, edge), :],
+            padded.at[pl.ds(dst, edge), :],
+            halo_sems.at[0, int(up_way)],
+            halo_sems.at[1, int(up_way)],
+            to,
+            tp,
+        )
+
+    inside = {True: sp < last_sp, False: sp > 0}
+    for up_way in (True, False):
+
+        @pl.when(inside[up_way])
+        def _():
+            halo_copy(up_way).start()
+
+    for k in range(near_relays, extent - 1):
+        relay(k)
+
+    for up_way in (True, False):
+        at = 0 if up_way else edge + row_count
+
+        @pl.when(inside[not up_way])
+        def _():
+            halo_copy(up_way).wait_recv()
+
+        @pl.when(jnp.logical_not(inside[not up_way]))
+        def _():
+            padded[at : at + edge, :] = jnp.zeros((edge, local), jnp.bfloat16)
+
+    tap_count = taps.shape[0]
+    reach = tap_count // 2
+    narrow = min(128, local)
+    spread[...] = padded[...].astype(jnp.float32)
+    depth = (edge + reach) // 8 * 8 + row_count
+
+    @pl.loop(0, local // narrow)
+    def _(n):
+        cut = pl.ds(pl.multiple_of(n * narrow, narrow), narrow)
+        acc = jnp.zeros((row_count, narrow), jnp.float32)
+        for s in range(8):
+            picks_at = [o for o in range(tap_count) if (edge + reach - o) % 8 == s]
+            if not picks_at:
+                continue
+            shifted = spread[s : s + depth, cut]
+            for o in picks_at:
+                m = (edge + reach - o) // 8 * 8
+                acc = acc + taps[o : o + 1, cut] * shifted[m : m + row_count]
+        values[:, cut] = acc.astype(jnp.bfloat16)
+
+    finish = pltpu.make_async_copy(values, input_out, load_sem.at[0])
+    finish.start()
+    for h in range(pieces):
+        for slot, there in ((z, z > 0), (extent, z < extent - 1)):
+
+            @pl.when(there)
+            def _():
+                sums_arrival(slot, h).wait_recv()
+                sums_own[:, piece_at(h)] = sums_own[:, piece_at(h)] + sums_got[
+                    slot, :, piece_at(h)
+                ].astype(jnp.float32)
+
+    store = pltpu.make_async_copy(sums_own, proj_out, load_sem.at[1])
+    store.start()
+    for i in range(2):
+        stat_copy(i).wait_send()
+    for up_way in (True, False):
+
+        @pl.when(inside[up_way])
+        def _():
+            halo_copy(up_way).wait_send()
+
+    @pl.loop(1, plane)
+    def _(i):
+        active_copy(plane_peer(i)).wait_send()
+
+    for j in range(columns):
+        token_copy(j).wait_send()
+
+        @pl.loop(1, plane)
+        def _(i):
+            for to_tp in range(2):
+                block_copy(j, plane_peer(i), to_tp).wait_send()
+
+        @pl.when(z != j)
+        def _():
+            for h in range(pieces):
+                sums_copy(j, h).wait_send()
 
     for i in range(1, extent):
         meta_copy(line_peer(i), z).wait_send()
@@ -633,16 +927,26 @@
         for out in results(origin):
             out.wait()
 
-    token_swap.wait()
-    last = pltpu.make_async_copy(tokens, tokens_out, load_sem.at[0])
-    last.start()
-    last.wait()
+    finish.wait()
+    store.wait()
 
 
 TOPK_ROWS = 2
 
 
-def routed_backward(mid_rows, cotangent, meta, gate_mat, up_mat, down_mat, capacity):
+def routed_backward(
+    mid_rows,
+    cotangent,
+    meta,
+    gate_mat,
+    up_mat,
+    down_mat,
+    filtered,
+    out_weight,
+    taps,
+    gain,
+    capacity,
+):
     sp_count = lax.axis_size("sp")
     extent = line_extent(sp_count)
     plane = sp_count // extent
@@ -651,68 +955,102 @@
     slots = plane * capacity
     kind = jnp.bfloat16
     any_space = pl.BlockSpec(memory_space=pl.ANY)
+    vmem = pl.BlockSpec(memory_space=pltpu.VMEM)
     dma = pltpu.SemaphoreType.DMA
-    columns = width // min(512, width)
+    columns = extent
+    row_count, local = filtered.shape
+    own_block = width // sp_count
+    lanes = min(max(own_block, 128), width // extent)
+    edge = -(-(taps.shape[0] // 2) // 16) * 16
     rows_shape = (extent, 2, plane, capacity, width)
     small_shape = (extent, 2 * slots, half)
+    scratch = [
+        pltpu.VMEM((2, extent, token_count, width), kind),
+        pltpu.VMEM((extent,) + meta.shape, jnp.float32),
+        pltpu.VMEM((2, extent, plane, capacity, width), kind),
+        pltpu.VMEM((2,) + rows_shape, kind),
+        pltpu.VMEM(gate_mat.shape, kind),
+        pltpu.VMEM(up_mat.shape, kind),
+        pltpu.VMEM(down_mat.shape, kind),
+        pltpu.VMEM((2 * slots, half), jnp.float32),
+        pltpu.VMEM((2 * slots, half), jnp.float32),
+        pltpu.VMEM(small_shape, kind),
+        pltpu.VMEM(small_shape, kind),
+        pltpu.VMEM(small_shape, kind),
+        pltpu.VMEM((extent, plane, capacity, width), kind),
+        pltpu.VMEM((extent, plane, capacity, width), kind),
+        pltpu.VMEM((extent, plane, capacity, width), kind),
+        pltpu.VMEM((extent, plane, capacity, width), kind),
+        pltpu.VMEM((extent, token_count, width), kind),
+        pltpu.VMEM((extent + 1, token_count, width), kind),
+        pltpu.VMEM((token_count, width), jnp.float32),
+        pltpu.VMEM((2, token_count, width), kind),
+        dma((7,)),
+        dma((2, extent)),
+        dma((2, extent, 2)),
+        dma((2, extent)),
+        dma((2, extent, plane)),
+        dma((2, extent, plane)),
+        dma((2, extent)),
+        dma((2, extent)),
+        dma((2, extent)),
+        dma((extent, plane)),
+        dma((extent, plane)),
+        dma((extent, columns)),
+        dma((extent + 1, columns)),
+        dma((5, extent)),
+        dma((2, columns)),
+        pltpu.VMEM((row_count, local), kind),
+        pltpu.VMEM(out_weight.shape, kind),
+        pltpu.VMEM((2, 2, row_count, 128), jnp.float32),
+        pltpu.VMEM((row_count, local), jnp.float32),
+        pltpu.VMEM((row_count, 128), jnp.float32),
+        pltpu.VMEM((plane, row_count, local), kind),
+        pltpu.VMEM((extent, plane, 2, token_count, lanes), kind),
+        pltpu.VMEM((extent, own_block, local), kind),
+        pltpu.VMEM((extent + 1, own_block, local), kind),
+        pltpu.VMEM((own_block, local), jnp.float32),
+        pltpu.VMEM((row_count + 2 * edge, local), kind),
+        pltpu.VMEM((row_count + 2 * edge, local), jnp.float32),
+        dma((2, 2)),
+        dma((plane,)),
+        dma((plane,)),
+        dma((extent, plane, 2)),
+        dma((extent, plane, 2)),
+        dma((extent, 2)),
+        dma((extent + 1, 2)),
+        dma((2, 2)),
+    ]
+    held = sum(
+        math.prod(s.shape) * jnp.dtype(s.dtype).itemsize
+        for s in scratch
+        if s.memory_space == pltpu.VMEM
+    )
     out = pl.pallas_call(
         functools.partial(routed_kernel, extent, plane, capacity),
         out_shape=[
-            jax.ShapeDtypeStruct((2, token_count, width), kind),
+            jax.ShapeDtypeStruct((own_block, local), jnp.float32),
+            jax.ShapeDtypeStruct((row_count, local), kind),
             jax.ShapeDtypeStruct(rows_shape, kind),
             jax.ShapeDtypeStruct(rows_shape, kind),
             jax.ShapeDtypeStruct(small_shape, kind),
             jax.ShapeDtypeStruct(small_shape, kind),
             jax.ShapeDtypeStruct(small_shape, kind),
         ],
-        in_specs=[any_space, any_space, pl.BlockSpec(memory_space=pltpu.VMEM)] + [any_space] * 3,
-        out_specs=[any_space] * 6,
-        scratch_shapes=[
-            pltpu.VMEM((2, extent, token_count, width), kind),
-            pltpu.VMEM((extent,) + meta.shape, jnp.float32),
-            pltpu.VMEM((2, extent, plane, capacity, width), kind),
-            pltpu.VMEM((2,) + rows_shape, kind),
-            pltpu.VMEM(gate_mat.shape, kind),
-            pltpu.VMEM(up_mat.shape, kind),
-            pltpu.VMEM(down_mat.shape, kind),
-            pltpu.VMEM((2 * slots, half), jnp.float32),
-            pltpu.VMEM((2 * slots, half), jnp.float32),
-            pltpu.VMEM(small_shape, kind),
-            pltpu.VMEM(small_shape, kind),
-            pltpu.VMEM(small_shape, kind),
-            pltpu.VMEM((plane, capacity, width), kind),
-            pltpu.VMEM((extent, plane, capacity, width), kind),
-            pltpu.VMEM((extent, plane, capacity, width), kind),
-            pltpu.VMEM((extent, plane, capacity, width), kind),
-            pltpu.VMEM((extent, plane, capacity, width), kind),
-            pltpu.VMEM((extent, token_count, width), kind),
-            pltpu.VMEM((extent + 1, token_count, width), kind),
-            pltpu.VMEM((token_count, width), jnp.float32),
-            pltpu.VMEM((2, token_count, width), kind),
-            dma((5,)),
-            dma((2, extent)),
-            dma((2, extent, 2)),
-            dma((2, extent)),
-            dma((2, extent, plane)),
-            dma((2, extent, plane)),
-            dma((2, extent)),
-            dma((2, extent)),
-            dma((2, extent)),
-            dma((extent, plane)),
-            dma((extent, plane)),
-            dma((extent, columns)),
-            dma((extent + 1, columns)),
-            dma((5, extent)),
-            dma((2,)),
-        ],
+        in_specs=[any_space] * 2 + [vmem] + [any_space] * 5 + [vmem] * 2,
+        out_specs=[any_space] * 7,
+        scratch_shapes=scratch,
         compiler_params=pltpu.CompilerParams(
-            collective_id=0, has_side_effects=True, vmem_limit_bytes=62 * 1024 * 1024
+            collective_id=0, has_side_effects=True, vmem_limit_bytes=min(held + SPARE, 67_043_328)
         ),
-    )(mid_rows, cotangent, meta, gate_mat, up_mat, down_mat)
-    tokens, inputs, routed, hidden, gate_pre, up_pre = out
+    )(
+        mid_rows, cotangent, meta, gate_mat, up_mat, down_mat, filtered, out_weight, taps, gain
+    )
+    proj_grad, input_grad, inputs, routed, hidden, gate_pre, up_pre = out
     every = 2 * slots * extent
     return (
-        tokens.reshape(2 * token_count, width),
+        proj_grad,
+        input_grad,
         inputs.reshape(every, width),
         routed.reshape(every, width),
         hidden.reshape(every, half),
@@ -740,44 +1078,25 @@
     local_experts = gate_weight.shape[0]
     experts = local_experts * sp_count
     capacity = 2 * token_count * per_token // sp_count
-    values = filtered.astype(jnp.float32)
-    channel_sum, squares = lax.psum(
-        (jnp.sum(values, axis=1), jnp.sum(values * values, axis=1)), "tp"
-    )
     target = slot_targets(routes, experts, capacity).astype(jnp.float32)
     meta = jnp.concatenate([target.T, route_weight.T], axis=0)
     meta = jnp.pad(meta, ((0, 8 - meta.shape[0]), (0, 0)))
-    grad_tokens, inputs, routed, hidden, gate_pre, up_pre = routed_backward(
-        mid_rows, cotangent, meta, gate_weight[0], up_weight[0], down_weight[0], capacity
+    proj_grad, input_grad, inputs, routed, hidden, gate_pre, up_pre = routed_backward(
+        mid_rows,
+        cotangent,
+        meta,
+        gate_weight[0],
+        up_weight[0],
+        down_weight[0],
+        filtered,
+        out_weight,
+        conv_taps,
+        norm_gain[None],
+        capacity,
     )
     gate_grad = transposed_product(inputs, gate_pre)[None]
     up_grad = transposed_product(inputs, up_pre)[None]
     down_grad = transposed_product(hidden, routed)[None]
-    average = channel_sum / model_width
-    variance = squares / model_width - average * average
-    inv_scale = lax.rsqrt(variance + NORM_EPS)[:, None]
-    normed = (values - average[:, None]) * inv_scale
-    scaled = normed * norm_gain
-    activated = jax.nn.silu(scaled).astype(jnp.bfloat16)
-    proj_grad, grad_tokens = reduced_products(grad_tokens, activated, "sp")
-    act_grad = lax.dot_general(
-        grad_tokens, out_weight, (((1,), (1,)), ((), ())), preferred_element_type=jnp.float32
-    )
-    scaled_grad = act_grad * silu_grad(scaled) * norm_gain
-    grad_total, corr_total = lax.psum(
-        (jnp.sum(scaled_grad, axis=1), jnp.sum(scaled_grad * normed, axis=1)), "tp"
-    )
-    grad_mean = (grad_total / model_width)[:, None]
-    grad_corr = (corr_total / model_width)[:, None]
-    conv_grad = (inv_scale * (scaled_grad - grad_mean - normed * grad_corr)).astype(jnp.bfloat16)
-    halo_width = conv_taps.shape[0] // 2
-    padded = extended(conv_grad, (("sp", 0),), halo_width)
-    seq_rows = conv_grad.shape[0]
-    accumulated = jnp.zeros(conv_grad.shape, jnp.float32)
-    for offset in range(conv_taps.shape[0]):
-        lead = 2 * halo_width - offset
-        accumulated = accumulated + conv_taps[offset] * padded[lead : lead + seq_rows]
-    input_grad = accumulated.astype(jnp.bfloat16)
     return (gate_grad, up_grad, down_grad, proj_grad, input_grad)
 
 

time: 229 us -> 209 us (0.913); the launches traced: 228 us -> 205 us
  Pallas kernels: 136 us -> 183 us
  starting transfers between devices: 21.5 us -> 0 us
  other arithmetic: 14.7 us -> 1.99 us
  waiting for transfers between devices: 12 us -> 0 us
  local copies, waits for them, and re-layouts: 14.3 us -> 2.73 us
  matrix products: 23.3 us -> 16.1 us
  blocking collectives: 5.11 us -> 0 us
    pallas_call x1, Pallas kernels: 136 us -> 183 us  [routed_backward(): pl.pallas_call(functools.partial(routed_kernel, extent, plane, capacity),...]
    ppermute x14 -> x0, starting transfers between devices: 21.5 us -> none  [the longest x12 15.1 us: reduced_products(): lax.ppermute(block, axis, [(i, i ^ 1 << order[step]) for i in range(count)])]
    ppermute x14 -> x0, waiting for transfers between devices: 12 us -> none  [the longest x12 12 us: reduced_products(): lax.ppermute(block, axis, [(i, i ^ 1 << order[step]) for i in range(count)])]
    convert_element_type x2 -> x0, other arithmetic: 7.63 us -> none  [the longest x1 7.3 us: per_device(): input_grad = accumulated.astype(jnp.bfloat16)]
    psum x2 -> x0, blocking collectives: 5.11 us -> none  [the longest x1 2.6 us: per_device(): lax.psum((jnp.sum(values, axis=1), jnp.sum(values * values, axis=1)), 'tp')]
    slice x5 -> x0, local copies, waits for them, and re-layouts: 4.8 us -> none  [the longest x2 2.48 us: per_device(): accumulated = accumulated + conv_taps[offset] * padded[lead:lead + seq_rows]]
    dot_general x1 -> x0, matrix products: 4.31 us -> none  [per_device(): lax.dot_general(grad_tokens, out_weight, (((1,), (1,)), ((), ())), prefer...]
    add x11 -> x0, other arithmetic: 2.91 us -> none  [reduced_products(): own_part + got.astype(jnp.float32)]
  transfers between devices with their start and end apart: 14 -> 0, of which waited for: 7 -> 0; matrix products, arithmetic and copies ran while one was open for 14% -> 0% of each run, Pallas kernels for 0% -> 0%
where the time goes in v2:
time: 209 us; the launch traced here: 205 us
  Pallas kernels  183 us (88%)
  matrix products  16.1 us (8%)
  local copies, waits for them, and re-layouts  2.73 us (1%)
    pallas_call x1, Pallas kernels, routed_backward(): pl.pallas_call(functools.partial(routed_kernel, extent, plane, capacity),...  183 us
    dot_general x3, matrix products, transposed_product(): lax.dot_general(left, right, (((0,), (0,)), ((), ())), preferred_element_...  15.9 us

profile of v2, /device:TPU:0, one launch (start us, length us, event | category | flops | bytes accessed | tf_op | source)
XLA Modules:
  0.0 204.8 jit_solution(11782499148922152374)
XLA Ops:
  0.6 0.8 copy.16
  1.4 0.1 eq.15
  1.6 0.2 fusion
  1.8 0.1 convert_element_type.15
  1.9 0.1 copy.17
  2.0 0.7 convert_bitcast_fusion
  2.7 1.3 select_maximum_fusion.meta
  4.0 183.3 %shard_map.146 = (f32[128,1024]{1,0:T(8,128)}, bf16[256,1024]{1,0:T(8,128)(2,1)}, bf16[4,2,4,32,2048]{4,3,2,1,0:T(8,128)(2,1)}, bf16[4,2,4,32,2048]{4,3,2,1,0:T(...) custom-call(bf16[128,2048]{1,0:T(8,128)(2,1)} %mid_hbm.1, ...), custom_call_target="tpu_custom_call" | custom-call | tf_op jit(solution)/shard_map/pallas_call | solution.py:1029
  187.3 0.0 copy-start.4
  187.3 0.0 copy-start.5
  187.3 7.0 %convolution_bitcast_fusion.2 = f32[1,2048,512]{2,1,0:T(8,128)} fusion(bf16[1024,2048]{1,0:T(8,128)(2,1)} %bitcast.31, bf16[1024,512]{1,0:T(8,128)(2,1)} %bitcast.34), kind=kOutput, calls=%fused_computation.2 | convolution fusion | flops 2147483648 | bytes 9437184 | tf_op jit(solution)/shard_map/dot_general | solution.py:28
  194.3 0.0 copy-done.4
  194.3 0.0 copy-done.5
  194.3 0.0 copy-start
  194.3 0.0 copy-start.1
  194.3 4.5 %convolution_bitcast_fusion.1 = f32[1,2048,512]{2,1,0:T(8,128)} fusion(bf16[1024,2048]{1,0:T(8,128)(2,1)S(1)} %bitcast.32, bf16[1024,512]{1,0:T(8,128)(2,1)S(1)} %bitcast.33), kind=kOutput, calls=%fused_computation.1 | convolution fusion | flops 2147483648 | bytes 9437184 | tf_op jit(solution)/shard_map/dot_general | solution.py:28
  198.8 0.0 copy-done
  198.8 0.0 copy-done.1
  198.8 0.0 copy-start.3
  198.8 0.0 copy-start.2
  198.8 4.4 %convolution_bitcast_fusion = f32[1,512,2048]{2,1,0:T(8,128)} fusion(bf16[1024,512]{1,0:T(8,128)(2,1)S(1)} %bitcast.25, bf16[1024,2048]{1,0:T(8,128)(2,1)S(1)} %bitcast.24), kind=kOutput, calls=%fused_computation | convolution fusion | flops 2147483648 | bytes 9437184 | tf_op jit(solution)/shard_map/dot_general | solution.py:28
  203.2 0.0 copy-done.3
  203.2 0.8 copy.20
  204.0 0.0 copy-done.2
  204.0 0.8 copy.21
  (1 shorter events, 0.0 us)
Async XLA Ops:
  187.3 7.1 %copy-start.4 = (bf16[4,2,4,32,2048]{4,3,2,1,0:T(8,128)(2,1)S(1)}, bf16[4,2,4,32,2048]{4,3,2,1,0:T(8,128)(2,1)}, u32[]{:S(2)}) copy-start(bf16[4,2,4,32,2048]{4,3,2,1,0:T(8,128)(2,1)} %get-tuple-element.12) | copy-start | bytes 12582916
  187.3 7.0 %copy-start.5 = (bf16[4,256,512]{2,1,0:T(8,128)(2,1)S(1)}, bf16[4,256,512]{2,1,0:T(8,128)(2,1)}, u32[]{:S(2)}) copy-start(bf16[4,256,512]{2,1,0:T(8,128)(2,1)} %get-tuple-element.14) | copy-start | bytes 3145732
  194.3 4.5 %copy-start = (bf16[4,2,4,32,2048]{4,3,2,1,0:T(8,128)(2,1)S(1)}, bf16[4,2,4,32,2048]{4,3,2,1,0:T(8,128)(2,1)}, u32[]{:S(2)}) copy-start(bf16[4,2,4,32,2048]{4,3,2,1,0:T(8,128)(2,1)} %get-tuple-element.16) | copy-start | bytes 12582916
  194.3 4.5 %copy-start.1 = (bf16[4,256,512]{2,1,0:T(8,128)(2,1)S(1)}, bf16[4,256,512]{2,1,0:T(8,128)(2,1)}, u32[]{:S(2)}) copy-start(bf16[4,256,512]{2,1,0:T(8,128)(2,1)} %get-tuple-element.15) | copy-start | bytes 3145732
  198.8 4.5 %copy-start.3 = (f32[128,1024]{1,0:T(8,128)S(1)}, f32[128,1024]{1,0:T(8,128)}, u32[]{:S(2)}) copy-start(f32[128,1024]{1,0:T(8,128)} %get-tuple-element.27) | copy-start | bytes 1572868
  198.8 5.3 %copy-start.2 = (bf16[256,1024]{1,0:T(8,128)(2,1)S(1)}, bf16[256,1024]{1,0:T(8,128)(2,1)}, u32[]{:S(2)}) copy-start(bf16[256,1024]{1,0:T(8,128)(2,1)} %get-tuple-element.28) | copy-start | bytes 1572868

commit v3 on v2

--- a/solution.py
+++ b/solution.py
@@ -42,7 +42,7 @@
         back = [i for i in range(extent) if i != own and i not in toward]
         back.sort(key=lambda i: abs(i - own))
         if own in (0, extent - 1):
-            order = toward
+            order = toward[1:] + toward[:1]
         else:
             order = toward[:1] + back + toward[1:]
         orders.append([own] + order)
@@ -157,6 +157,7 @@
     active_recv,
     block_send,
     block_recv,
+    block_swaps,
     sums_send,
     sums_recv,
     halo_sems,
@@ -210,7 +211,6 @@
     @pl.loop(1, plane)
     def _(i):
         greet(z * plane + plane_peer(i), tp)
-        greet(z * plane + plane_peer(i), other)
 
     greet(sp, other)
     last_sp = extent * plane - 1
@@ -224,7 +224,7 @@
         greet(sp + 1, tp)
 
     ends = jnp.where(sp > 0, 1, 0) + jnp.where(sp < last_sp, 1, 0)
-    pl.semaphore_wait(barrier, extent - 1 + 2 * (plane - 1) + 1 + ends)
+    pl.semaphore_wait(barrier, extent - 1 + plane - 1 + 1 + ends)
 
     def meta_copy(to_z, from_z):
         return remote(
@@ -351,20 +351,54 @@
         )
         return jnp.sum(weighted, axis=1, keepdims=True)
 
+    def late(up_way):
+        if extent < 3:
+            return False
+        return (z == extent - 2) if up_way else (z == 1)
+
+    def send_own(t, held_back):
+        for up_way in (False, True):
+            now = forwards(z, up_way)
+            if t == 1 and extent > 2:
+                now = now & (late(up_way) == held_back)
+            elif held_back:
+                continue
+
+            @pl.when(now)
+            def _():
+                tok_copy(t, z, up_way).start()
+
+    def forward(t, distance):
+        below = lax.rem(z - distance + extent, extent)
+        above = lax.rem(z + distance, extent)
+        for origin, up_way, there in (
+            (above, False, (z + distance < extent) & (z > 0)),
+            (below, True, (z >= distance) & (z < extent - 1)),
+        ):
+
+            @pl.when(there)
+            def _():
+                tok_copy(t, origin, up_way).wait_recv()
+                tok_copy(t, origin, up_way).start()
+
+        if t == 1 and extent > 2:
+
+            @pl.when(distance == extent - 2)
+            def _():
+                send_own(1, True)
+
     def arrive(t, k):
         origin = looked_up(orders, z, k)
 
-        @pl.when(k > 0)
+        @pl.when((origin != z) & jnp.logical_not(has_inflow(origin)))
         def _():
             tok_copy(t, origin, True).wait_recv()
-            if t == 0:
+
+        if t == 0:
+
+            @pl.when(origin != z)
+            def _():
                 meta_copy(origin, origin).wait_recv()
-
-        for up_way in (False, True):
-
-            @pl.when(forwards(origin, up_way))
-            def _():
-                tok_copy(t, origin, up_way).start()
 
         select = chooser(origin)
         if t == 1:
@@ -550,14 +584,12 @@
         merged = (stats[i, 0] + stats[i, 1]) / width
         return merged[:, 0:1], merged[:, 1:2]
 
-    def active_copy(q):
-        return remote(
-            active.at[p], active.at[p], active_send.at[q], active_recv.at[p], z * plane + q, tp
-        )
-
-    def active_arrival(q):
-        return remote(
-            active.at[q], active.at[q], active_send.at[q], active_recv.at[q], z * plane + q, tp
+    share = row_count // extent
+
+    def active_copy(q, owner, i):
+        part = active.at[owner, pl.ds(i * share, share)]
+        return remote(
+            part, part, active_send.at[q, i], active_recv.at[owner, i], z * plane + q, tp
         )
 
     def prepare():
@@ -579,28 +611,37 @@
             scaled = flat * gain[:, cut]
             active[p, :, cut] = (scaled * jax.nn.sigmoid(scaled)).astype(jnp.bfloat16)
 
+    def share_active(k):
         @pl.loop(1, plane)
         def _(i):
-            active_copy(plane_peer(i)).start()
-
+            active_copy(plane_peer(i), p, k).start()
+
+    send_own(0, False)
+    send_own(1, False)
     arrive(0, 0)
+    arrive(1, 0)
     prepare()
 
     @pl.loop(0, extent)
     def _(k):
-        arrive(1, k)
+        @pl.when(k > 0)
+        def _():
+            forward(1, k)
+            arrive(1, k)
+
         swap(0, k)
         first_products(k)
+        swap(1, k)
+        share_active(k)
+
+        @pl.when(k < extent - 1)
+        def _():
+            forward(0, k + 1)
+            arrive(0, k + 1)
 
         @pl.when(k > 0)
         def _():
             combine(k - 1)
-
-        swap(1, k)
-
-        @pl.when(k < extent - 1)
-        def _():
-            arrive(0, k + 1)
 
         products(k)
         send_back(k)
@@ -648,24 +689,44 @@
             other,
         )
 
-    def block_copy(j, q, to_tp):
+    def block_copy(j, q):
         return remote(
             tokens.at[tp, :, block_at(j, q)],
-            blocks.at[j, p, tp],
-            block_send.at[j, q, to_tp],
-            block_recv.at[j, p, tp],
+            blocks.at[j, tp, p],
+            block_send.at[j, q],
+            block_recv.at[j, p],
             z * plane + q,
-            to_tp,
-        )
-
-    def block_arrival(j, q, from_tp):
+            tp,
+        )
+
+    def block_arrival(j, q):
         return remote(
             tokens.at[tp, :, block_at(j, q)],
-            blocks.at[j, q, from_tp],
-            block_send.at[j, q, from_tp],
-            block_recv.at[j, q, from_tp],
+            blocks.at[j, tp, q],
+            block_send.at[j, q],
+            block_recv.at[j, q],
             z * plane + q,
-            from_tp,
+            tp,
+        )
+
+    def block_swap(j):
+        return remote(
+            blocks.at[j, tp],
+            blocks.at[j, tp],
+            block_swaps.at[0, j],
+            block_swaps.at[1, j],
+            sp,
+            other,
+        )
+
+    def block_swap_arrival(j):
+        return remote(
+            blocks.at[j, other],
+            blocks.at[j, other],
+            block_swaps.at[0, j],
+            block_swaps.at[1, j],
+            sp,
+            other,
         )
 
     for j in range(columns):
@@ -684,8 +745,7 @@
 
         @pl.loop(1, plane)
         def _(i):
-            for to_tp in range(2):
-                block_copy(j, plane_peer(i), to_tp).start()
+            block_copy(j, plane_peer(i)).start()
 
         token_copy(j).start()
 
@@ -717,60 +777,9 @@
             other,
         )
 
-    @pl.loop(1, plane)
-    def _(i):
-        active_arrival(plane_peer(i)).wait_recv()
-
-    @pl.loop(0, extent)
-    def _(k):
-        j = looked_up(sum_orders(extent), z, k)
-
-        @pl.loop(1, plane)
-        def _(i):
-            for from_tp in range(2):
-                block_arrival(j, plane_peer(i), from_tp).wait_recv()
-
+    loads[6].wait()
+    for j in range(columns):
         token_arrival(j).wait_recv()
-        for half_at in range(2):
-            blocks[j, p, half_at] = tokens[half_at, :, block_at(j, p)]
-        for n in range(strips):
-            cut = slice(n * strip, (n + 1) * strip)
-            spread[:lanes, cut] = lax.dot_general(
-                blocks[j].reshape(plane * row_count, lanes),
-                active[:, :, cut].reshape(plane * row_count, strip),
-                (((0,), (0,)), ((), ())),
-                preferred_element_type=jnp.float32,
-            )
-        start = lax.rem((j * plane + p) * own_block, lanes)
-        mine = spread[pl.ds(pl.multiple_of(start, own_block), own_block), :]
-
-        @pl.when(j == z)
-        def _():
-            sums_own[...] = mine
-
-        @pl.when(j != z)
-        def _():
-            sums_sent[j] = mine.astype(jnp.bfloat16)
-
-        @pl.when((j != z) & jnp.logical_not(has_inflow(j)))
-        def _():
-            for h in range(pieces):
-                sums_copy(j, h).start()
-
-    def relay(k):
-        j = looked_up(sum_relays(extent), z, k)
-
-        @pl.when(has_inflow(j))
-        def _():
-            for h in range(pieces):
-                sums_arrival(j, h).wait_recv()
-                sums_sent[j, :, piece_at(h)] = (
-                    sums_sent[j, :, piece_at(h)].astype(jnp.float32)
-                    + sums_got[j, :, piece_at(h)].astype(jnp.float32)
-                ).astype(jnp.bfloat16)
-                sums_copy(j, h).start()
-
-    loads[6].wait()
     grad_sum = jnp.zeros((row_count, 1), jnp.float32)
     grad_corr = jnp.zeros((row_count, 1), jnp.float32)
     for n in range(strips):
@@ -790,9 +799,6 @@
         grad_sum = grad_sum + jnp.sum(slope, axis=1, keepdims=True)
         grad_corr = grad_corr + jnp.sum(slope * flat, axis=1, keepdims=True)
     paired(1, grad_sum, grad_corr)
-    near_relays = max(0, extent - 1 - 1)
-    for k in range(near_relays):
-        relay(k)
     mean, corr = both_sums(1)
     edge = (padded.shape[0] - row_count) // 2
     scale = inverse[:, 0:1]
@@ -823,8 +829,66 @@
         def _():
             halo_copy(up_way).start()
 
-    for k in range(near_relays, extent - 1):
-        relay(k)
+    @pl.loop(1, plane)
+    def _(i):
+        for k in range(extent):
+            active_copy(plane_peer(i), plane_peer(i), k).wait_recv()
+
+    @pl.loop(0, extent)
+    def _(j):
+        blocks[j, tp, p] = tokens[tp, :, block_at(j, p)]
+
+        @pl.loop(1, plane)
+        def _(i):
+            block_arrival(j, plane_peer(i)).wait_recv()
+
+        block_swap(j).start()
+
+    @pl.loop(0, extent)
+    def _(k):
+        j = looked_up(sum_orders(extent), z, k)
+        block_swap_arrival(j).wait_recv()
+        for n in range(strips):
+            cut = slice(n * strip, (n + 1) * strip)
+            spread[:lanes, cut] = sum(
+                lax.dot_general(
+                    blocks[j, side].reshape(plane * token_count, lanes),
+                    active[:, side * token_count : (side + 1) * token_count, cut].reshape(
+                        plane * token_count, strip
+                    ),
+                    (((0,), (0,)), ((), ())),
+                    preferred_element_type=jnp.float32,
+                )
+                for side in range(2)
+            )
+        start = lax.rem((j * plane + p) * own_block, lanes)
+        mine = spread[pl.ds(pl.multiple_of(start, own_block), own_block), :]
+
+        @pl.when(j == z)
+        def _():
+            sums_own[...] = mine
+
+        @pl.when(j != z)
+        def _():
+            sums_sent[j] = mine.astype(jnp.bfloat16)
+
+        @pl.when((j != z) & jnp.logical_not(has_inflow(j)))
+        def _():
+            for h in range(pieces):
+                sums_copy(j, h).start()
+
+    def relay(k):
+        j = looked_up(sum_relays(extent), z, k)
+
+        @pl.when(has_inflow(j))
+        def _():
+            for h in range(pieces):
+                sums_arrival(j, h).wait_recv()
+                sums_sent[j, :, piece_at(h)] = (
+                    sums_sent[j, :, piece_at(h)].astype(jnp.float32)
+                    + sums_got[j, :, piece_at(h)].astype(jnp.float32)
+                ).astype(jnp.bfloat16)
+                sums_copy(j, h).start()
 
     for up_way in (True, False):
         at = 0 if up_way else edge + row_count
@@ -859,6 +923,8 @@
 
     finish = pltpu.make_async_copy(values, input_out, load_sem.at[0])
     finish.start()
+    for k in range(extent - 1):
+        relay(k)
     for h in range(pieces):
         for slot, there in ((z, z > 0), (extent, z < extent - 1)):
 
@@ -881,15 +947,17 @@
 
     @pl.loop(1, plane)
     def _(i):
-        active_copy(plane_peer(i)).wait_send()
+        for k in range(extent):
+            active_copy(plane_peer(i), p, k).wait_send()
 
     for j in range(columns):
         token_copy(j).wait_send()
 
         @pl.loop(1, plane)
         def _(i):
-            for to_tp in range(2):
-                block_copy(j, plane_peer(i), to_tp).wait_send()
+            block_copy(j, plane_peer(i)).wait_send()
+
+        block_swap(j).wait_send()
 
         @pl.when(z != j)
         def _():
@@ -1006,17 +1074,18 @@
         pltpu.VMEM((row_count, local), jnp.float32),
         pltpu.VMEM((row_count, 128), jnp.float32),
         pltpu.VMEM((plane, row_count, local), kind),
-        pltpu.VMEM((extent, plane, 2, token_count, lanes), kind),
+        pltpu.VMEM((extent, 2, plane, token_count, lanes), kind),
         pltpu.VMEM((extent, own_block, local), kind),
         pltpu.VMEM((extent + 1, own_block, local), kind),
         pltpu.VMEM((own_block, local), jnp.float32),
         pltpu.VMEM((row_count + 2 * edge, local), kind),
         pltpu.VMEM((row_count + 2 * edge, local), jnp.float32),
         dma((2, 2)),
-        dma((plane,)),
-        dma((plane,)),
-        dma((extent, plane, 2)),
-        dma((extent, plane, 2)),
+        dma((plane, extent)),
+        dma((plane, extent)),
+        dma((extent, plane)),
+        dma((extent, plane)),
+        dma((2, extent)),
         dma((extent, 2)),
         dma((extent + 1, 2)),
         dma((2, 2)),

time: 209 us -> 188 us (0.90); the launches traced: 205 us -> 187 us
  Pallas kernels: 183 us -> 166 us
    pallas_call x1, Pallas kernels: 183 us -> 166 us  [routed_backward(): pl.pallas_call(functools.partial(routed_kernel, extent, plane, capacity),...]
where the time goes in v3:
time: 188 us; the launch traced here: 187 us
  Pallas kernels  166 us (88%)
  matrix products  16.1 us (9%)
  local copies, waits for them, and re-layouts  2.73 us (1%)
  other arithmetic  1.99 us (1%)
    pallas_call x1, Pallas kernels, routed_backward(): pl.pallas_call(functools.partial(routed_kernel, extent, plane, capacity),...  166 us
    dot_general x3, matrix products, transposed_product(): lax.dot_general(left, right, (((0,), (0,)), ((), ())), preferred_element_...  15.9 us

profile of v3, /device:TPU:0, one launch (start us, length us, event | category | flops | bytes accessed | tf_op | source)
XLA Modules:
  0.0 187.3 jit_solution(5073779013119911769)
XLA Ops:
  0.6 0.8 copy.16
  1.4 0.1 eq.15
  1.6 0.2 fusion
  1.8 0.1 convert_element_type.15
  1.9 0.1 copy.17
  2.0 0.7 convert_bitcast_fusion
  2.7 1.3 select_maximum_fusion.meta
  4.0 165.8 %shard_map.146 = (f32[128,1024]{1,0:T(8,128)}, bf16[256,1024]{1,0:T(8,128)(2,1)}, bf16[4,2,4,32,2048]{4,3,2,1,0:T(8,128)(2,1)}, bf16[4,2,4,32,2048]{4,3,2,1,0:T(...) custom-call(bf16[128,2048]{1,0:T(8,128)(2,1)} %mid_hbm.1, ...), custom_call_target="tpu_custom_call" | custom-call | tf_op jit(solution)/shard_map/pallas_call | solution.py:1098
  169.8 0.0 copy-start.4
  169.8 0.0 copy-start.5
  169.8 7.0 %convolution_bitcast_fusion.2 = f32[1,2048,512]{2,1,0:T(8,128)} fusion(bf16[1024,2048]{1,0:T(8,128)(2,1)} %bitcast.31, bf16[1024,512]{1,0:T(8,128)(2,1)} %bitcast.34), kind=kOutput, calls=%fused_computation.2 | convolution fusion | flops 2147483648 | bytes 9437184 | tf_op jit(solution)/shard_map/dot_general | solution.py:28
  176.8 0.0 copy-done.4
  176.8 0.0 copy-done.5
  176.8 0.0 copy-start
  176.8 0.0 copy-start.1
  176.8 4.5 %convolution_bitcast_fusion.1 = f32[1,2048,512]{2,1,0:T(8,128)} fusion(bf16[1024,2048]{1,0:T(8,128)(2,1)S(1)} %bitcast.32, bf16[1024,512]{1,0:T(8,128)(2,1)S(1)} %bitcast.33), kind=kOutput, calls=%fused_computation.1 | convolution fusion | flops 2147483648 | bytes 9437184 | tf_op jit(solution)/shard_map/dot_general | solution.py:28
  181.3 0.0 copy-done
  181.3 0.0 copy-done.1
  181.3 0.0 copy-start.3
  181.3 0.0 copy-start.2
  181.3 4.4 %convolution_bitcast_fusion = f32[1,512,2048]{2,1,0:T(8,128)} fusion(bf16[1024,512]{1,0:T(8,128)(2,1)S(1)} %bitcast.25, bf16[1024,2048]{1,0:T(8,128)(2,1)S(1)} %bitcast.24), kind=kOutput, calls=%fused_computation | convolution fusion | flops 2147483648 | bytes 9437184 | tf_op jit(solution)/shard_map/dot_general | solution.py:28
  185.7 0.0 copy-done.3
  185.7 0.8 copy.20
  186.5 0.0 copy-done.2
  186.5 0.8 copy.21
  (1 shorter events, 0.0 us)
Async XLA Ops:
  169.8 7.1 %copy-start.4 = (bf16[4,2,4,32,2048]{4,3,2,1,0:T(8,128)(2,1)S(1)}, bf16[4,2,4,32,2048]{4,3,2,1,0:T(8,128)(2,1)}, u32[]{:S(2)}) copy-start(bf16[4,2,4,32,2048]{4,3,2,1,0:T(8,128)(2,1)} %get-tuple-element.12) | copy-start | bytes 12582916
  169.8 7.0 %copy-start.5 = (bf16[4,256,512]{2,1,0:T(8,128)(2,1)S(1)}, bf16[4,256,512]{2,1,0:T(8,128)(2,1)}, u32[]{:S(2)}) copy-start(bf16[4,256,512]{2,1,0:T(8,128)(2,1)} %get-tuple-element.14) | copy-start | bytes 3145732
  176.8 4.5 %copy-start = (bf16[4,2,4,32,2048]{4,3,2,1,0:T(8,128)(2,1)S(1)}, bf16[4,2,4,32,2048]{4,3,2,1,0:T(8,128)(2,1)}, u32[]{:S(2)}) copy-start(bf16[4,2,4,32,2048]{4,3,2,1,0:T(8,128)(2,1)} %get-tuple-element.16) | copy-start | bytes 12582916
  176.8 4.5 %copy-start.1 = (bf16[4,256,512]{2,1,0:T(8,128)(2,1)S(1)}, bf16[4,256,512]{2,1,0:T(8,128)(2,1)}, u32[]{:S(2)}) copy-start(bf16[4,256,512]{2,1,0:T(8,128)(2,1)} %get-tuple-element.15) | copy-start | bytes 3145732
  181.3 4.5 %copy-start.3 = (f32[128,1024]{1,0:T(8,128)S(1)}, f32[128,1024]{1,0:T(8,128)}, u32[]{:S(2)}) copy-start(f32[128,1024]{1,0:T(8,128)} %get-tuple-element.27) | copy-start | bytes 1572868
  181.3 5.3 %copy-start.2 = (bf16[256,1024]{1,0:T(8,128)(2,1)S(1)}, bf16[256,1024]{1,0:T(8,128)(2,1)}, u32[]{:S(2)}) copy-start(bf16[256,1024]{1,0:T(8,128)(2,1)} %get-tuple-element.28) | copy-start | bytes 1572868

commit v4 on v3

--- a/solution.py
+++ b/solution.py
@@ -47,6 +47,22 @@
             order = toward[:1] + back + toward[1:]
         orders.append([own] + order)
     return orders
+
+
+def pick_events(extent):
+    table = []
+    for own, order in enumerate(chunk_orders(extent)):
+        rest = order[1:]
+        if own in (0, extent - 1):
+            near, far = rest[-1], rest[:-1]
+            events = [(0, near)] + [(t, i) for i in far for t in range(2)] + [(1, near)]
+        else:
+            near = [i for i in rest if abs(i - own) == 1]
+            far = [i for i in rest if abs(i - own) > 1]
+            events = [(t, i) for t in range(2) for i in near]
+            events = events + [(t, i) for i in far for t in range(2)]
+        table.append(events)
+    return table
 
 
 def relay_orders(extent):
@@ -308,7 +324,10 @@
         )
 
     def band(j):
-        return pl.ds(j * step, step)
+        return pl.ds(pl.multiple_of(j * step, step), step)
+
+    def band_for(home, jj):
+        return looked_up(sum_orders(extent), home, jj)
 
     def line_copy(home, j):
         to_z = jnp.where(home > z, z + 1, z - 1)
@@ -387,28 +406,21 @@
             def _():
                 send_own(1, True)
 
-    def arrive(t, k):
-        origin = looked_up(orders, z, k)
-
+    def arrive(t, origin):
         @pl.when((origin != z) & jnp.logical_not(has_inflow(origin)))
         def _():
             tok_copy(t, origin, True).wait_recv()
 
-        if t == 0:
-
-            @pl.when(origin != z)
-            def _():
-                meta_copy(origin, origin).wait_recv()
+        @pl.when((origin != z) & (t == 0))
+        def _():
+            meta_copy(origin, origin).wait_recv()
 
         select = chooser(origin)
-        if t == 1:
-            scale = scale_of(origin)
+        scale = jnp.where(t == 1, scale_of(origin), 1.0)
         for j in range(columns):
-            picked = jnp.dot(
+            picked = scale * jnp.dot(
                 select, tok[t, origin, :, band(j)], preferred_element_type=jnp.float32
             )
-            if t == 1:
-                picked = scale * picked
             picks[t, origin, :, :, band(j)] = picked.astype(jnp.bfloat16).reshape(
                 plane, capacity, step
             )
@@ -418,6 +430,11 @@
             row_copy(t, origin, plane_peer(i)).start()
 
         rows[t, origin, 0, p] = picks[t, origin, p]
+
+    def event(i):
+        kinds = [[t for t, _ in row] for row in pick_events(extent)]
+        origins = [[origin for _, origin in row] for row in pick_events(extent)]
+        arrive(looked_up(kinds, z, i), looked_up(origins, z, i))
 
     def swap(t, k):
         origin = looked_up(orders, z, k)
@@ -538,7 +555,8 @@
             ret_arrival(origin, plane_peer(i)).wait_recv()
 
         select = chooser(origin)
-        for j in range(columns):
+        for jj in range(columns):
+            j = band_for(origin, jj)
             back = ret_got[origin, :, :, band(j)].reshape(slots, step)
             added = lax.dot_general(
                 select, back, (((0,), (0,)), ((), ())), preferred_element_type=jnp.float32
@@ -555,6 +573,20 @@
             @pl.when((origin != z) & jnp.logical_not(has_inflow(origin)))
             def _():
                 line_copy(origin, j).start()
+
+    def line_relay(k):
+        home = looked_up(relays, z, k)
+
+        @pl.when(has_inflow(home))
+        def _():
+            for jj in range(columns):
+                j = band_for(home, jj)
+                line_arrival(home, j).wait_recv()
+                line_sent[home, :, band(j)] = (
+                    line_sent[home, :, band(j)].astype(jnp.float32)
+                    + line_got[home, :, band(j)].astype(jnp.float32)
+                ).astype(jnp.bfloat16)
+                line_copy(home, j).start()
 
     for load in loads[:2]:
         load.wait()
@@ -618,8 +650,8 @@
 
     send_own(0, False)
     send_own(1, False)
-    arrive(0, 0)
-    arrive(1, 0)
+    arrive(0, z)
+    arrive(1, z)
     prepare()
 
     @pl.loop(0, extent)
@@ -627,40 +659,46 @@
         @pl.when(k > 0)
         def _():
             forward(1, k)
-            arrive(1, k)
 
         swap(0, k)
         first_products(k)
+
+        @pl.when(k == 0)
+        def _():
+            forward(0, 1)
+
+        @pl.when(k < extent - 1)
+        def _():
+            event(2 * k)
+
+        @pl.when((k > 0) & (k < extent - 1))
+        def _():
+            forward(0, k + 1)
+
+        @pl.when((k > 0) & (k < extent - 1))
+        def _():
+            combine(k - 1)
+
         swap(1, k)
         share_active(k)
+        products(k)
 
         @pl.when(k < extent - 1)
         def _():
-            forward(0, k + 1)
-            arrive(0, k + 1)
-
-        @pl.when(k > 0)
+            event(2 * k + 1)
+
+        @pl.when(k == extent - 1)
         def _():
             combine(k - 1)
 
-        products(k)
         send_back(k)
 
+    line_relay(0)
     combine(extent - 1)
 
-    @pl.loop(0, extent - 1)
+    @pl.loop(1, extent - 1)
     def _(k):
-        home = looked_up(relays, z, k)
-
-        @pl.when(has_inflow(home))
-        def _():
-            for j in range(columns):
-                line_arrival(home, j).wait_recv()
-                line_sent[home, :, band(j)] = (
-                    line_sent[home, :, band(j)].astype(jnp.float32)
-                    + line_got[home, :, band(j)].astype(jnp.float32)
-                ).astype(jnp.bfloat16)
-                line_copy(home, j).start()
+        line_relay(k)
 
     own_block = width // (extent * plane)
     lanes = blocks.shape[4]
@@ -729,7 +767,8 @@
             other,
         )
 
-    for j in range(columns):
+    def home_band(jj):
+        j = band_for(z, jj)
         for slot, there in ((z, z > 0), (extent, z < extent - 1)):
 
             @pl.when(there)
@@ -742,12 +781,22 @@
         tokens[tp, :, band(j)] = (
             tok[1, z, :, band(j)].astype(jnp.float32) + total[:, band(j)]
         ).astype(jnp.bfloat16)
+        token_copy(j).start()
 
         @pl.loop(1, plane)
         def _(i):
             block_copy(j, plane_peer(i)).start()
 
-        token_copy(j).start()
+        blocks[j, tp, p] = tokens[tp, :, block_at(j, p)]
+
+    def swap_block(jj):
+        j = band_for(z, jj)
+
+        @pl.loop(1, plane)
+        def _(i):
+            block_arrival(j, plane_peer(i)).wait_recv()
+
+        block_swap(j).start()
 
     pieces = 2
     piece = local // pieces
@@ -777,80 +826,37 @@
             other,
         )
 
-    loads[6].wait()
-    for j in range(columns):
-        token_arrival(j).wait_recv()
-    grad_sum = jnp.zeros((row_count, 1), jnp.float32)
-    grad_corr = jnp.zeros((row_count, 1), jnp.float32)
-    for n in range(strips):
-        cut = slice(n * strip, (n + 1) * strip)
-        act_grad = lax.dot_general(
-            tokens[...].reshape(row_count, width),
-            out_weight[cut, :],
-            (((1,), (1,)), ((), ())),
-            preferred_element_type=jnp.float32,
-        )
-        flat = normed[:, cut]
-        weight = gain[:, cut]
-        scaled = flat * weight
-        logistic = jax.nn.sigmoid(scaled)
-        slope = act_grad * (logistic * (1.0 + scaled * (1.0 - logistic))) * weight
-        spread[:row_count, cut] = slope
-        grad_sum = grad_sum + jnp.sum(slope, axis=1, keepdims=True)
-        grad_corr = grad_corr + jnp.sum(slope * flat, axis=1, keepdims=True)
-    paired(1, grad_sum, grad_corr)
-    mean, corr = both_sums(1)
-    edge = (padded.shape[0] - row_count) // 2
-    scale = inverse[:, 0:1]
-    for n in range(strips):
-        cut = slice(n * strip, (n + 1) * strip)
-        padded[edge : edge + row_count, cut] = (
-            scale * (spread[:row_count, cut] - mean - normed[:, cut] * corr)
-        ).astype(jnp.bfloat16)
-
-    def halo_copy(up_way):
-        if up_way:
-            src, dst, to = row_count, 0, sp + 1
-        else:
-            src, dst, to = edge, edge + row_count, sp - 1
-        return remote(
-            padded.at[pl.ds(src, edge), :],
-            padded.at[pl.ds(dst, edge), :],
-            halo_sems.at[0, int(up_way)],
-            halo_sems.at[1, int(up_way)],
-            to,
-            tp,
-        )
-
-    inside = {True: sp < last_sp, False: sp > 0}
-    for up_way in (True, False):
-
-        @pl.when(inside[up_way])
-        def _():
-            halo_copy(up_way).start()
-
-    @pl.loop(1, plane)
-    def _(i):
-        for k in range(extent):
-            active_copy(plane_peer(i), plane_peer(i), k).wait_recv()
-
-    @pl.loop(0, extent)
-    def _(j):
-        blocks[j, tp, p] = tokens[tp, :, block_at(j, p)]
-
-        @pl.loop(1, plane)
-        def _(i):
-            block_arrival(j, plane_peer(i)).wait_recv()
-
-        block_swap(j).start()
-
-    @pl.loop(0, extent)
-    def _(k):
-        j = looked_up(sum_orders(extent), z, k)
-        block_swap_arrival(j).wait_recv()
+    def act_grads():
+        loads[6].wait()
+        for j in range(columns):
+            token_arrival(j).wait_recv()
+        grad_sum = jnp.zeros((row_count, 1), jnp.float32)
+        grad_corr = jnp.zeros((row_count, 1), jnp.float32)
         for n in range(strips):
             cut = slice(n * strip, (n + 1) * strip)
-            spread[:lanes, cut] = sum(
+            act_grad = lax.dot_general(
+                tokens[...].reshape(row_count, width),
+                out_weight[cut, :],
+                (((1,), (1,)), ((), ())),
+                preferred_element_type=jnp.float32,
+            )
+            flat = normed[:, cut]
+            weight = gain[:, cut]
+            scaled = flat * weight
+            logistic = jax.nn.sigmoid(scaled)
+            slope = act_grad * (logistic * (1.0 + scaled * (1.0 - logistic))) * weight
+            spread[:row_count, cut] = slope
+            grad_sum = grad_sum + jnp.sum(slope, axis=1, keepdims=True)
+            grad_corr = grad_corr + jnp.sum(slope * flat, axis=1, keepdims=True)
+        paired(1, grad_sum, grad_corr)
+
+    def partial_block(jj):
+        j = band_for(z, jj)
+        block_swap_arrival(j).wait_recv()
+        at = lax.rem((j * plane + p) * own_block, lanes)
+        for n in range(strips):
+            cut = slice(n * strip, (n + 1) * strip)
+            mine = sum(
                 lax.dot_general(
                     blocks[j, side].reshape(plane * token_count, lanes),
                     active[:, side * token_count : (side + 1) * token_count, cut].reshape(
@@ -861,21 +867,77 @@
                 )
                 for side in range(2)
             )
-        start = lax.rem((j * plane + p) * own_block, lanes)
-        mine = spread[pl.ds(pl.multiple_of(start, own_block), own_block), :]
-
-        @pl.when(j == z)
-        def _():
-            sums_own[...] = mine
-
-        @pl.when(j != z)
-        def _():
-            sums_sent[j] = mine.astype(jnp.bfloat16)
+            if own_block != lanes:
+                mine = sum(
+                    jnp.where(at == start, mine[start : start + own_block], 0.0)
+                    for start in range(0, lanes, own_block)
+                )
+
+            @pl.when(j == z)
+            def _():
+                sums_own[:, cut] = mine
+
+            @pl.when(j != z)
+            def _():
+                sums_sent[j, :, cut] = mine.astype(jnp.bfloat16)
 
         @pl.when((j != z) & jnp.logical_not(has_inflow(j)))
         def _():
             for h in range(pieces):
                 sums_copy(j, h).start()
+
+    @pl.loop(1, plane)
+    def _(i):
+        for k in range(extent):
+            active_copy(plane_peer(i), plane_peer(i), k).wait_recv()
+
+    @pl.loop(0, extent + 2)
+    def _(jj):
+        @pl.when(jj < extent)
+        def _():
+            home_band(jj)
+
+        @pl.when(jj == extent)
+        def _():
+            act_grads()
+
+        @pl.when((jj > 0) & (jj <= extent))
+        def _():
+            swap_block(jj - 1)
+
+        @pl.when(jj > 1)
+        def _():
+            partial_block(jj - 2)
+
+    mean, corr = both_sums(1)
+    edge = (padded.shape[0] - row_count) // 2
+    scale = inverse[:, 0:1]
+    for n in range(strips):
+        cut = slice(n * strip, (n + 1) * strip)
+        padded[edge : edge + row_count, cut] = (
+            scale * (spread[:row_count, cut] - mean - normed[:, cut] * corr)
+        ).astype(jnp.bfloat16)
+
+    def halo_copy(up_way):
+        if up_way:
+            src, dst, to = row_count, 0, sp + 1
+        else:
+            src, dst, to = edge, edge + row_count, sp - 1
+        return remote(
+            padded.at[pl.ds(src, edge), :],
+            padded.at[pl.ds(dst, edge), :],
+            halo_sems.at[0, int(up_way)],
+            halo_sems.at[1, int(up_way)],
+            to,
+            tp,
+        )
+
+    inside = {True: sp < last_sp, False: sp > 0}
+    for up_way in (True, False):
+
+        @pl.when(inside[up_way])
+        def _():
+            halo_copy(up_way).start()
 
     def relay(k):
         j = looked_up(sum_relays(extent), z, k)
@@ -890,6 +952,7 @@
                 ).astype(jnp.bfloat16)
                 sums_copy(j, h).start()
 
+    relay(0)
     for up_way in (True, False):
         at = 0 if up_way else edge + row_count
 
@@ -923,7 +986,7 @@
 
     finish = pltpu.make_async_copy(values, input_out, load_sem.at[0])
     finish.start()
-    for k in range(extent - 1):
+    for k in range(1, extent - 1):
         relay(k)
     for h in range(pieces):
         for slot, there in ((z, z > 0), (extent, z < extent - 1)):

time: 188 us -> 179 us (0.952)
  Pallas kernels: 166 us -> 157 us
    pallas_call x1, Pallas kernels: 166 us -> 157 us  [routed_backward(): pl.pallas_call(functools.partial(routed_kernel, extent, plane, capacity),...]
where the time goes in v4:
time: 179 us
  Pallas kernels  157 us (88%)
  matrix products  16.1 us (9%)
  local copies, waits for them, and re-layouts  2.73 us (2%)
  other arithmetic  1.99 us (1%)
    pallas_call x1, Pallas kernels, routed_backward(): pl.pallas_call(functools.partial(routed_kernel, extent, plane, capacity),...  157 us
    dot_general x3, matrix products, transposed_product(): lax.dot_general(left, right, (((0,), (0,)), ((), ())), preferred_element_...  15.9 us

profile of v4, /device:TPU:0, one launch (start us, length us, event | category | flops | bytes accessed | tf_op | source)
XLA Modules:
  0.0 178.7 jit_solution(9668611730113214358)
XLA Ops:
  0.6 0.8 copy.16
  1.4 0.1 eq.15
  1.6 0.2 fusion
  1.8 0.1 convert_element_type.15
  1.9 0.1 copy.17
  2.0 0.7 convert_bitcast_fusion
  2.7 1.3 select_maximum_fusion.meta
  4.0 157.2 %shard_map.146 = (f32[128,1024]{1,0:T(8,128)}, bf16[256,1024]{1,0:T(8,128)(2,1)}, bf16[4,2,4,32,2048]{4,3,2,1,0:T(8,128)(2,1)}, bf16[4,2,4,32,2048]{4,3,2,1,0:T(...) custom-call(bf16[128,2048]{1,0:T(8,128)(2,1)} %mid_hbm.1, ...), custom_call_target="tpu_custom_call" | custom-call | tf_op jit(solution)/shard_map/pallas_call | solution.py:1161
  161.2 0.0 copy-start.4
  161.2 0.0 copy-start.5
  161.2 7.0 %convolution_bitcast_fusion.2 = f32[1,2048,512]{2,1,0:T(8,128)} fusion(bf16[1024,2048]{1,0:T(8,128)(2,1)} %bitcast.31, bf16[1024,512]{1,0:T(8,128)(2,1)} %bitcast.34), kind=kOutput, calls=%fused_computation.2 | convolution fusion | flops 2147483648 | bytes 9437184 | tf_op jit(solution)/shard_map/dot_general | solution.py:28
  168.2 0.0 copy-done.4
  168.2 0.0 copy-done.5
  168.2 0.0 copy-start
  168.2 0.0 copy-start.1
  168.2 4.5 %convolution_bitcast_fusion.1 = f32[1,2048,512]{2,1,0:T(8,128)} fusion(bf16[1024,2048]{1,0:T(8,128)(2,1)S(1)} %bitcast.32, bf16[1024,512]{1,0:T(8,128)(2,1)S(1)} %bitcast.33), kind=kOutput, calls=%fused_computation.1 | convolution fusion | flops 2147483648 | bytes 9437184 | tf_op jit(solution)/shard_map/dot_general | solution.py:28
  172.7 0.0 copy-done
  172.7 0.0 copy-done.1
  172.7 0.0 copy-start.3
  172.7 0.0 copy-start.2
  172.7 4.4 %convolution_bitcast_fusion = f32[1,512,2048]{2,1,0:T(8,128)} fusion(bf16[1024,512]{1,0:T(8,128)(2,1)S(1)} %bitcast.25, bf16[1024,2048]{1,0:T(8,128)(2,1)S(1)} %bitcast.24), kind=kOutput, calls=%fused_computation | convolution fusion | flops 2147483648 | bytes 9437184 | tf_op jit(solution)/shard_map/dot_general | solution.py:28
  177.1 0.0 copy-done.3
  177.1 0.8 copy.20
  177.9 0.0 copy-done.2
  177.9 0.8 copy.21
  (1 shorter events, 0.0 us)
Async XLA Ops:
  161.2 7.1 %copy-start.4 = (bf16[4,2,4,32,2048]{4,3,2,1,0:T(8,128)(2,1)S(1)}, bf16[4,2,4,32,2048]{4,3,2,1,0:T(8,128)(2,1)}, u32[]{:S(2)}) copy-start(bf16[4,2,4,32,2048]{4,3,2,1,0:T(8,128)(2,1)} %get-tuple-element.12) | copy-start | bytes 12582916
  161.2 7.0 %copy-start.5 = (bf16[4,256,512]{2,1,0:T(8,128)(2,1)S(1)}, bf16[4,256,512]{2,1,0:T(8,128)(2,1)}, u32[]{:S(2)}) copy-start(bf16[4,256,512]{2,1,0:T(8,128)(2,1)} %get-tuple-element.14) | copy-start | bytes 3145732
  168.2 4.5 %copy-start = (bf16[4,2,4,32,2048]{4,3,2,1,0:T(8,128)(2,1)S(1)}, bf16[4,2,4,32,2048]{4,3,2,1,0:T(8,128)(2,1)}, u32[]{:S(2)}) copy-start(bf16[4,2,4,32,2048]{4,3,2,1,0:T(8,128)(2,1)} %get-tuple-element.16) | copy-start | bytes 12582916
  168.2 4.5 %copy-start.1 = (bf16[4,256,512]{2,1,0:T(8,128)(2,1)S(1)}, bf16[4,256,512]{2,1,0:T(8,128)(2,1)}, u32[]{:S(2)}) copy-start(bf16[4,256,512]{2,1,0:T(8,128)(2,1)} %get-tuple-element.15) | copy-start | bytes 3145732
  172.7 4.5 %copy-start.3 = (f32[128,1024]{1,0:T(8,128)S(1)}, f32[128,1024]{1,0:T(8,128)}, u32[]{:S(2)}) copy-start(f32[128,1024]{1,0:T(8,128)} %get-tuple-element.27) | copy-start | bytes 1572868
  172.7 5.3 %copy-start.2 = (bf16[256,1024]{1,0:T(8,128)(2,1)S(1)}, bf16[256,1024]{1,0:T(8,128)(2,1)}, u32[]{:S(2)}) copy-start(bf16[256,1024]{1,0:T(8,128)(2,1)} %get-tuple-element.28) | copy-start | bytes 1572868

commit v5 on v4

--- a/solution.py
+++ b/solution.py
@@ -11,23 +11,6 @@
 MESH = pl.DeviceIdType.MESH
 NORM_EPS = 1e-05
 SPARE = 4 << 20
-
-
-def slot_targets(routes, experts, capacity):
-    token_count, per_token = routes.shape
-    flattened = routes.reshape(token_count * per_token)
-    one_hot = flattened[:, None] == jnp.arange(experts, dtype=jnp.int32)[None, :]
-    route_ids = jnp.arange(token_count * per_token, dtype=jnp.int32)
-    before = (route_ids[None, :] < route_ids[:, None]).astype(jnp.bfloat16)
-    earlier = jnp.dot(before, one_hot.astype(jnp.bfloat16), preferred_element_type=jnp.float32)
-    positions = jnp.sum(jnp.where(one_hot, earlier, 0.0), axis=1).astype(jnp.int32)
-    return (flattened * capacity + positions).reshape(token_count, per_token)
-
-
-def transposed_product(left, right):
-    return lax.dot_general(
-        left, right, (((0,), (0,)), ((), ())), preferred_element_type=jnp.float32
-    )
 
 
 def line_extent(count):
@@ -106,7 +89,8 @@
     capacity,
     mid_hbm,
     cot_hbm,
-    meta,
+    routes,
+    route_weight,
     gate_hbm,
     up_hbm,
     down_hbm,
@@ -116,12 +100,11 @@
     gain,
     proj_out,
     input_out,
-    inputs_out,
-    routed_out,
-    hidden_out,
-    gate_pre_out,
-    up_pre_out,
+    gate_out,
+    up_out,
+    down_out,
     tok,
+    meta,
     metas,
     picks,
     rows,
@@ -208,6 +191,24 @@
     ]
     for load in loads:
         load.start()
+    experts = extent * plane
+    chosen = [
+        lax.broadcasted_iota(jnp.int32, (experts, token_count), 0) == routes[k : k + 1, :]
+        for k in range(TOPK_ROWS)
+    ]
+    taken = jnp.where(chosen[0] | chosen[1], 1.0, 0.0).astype(jnp.bfloat16)
+    square = (token_count, token_count)
+    before = lax.broadcasted_iota(jnp.int32, square, 0) < lax.broadcasted_iota(jnp.int32, square, 1)
+    earlier = jnp.dot(
+        taken,
+        jnp.where(before, 1.0, 0.0).astype(jnp.bfloat16),
+        preferred_element_type=jnp.float32,
+    )
+    for k in range(TOPK_ROWS):
+        place = jnp.sum(jnp.where(chosen[k], earlier, 0.0), axis=0, keepdims=True)
+        meta[k : k + 1, :] = place + (routes[k : k + 1, :] * capacity).astype(jnp.float32)
+        meta[TOPK_ROWS + k : TOPK_ROWS + k + 1, :] = route_weight[k : k + 1, :]
+    meta[2 * TOPK_ROWS :, :] = jnp.zeros((8 - 2 * TOPK_ROWS, token_count), jnp.float32)
     metas[z] = meta[...]
 
     barrier = pltpu.get_barrier_semaphore()
@@ -516,21 +517,35 @@
             part_sent[origin, :, :, cut] = part[1]
 
         part_copy(origin).start()
-        for out in results(origin):
-            out.start()
-
-    def results(origin):
-        pairs = [
-            (rows.at[0, origin], inputs_out.at[origin]),
-            (rows.at[1, origin], routed_out.at[origin]),
-            (hidden.at[origin], hidden_out.at[origin]),
-            (gate_pre.at[origin], gate_pre_out.at[origin]),
-            (up_pre.at[origin], up_pre_out.at[origin]),
-        ]
-        return [
-            pltpu.make_async_copy(src, dst, out_sems.at[i, origin])
-            for i, (src, dst) in enumerate(pairs)
-        ]
+
+    def all_rows(t, cut):
+        return rows[t, :, :, :, :, cut].reshape(extent * 2 * slots, -1)
+
+    def small_rows(ref, cut):
+        return ref[:, :, cut].reshape(extent * 2 * slots, -1)
+
+    def weight_grads(which):
+        store = pltpu.make_async_copy(
+            (gate, up, down)[which], (gate_out, up_out, down_out)[which], out_sems.at[which]
+        )
+        size = width if which < 2 else half
+        deep = min(256, size)
+
+        @pl.loop(0, size // deep)
+        def _(n):
+            cut = pl.ds(pl.multiple_of(n * deep, deep), deep)
+            if which < 2:
+                left = all_rows(0, cut)
+                right = small_rows((gate_pre, up_pre)[which], slice(None))
+            else:
+                left = small_rows(hidden, cut)
+                right = all_rows(1, slice(None))
+            (gate, up, down)[which][cut, :] = lax.dot_general(
+                left, right, (((0,), (0,)), ((), ())), preferred_element_type=jnp.float32
+            ).astype(jnp.bfloat16)
+
+        store.start()
+        return store
 
     def send_back(k):
         origin = looked_up(orders, z, k)
@@ -696,9 +711,16 @@
     line_relay(0)
     combine(extent - 1)
 
-    @pl.loop(1, extent - 1)
+    stores = [weight_grads(0)]
+    if extent > 2:
+        line_relay(1)
+    stores.append(weight_grads(1))
+
+    @pl.loop(2, extent - 1)
     def _(k):
         line_relay(k)
+
+    stores.append(weight_grads(2))
 
     own_block = width // (extent * plane)
     lanes = blocks.shape[4]
@@ -953,41 +975,48 @@
                 sums_copy(j, h).start()
 
     relay(0)
-    for up_way in (True, False):
-        at = 0 if up_way else edge + row_count
-
-        @pl.when(inside[not up_way])
-        def _():
-            halo_copy(up_way).wait_recv()
-
-        @pl.when(jnp.logical_not(inside[not up_way]))
-        def _():
-            padded[at : at + edge, :] = jnp.zeros((edge, local), jnp.bfloat16)
-
     tap_count = taps.shape[0]
     reach = tap_count // 2
     narrow = min(128, local)
-    spread[...] = padded[...].astype(jnp.float32)
-    depth = (edge + reach) // 8 * 8 + row_count
-
-    @pl.loop(0, local // narrow)
-    def _(n):
-        cut = pl.ds(pl.multiple_of(n * narrow, narrow), narrow)
-        acc = jnp.zeros((row_count, narrow), jnp.float32)
-        for s in range(8):
-            picks_at = [o for o in range(tap_count) if (edge + reach - o) % 8 == s]
-            if not picks_at:
-                continue
-            shifted = spread[s : s + depth, cut]
-            for o in picks_at:
-                m = (edge + reach - o) // 8 * 8
-                acc = acc + taps[o : o + 1, cut] * shifted[m : m + row_count]
-        values[:, cut] = acc.astype(jnp.bfloat16)
-
+    extra = (edge + reach) // 8 * 8
+
+    def convolve(first, count):
+        @pl.loop(0, local // narrow)
+        def _(n):
+            cut = pl.ds(pl.multiple_of(n * narrow, narrow), narrow)
+            acc = jnp.zeros((count, narrow), jnp.float32)
+            for s in range(8):
+                taps_at = [o for o in range(tap_count) if (edge + reach - o) % 8 == s]
+                if not taps_at:
+                    continue
+                shifted = spread[first + s : first + s + extra + count, cut]
+                for o in taps_at:
+                    m = (edge + reach - o) // 8 * 8
+                    acc = acc + taps[o : o + 1, cut] * shifted[m : m + count]
+            values[first : first + count, cut] = acc.astype(jnp.bfloat16)
+
+    inner = slice(edge, edge + row_count)
+    spread[inner] = padded[inner].astype(jnp.float32)
+    if row_count > 2 * edge:
+        convolve(edge, row_count - 2 * edge)
+    for k in range(1, extent - 1):
+        relay(k)
+    for up_way in (True, False):
+        at = 0 if up_way else edge + row_count
+
+        @pl.when(inside[not up_way])
+        def _():
+            halo_copy(up_way).wait_recv()
+            spread[at : at + edge, :] = padded[at : at + edge, :].astype(jnp.float32)
+
+        @pl.when(jnp.logical_not(inside[not up_way]))
+        def _():
+            spread[at : at + edge, :] = jnp.zeros((edge, local), jnp.float32)
+
+    convolve(0, edge)
+    convolve(row_count - edge, edge)
     finish = pltpu.make_async_copy(values, input_out, load_sem.at[0])
     finish.start()
-    for k in range(1, extent - 1):
-        relay(k)
     for h in range(pieces):
         for slot, there in ((z, z > 0), (extent, z < extent - 1)):
 
@@ -1055,11 +1084,11 @@
             for j in range(columns):
                 line_copy(origin, j).wait_send()
 
-        for out in results(origin):
-            out.wait()
 
     finish.wait()
     store.wait()
+    for store in stores:
+        store.wait()
 
 
 TOPK_ROWS = 2
@@ -1068,7 +1097,8 @@
 def routed_backward(
     mid_rows,
     cotangent,
-    meta,
+    routes,
+    route_weight,
     gate_mat,
     up_mat,
     down_mat,
@@ -1097,7 +1127,8 @@
     small_shape = (extent, 2 * slots, half)
     scratch = [
         pltpu.VMEM((2, extent, token_count, width), kind),
-        pltpu.VMEM((extent,) + meta.shape, jnp.float32),
+        pltpu.VMEM((8, token_count), jnp.float32),
+        pltpu.VMEM((extent, 8, token_count), jnp.float32),
         pltpu.VMEM((2, extent, plane, capacity, width), kind),
         pltpu.VMEM((2,) + rows_shape, kind),
         pltpu.VMEM(gate_mat.shape, kind),
@@ -1129,7 +1160,7 @@
         dma((extent, plane)),
         dma((extent, columns)),
         dma((extent + 1, columns)),
-        dma((5, extent)),
+        dma((3,)),
         dma((2, columns)),
         pltpu.VMEM((row_count, local), kind),
         pltpu.VMEM(out_weight.shape, kind),
@@ -1163,32 +1194,30 @@
         out_shape=[
             jax.ShapeDtypeStruct((own_block, local), jnp.float32),
             jax.ShapeDtypeStruct((row_count, local), kind),
-            jax.ShapeDtypeStruct(rows_shape, kind),
-            jax.ShapeDtypeStruct(rows_shape, kind),
-            jax.ShapeDtypeStruct(small_shape, kind),
-            jax.ShapeDtypeStruct(small_shape, kind),
-            jax.ShapeDtypeStruct(small_shape, kind),
+            jax.ShapeDtypeStruct(gate_mat.shape, kind),
+            jax.ShapeDtypeStruct(up_mat.shape, kind),
+            jax.ShapeDtypeStruct(down_mat.shape, kind),
         ],
-        in_specs=[any_space] * 2 + [vmem] + [any_space] * 5 + [vmem] * 2,
-        out_specs=[any_space] * 7,
+        in_specs=[any_space] * 2 + [vmem] * 2 + [any_space] * 5 + [vmem] * 2,
+        out_specs=[any_space] * 5,
         scratch_shapes=scratch,
         compiler_params=pltpu.CompilerParams(
             collective_id=0, has_side_effects=True, vmem_limit_bytes=min(held + SPARE, 67_043_328)
         ),
     )(
-        mid_rows, cotangent, meta, gate_mat, up_mat, down_mat, filtered, out_weight, taps, gain
+        mid_rows,
+        cotangent,
+        routes,
+        route_weight,
+        gate_mat,
+        up_mat,
+        down_mat,
+        filtered,
+        out_weight,
+        taps,
+        gain,
     )
-    proj_grad, input_grad, inputs, routed, hidden, gate_pre, up_pre = out
-    every = 2 * slots * extent
-    return (
-        proj_grad,
-        input_grad,
-        inputs.reshape(every, width),
-        routed.reshape(every, width),
-        hidden.reshape(every, half),
-        gate_pre.reshape(every, half),
-        up_pre.reshape(every, half),
-    )
+    return out
 
 
 def per_device(
@@ -1210,13 +1239,11 @@
     local_experts = gate_weight.shape[0]
     experts = local_experts * sp_count
     capacity = 2 * token_count * per_token // sp_count
-    target = slot_targets(routes, experts, capacity).astype(jnp.float32)
-    meta = jnp.concatenate([target.T, route_weight.T], axis=0)
-    meta = jnp.pad(meta, ((0, 8 - meta.shape[0]), (0, 0)))
-    proj_grad, input_grad, inputs, routed, hidden, gate_pre, up_pre = routed_backward(
+    proj_grad, input_grad, *weight_grads = routed_backward(
         mid_rows,
         cotangent,
-        meta,
+        routes.T,
+        route_weight.T,
         gate_weight[0],
         up_weight[0],
         down_weight[0],
@@ -1226,9 +1253,7 @@
         norm_gain[None],
         capacity,
     )
-    gate_grad = transposed_product(inputs, gate_pre)[None]
-    up_grad = transposed_product(inputs, up_pre)[None]
-    down_grad = transposed_product(hidden, routed)[None]
+    gate_grad, up_grad, down_grad = (grad.astype(jnp.float32)[None] for grad in weight_grads)
     return (gate_grad, up_grad, down_grad, proj_grad, input_grad)
 
 

time: 179 us -> 165 us (0.922)
  matrix products: 16.1 us -> 0 us
  other arithmetic: 1.99 us -> 9.51 us
  Pallas kernels: 157 us -> 153 us
    dot_general x4 -> x0, matrix products: 16.1 us -> none  [the longest x3 15.9 us: transposed_product(): lax.dot_general(left, right, (((0,), (0,)), ((), ())), preferred_element_...]
    broadcast_in_dim x0 -> x2, other arithmetic: none -> 9.51 us  [per_device(): grad.astype(jnp.float32)[None]]
    pallas_call x1, Pallas kernels: 157 us -> 153 us  [routed_backward(): pl.pallas_call(functools.partial(routed_kernel, extent, plane, capacity),...]
where the time goes in v5:
time: 165 us
  Pallas kernels  153 us (93%)
  other arithmetic  9.51 us (6%)
    pallas_call x1, Pallas kernels, routed_backward(): pl.pallas_call(functools.partial(routed_kernel, extent, plane, capacity),...  153 us
    broadcast_in_dim x2, other arithmetic, per_device(): grad.astype(jnp.float32)[None]  9.51 us

profile of v5, /device:TPU:0, one launch (start us, length us, event | category | flops | bytes accessed | tf_op | source)
XLA Modules:
  0.0 165.3 jit_solution(14291439533978934074)
XLA Ops:
  0.6 153.5 %shard_map.146 = (f32[128,1024]{1,0:T(8,128)}, bf16[256,1024]{1,0:T(8,128)(2,1)}, bf16[2048,512]{1,0:T(8,128)(2,1)}, bf16[2048,512]{1,0:T(8,128)(2,1)}, bf16[512,2048]{1,0:T(8,128)(2,1)}) custom-call(bf16[128,2048]{1,0:T(8,128)(2,1)} %mid_hbm.1, bf16[128,2048]{1,0:T(8,128)(2,1)} %cot_hbm.1, s32[2,128]{1,0:T(2,128)} %bitcast.19, f32[2,128]{1,0:T(2,128)} %bitcast.20, ...), custom_call_target="tpu_custom_call" | custom-call | tf_op jit(solution)/shard_map/pallas_call | solution.py:1192
  154.1 0.0 copy-start
  154.2 7.0 %bitcast_convert_fusion.1 = (f32[1,2048,512]{2,1,0:T(8,128)}, f32[1,2048,512]{2,1,0:T(8,128)}) fusion(bf16[2048,512]{1,0:T(8,128)(2,1)} %get-tuple-element.11, bf16[2048,512]{1,0:T(8,128)(2,1)} %get-tuple-element.10), kind=kLoop, calls=%fused_computation.1 | loop fusion | flops 2097152 | bytes 12582912 | tf_op jit(solution)/shard_map/broadcast_in_dim | solution.py:1256
  161.1 0.0 copy-done
  161.1 0.0 copy-start.2
  161.1 0.0 copy-start.1
  161.1 2.5 %bitcast_convert_fusion = f32[1,512,2048]{2,1,0:T(8,128)} fusion(bf16[512,2048]{1,0:T(8,128)(2,1)S(1)} %copy-done), kind=kLoop, calls=%fused_computation | loop fusion | flops 1048576 | bytes 6291456 | tf_op jit(solution)/shard_map/broadcast_in_dim | solution.py:1256
  163.7 0.0 copy-done.2
  163.7 0.8 copy.18
  164.5 0.0 copy-done.1
  164.5 0.8 copy.19
Async XLA Ops:
  154.1 7.0 %copy-start = (bf16[512,2048]{1,0:T(8,128)(2,1)S(1)}, bf16[512,2048]{1,0:T(8,128)(2,1)}, u32[]{:S(2)}) copy-start(bf16[512,2048]{1,0:T(8,128)(2,1)} %get-tuple-element.12) | copy-start | bytes 6291460
  161.1 2.5 %copy-start.2 = (f32[128,1024]{1,0:T(8,128)S(1)}, f32[128,1024]{1,0:T(8,128)}, u32[]{:S(2)}) copy-start(f32[128,1024]{1,0:T(8,128)} %get-tuple-element.25) | copy-start | bytes 1572868
  161.1 3.3 %copy-start.1 = (bf16[256,1024]{1,0:T(8,128)(2,1)S(1)}, bf16[256,1024]{1,0:T(8,128)(2,1)}, u32[]{:S(2)}) copy-start(bf16[256,1024]{1,0:T(8,128)(2,1)} %get-tuple-element.26) | copy-start | bytes 1572868

commit v6 on v5

--- a/solution.py
+++ b/solution.py
@@ -372,19 +372,15 @@
         return jnp.sum(weighted, axis=1, keepdims=True)
 
     def late(up_way):
-        if extent < 3:
-            return False
         return (z == extent - 2) if up_way else (z == 1)
 
-    def send_own(t, held_back):
+    def send_own(t):
         for up_way in (False, True):
-            now = forwards(z, up_way)
-            if t == 1 and extent > 2:
-                now = now & (late(up_way) == held_back)
-            elif held_back:
-                continue
-
-            @pl.when(now)
+            whole = forwards(z, up_way)
+            if t == 1 and extent > 3:
+                whole = whole & jnp.logical_not(late(up_way))
+
+            @pl.when(whole)
             def _():
                 tok_copy(t, z, up_way).start()
 
@@ -401,11 +397,12 @@
                 tok_copy(t, origin, up_way).wait_recv()
                 tok_copy(t, origin, up_way).start()
 
-        if t == 1 and extent > 2:
-
-            @pl.when(distance == extent - 2)
-            def _():
-                send_own(1, True)
+        if t == 1 and extent > 3:
+            for up_way in (False, True):
+
+                @pl.when((distance == extent - 2) & late(up_way))
+                def _():
+                    tok_copy(1, z, up_way).start()
 
     def arrive(t, origin):
         @pl.when((origin != z) & jnp.logical_not(has_inflow(origin)))
@@ -524,16 +521,15 @@
     def small_rows(ref, cut):
         return ref[:, :, cut].reshape(extent * 2 * slots, -1)
 
-    def weight_grads(which):
-        store = pltpu.make_async_copy(
+    def grad_store(which):
+        return pltpu.make_async_copy(
             (gate, up, down)[which], (gate_out, up_out, down_out)[which], out_sems.at[which]
         )
-        size = width if which < 2 else half
-        deep = min(256, size)
-
-        @pl.loop(0, size // deep)
+
+    def grad_tiles(which, first, count, size):
+        @pl.loop(first, first + count)
         def _(n):
-            cut = pl.ds(pl.multiple_of(n * deep, deep), deep)
+            cut = pl.ds(pl.multiple_of(n * size, size), size)
             if which < 2:
                 left = all_rows(0, cut)
                 right = small_rows((gate_pre, up_pre)[which], slice(None))
@@ -544,8 +540,10 @@
                 left, right, (((0,), (0,)), ((), ())), preferred_element_type=jnp.float32
             ).astype(jnp.bfloat16)
 
-        store.start()
-        return store
+    def gate_up_share(which, jj):
+        size = min(256, width // columns)
+        each = width // columns // size
+        grad_tiles(which, jj * each, each, size)
 
     def send_back(k):
         origin = looked_up(orders, z, k)
@@ -589,19 +587,63 @@
             def _():
                 line_copy(origin, j).start()
 
-    def line_relay(k):
+    def drain(k):
+        origin = looked_up(orders, z, k)
+        for t in range(2):
+            for up_way in (False, True):
+                sent = forwards(origin, up_way)
+                if t == 1 and extent > 3:
+                    sent = sent & jnp.logical_not((origin == z) & late(up_way))
+
+                @pl.when(sent)
+                def _():
+                    tok_copy(t, origin, up_way).wait_send()
+
+            @pl.loop(1, plane)
+            def _(i):
+                row_copy(t, origin, plane_peer(i)).wait_send()
+
+            swap_copy(t, origin).wait_send()
+        part_copy(origin).wait_send()
+
+    def drain_returns():
+        for i in range(1, extent):
+            meta_copy(line_peer(i), z).wait_send()
+        if extent > 3:
+            for up_way in (False, True):
+
+                @pl.when(late(up_way))
+                def _():
+                    tok_copy(1, z, up_way).wait_send()
+
+        @pl.loop(0, extent)
+        def _(origin):
+            @pl.loop(1, plane)
+            def _(i):
+                ret_copy(origin, plane_peer(i)).wait_send()
+
+            @pl.when(origin != z)
+            def _():
+                for j in range(columns):
+                    line_copy(origin, j).wait_send()
+
+        @pl.loop(1, plane)
+        def _(i):
+            for k in range(extent):
+                active_copy(plane_peer(i), p, k).wait_send()
+
+    def relay_band(k, jj):
         home = looked_up(relays, z, k)
 
         @pl.when(has_inflow(home))
         def _():
-            for jj in range(columns):
-                j = band_for(home, jj)
-                line_arrival(home, j).wait_recv()
-                line_sent[home, :, band(j)] = (
-                    line_sent[home, :, band(j)].astype(jnp.float32)
-                    + line_got[home, :, band(j)].astype(jnp.float32)
-                ).astype(jnp.bfloat16)
-                line_copy(home, j).start()
+            j = band_for(home, jj)
+            line_arrival(home, j).wait_recv()
+            line_sent[home, :, band(j)] = (
+                line_sent[home, :, band(j)].astype(jnp.float32)
+                + line_got[home, :, band(j)].astype(jnp.float32)
+            ).astype(jnp.bfloat16)
+            line_copy(home, j).start()
 
     for load in loads[:2]:
         load.wait()
@@ -663,8 +705,8 @@
         def _(i):
             active_copy(plane_peer(i), p, k).start()
 
-    send_own(0, False)
-    send_own(1, False)
+    send_own(0)
+    send_own(1)
     arrive(0, z)
     arrive(1, z)
     prepare()
@@ -694,6 +736,10 @@
         def _():
             combine(k - 1)
 
+        @pl.when(k > 0)
+        def _():
+            drain(k - 1)
+
         swap(1, k)
         share_active(k)
         products(k)
@@ -708,19 +754,27 @@
 
         send_back(k)
 
-    line_relay(0)
+    @pl.loop(0, columns)
+    def _(jj):
+        relay_band(0, jj)
+
+    drain(extent - 1)
     combine(extent - 1)
 
-    stores = [weight_grads(0)]
-    if extent > 2:
-        line_relay(1)
-    stores.append(weight_grads(1))
-
-    @pl.loop(2, extent - 1)
-    def _(k):
-        line_relay(k)
-
-    stores.append(weight_grads(2))
+    @pl.loop(0, columns)
+    def _(jj):
+        relay_band(1, jj)
+        gate_up_share(0, jj)
+
+    grad_store(0).start()
+
+    @pl.loop(0, columns)
+    def _(jj):
+        for k in range(2, extent - 1):
+            relay_band(k, jj)
+        gate_up_share(1, jj)
+
+    grad_store(1).start()
 
     own_block = width // (extent * plane)
     lanes = blocks.shape[4]
@@ -913,17 +967,11 @@
         for k in range(extent):
             active_copy(plane_peer(i), plane_peer(i), k).wait_recv()
 
-    @pl.loop(0, extent + 2)
+    @pl.loop(0, extent)
     def _(jj):
-        @pl.when(jj < extent)
-        def _():
-            home_band(jj)
-
-        @pl.when(jj == extent)
-        def _():
-            act_grads()
-
-        @pl.when((jj > 0) & (jj <= extent))
+        home_band(jj)
+
+        @pl.when(jj > 0)
         def _():
             swap_block(jj - 1)
 
@@ -931,6 +979,8 @@
         def _():
             partial_block(jj - 2)
 
+    act_grads()
+    swap_block(extent - 1)
     mean, corr = both_sums(1)
     edge = (padded.shape[0] - row_count) // 2
     scale = inverse[:, 0:1]
@@ -973,6 +1023,10 @@
                     + sums_got[j, :, piece_at(h)].astype(jnp.float32)
                 ).astype(jnp.bfloat16)
                 sums_copy(j, h).start()
+
+    @pl.loop(max(0, extent - 2), extent)
+    def _(jj):
+        partial_block(jj)
 
     relay(0)
     tap_count = taps.shape[0]
@@ -1001,6 +1055,8 @@
         convolve(edge, row_count - 2 * edge)
     for k in range(1, extent - 1):
         relay(k)
+    grad_tiles(2, 0, half // min(256, half), min(256, half))
+    grad_store(2).start()
     for up_way in (True, False):
         at = 0 if up_way else edge + row_count
 
@@ -1017,6 +1073,7 @@
     convolve(row_count - edge, edge)
     finish = pltpu.make_async_copy(values, input_out, load_sem.at[0])
     finish.start()
+    drain_returns()
     for h in range(pieces):
         for slot, there in ((z, z > 0), (extent, z < extent - 1)):
 
@@ -1037,11 +1094,6 @@
         def _():
             halo_copy(up_way).wait_send()
 
-    @pl.loop(1, plane)
-    def _(i):
-        for k in range(extent):
-            active_copy(plane_peer(i), p, k).wait_send()
-
     for j in range(columns):
         token_copy(j).wait_send()
 
@@ -1056,39 +1108,10 @@
             for h in range(pieces):
                 sums_copy(j, h).wait_send()
 
-    for i in range(1, extent):
-        meta_copy(line_peer(i), z).wait_send()
-
-    @pl.loop(0, extent)
-    def _(origin):
-        for t in range(2):
-            for up_way in (False, True):
-
-                @pl.when(forwards(origin, up_way))
-                def _():
-                    tok_copy(t, origin, up_way).wait_send()
-
-            @pl.loop(1, plane)
-            def _(i):
-                row_copy(t, origin, plane_peer(i)).wait_send()
-
-            swap_copy(t, origin).wait_send()
-        part_copy(origin).wait_send()
-
-        @pl.loop(1, plane)
-        def _(i):
-            ret_copy(origin, plane_peer(i)).wait_send()
-
-        @pl.when(origin != z)
-        def _():
-            for j in range(columns):
-                line_copy(origin, j).wait_send()
-
-
     finish.wait()
     store.wait()
-    for store in stores:
-        store.wait()
+    for which in range(3):
+        grad_store(which).wait()
 
 
 TOPK_ROWS = 2

time: 165 us -> 163 us (0.988)
  Pallas kernels: 153 us -> 151 us
    pallas_call x1, Pallas kernels: 153 us -> 151 us  [routed_backward(): pl.pallas_call(functools.partial(routed_kernel, extent, plane, capacity),...]
where the time goes in v6:
time: 163 us; the launch traced here: 162 us
  Pallas kernels  151 us (93%)
  other arithmetic  9.51 us (6%)
    pallas_call x1, Pallas kernels, routed_backward(): pl.pallas_call(functools.partial(routed_kernel, extent, plane, capacity),...  151 us
    broadcast_in_dim x2, other arithmetic, per_device(): grad.astype(jnp.float32)[None]  9.51 us

profile of v6, /device:TPU:0, one launch (start us, length us, event | category | flops | bytes accessed | tf_op | source)
XLA Modules:
  0.0 162.4 jit_solution(1527018727159375081)
XLA Ops:
  0.6 150.7 %shard_map.146 = (f32[128,1024]{1,0:T(8,128)}, bf16[256,1024]{1,0:T(8,128)(2,1)}, bf16[2048,512]{1,0:T(8,128)(2,1)}, bf16[2048,512]{1,0:T(8,128)(2,1)}, bf16[512,2048]{1,0:T(8,128)(2,1)}) custom-call(bf16[128,2048]{1,0:T(8,128)(2,1)} %mid_hbm.1, bf16[128,2048]{1,0:T(8,128)(2,1)} %cot_hbm.1, s32[2,128]{1,0:T(2,128)} %bitcast.19, f32[2,128]{1,0:T(2,128)} %bitcast.20, ...), custom_call_target="tpu_custom_call" | custom-call | tf_op jit(solution)/shard_map/pallas_call | solution.py:1215
  151.3 0.0 copy-start
  151.3 7.0 %bitcast_convert_fusion.1 = (f32[1,2048,512]{2,1,0:T(8,128)}, f32[1,2048,512]{2,1,0:T(8,128)}) fusion(bf16[2048,512]{1,0:T(8,128)(2,1)} %get-tuple-element.11, bf16[2048,512]{1,0:T(8,128)(2,1)} %get-tuple-element.10), kind=kLoop, calls=%fused_computation.1 | loop fusion | flops 2097152 | bytes 12582912 | tf_op jit(solution)/shard_map/broadcast_in_dim | solution.py:1279
  158.3 0.0 copy-done
  158.3 0.0 copy-start.2
  158.3 0.0 copy-start.1
  158.3 2.5 %bitcast_convert_fusion = f32[1,512,2048]{2,1,0:T(8,128)} fusion(bf16[512,2048]{1,0:T(8,128)(2,1)S(1)} %copy-done), kind=kLoop, calls=%fused_computation | loop fusion | flops 1048576 | bytes 6291456 | tf_op jit(solution)/shard_map/broadcast_in_dim | solution.py:1279
  160.8 0.0 copy-done.2
  160.8 0.8 copy.18
  161.6 0.0 copy-done.1
  161.6 0.8 copy.19
Async XLA Ops:
  151.3 7.0 %copy-start = (bf16[512,2048]{1,0:T(8,128)(2,1)S(1)}, bf16[512,2048]{1,0:T(8,128)(2,1)}, u32[]{:S(2)}) copy-start(bf16[512,2048]{1,0:T(8,128)(2,1)} %get-tuple-element.12) | copy-start | bytes 6291460
  158.3 2.5 %copy-start.2 = (f32[128,1024]{1,0:T(8,128)S(1)}, f32[128,1024]{1,0:T(8,128)}, u32[]{:S(2)}) copy-start(f32[128,1024]{1,0:T(8,128)} %get-tuple-element.25) | copy-start | bytes 1572868
  158.3 3.3 %copy-start.1 = (bf16[256,1024]{1,0:T(8,128)(2,1)S(1)}, bf16[256,1024]{1,0:T(8,128)(2,1)}, u32[]{:S(2)}) copy-start(bf16[256,1024]{1,0:T(8,128)(2,1)} %get-tuple-element.26) | copy-start | bytes 1572868

commit v7 on v6

--- a/solution.py
+++ b/solution.py
@@ -740,6 +740,12 @@
         def _():
             drain(k - 1)
 
+        @pl.when(k == extent - 1)
+        def _():
+            @pl.loop(0, columns)
+            def _(jj):
+                relay_band(0, jj)
+
         swap(1, k)
         share_active(k)
         products(k)
@@ -753,10 +759,6 @@
             combine(k - 1)
 
         send_back(k)
-
-    @pl.loop(0, columns)
-    def _(jj):
-        relay_band(0, jj)
 
     drain(extent - 1)
     combine(extent - 1)
@@ -975,9 +977,9 @@
         def _():
             swap_block(jj - 1)
 
-        @pl.when(jj > 1)
-        def _():
-            partial_block(jj - 2)
+        @pl.when((jj > 0) & (jj < extent - 1))
+        def _():
+            partial_block(jj - 1)
 
     act_grads()
     swap_block(extent - 1)

time: 163 us -> 162 us (level)
  no operation moved by 1% of the time
where the time goes in v7:
time: 162 us; the launch traced here: 161 us
  Pallas kernels  150 us (93%)
  other arithmetic  9.51 us (6%)
    pallas_call x1, Pallas kernels, routed_backward(): pl.pallas_call(functools.partial(routed_kernel, extent, plane, capacity),...  150 us
    broadcast_in_dim x2, other arithmetic, per_device(): grad.astype(jnp.float32)[None]  9.51 us

profile of v7, /device:TPU:0, one launch (start us, length us, event | category | flops | bytes accessed | tf_op | source)
XLA Modules:
  0.0 161.3 jit_solution(9247355318206313674)
XLA Ops:
  0.6 149.6 %shard_map.146 = (f32[128,1024]{1,0:T(8,128)}, bf16[256,1024]{1,0:T(8,128)(2,1)}, bf16[2048,512]{1,0:T(8,128)(2,1)}, bf16[2048,512]{1,0:T(8,128)(2,1)}, bf16[512,2048]{1,0:T(8,128)(2,1)}) custom-call(bf16[128,2048]{1,0:T(8,128)(2,1)} %mid_hbm.1, bf16[128,2048]{1,0:T(8,128)(2,1)} %cot_hbm.1, s32[2,128]{1,0:T(2,128)} %bitcast.19, f32[2,128]{1,0:T(2,128)} %bitcast.20, ...), custom_call_target="tpu_custom_call" | custom-call | tf_op jit(solution)/shard_map/pallas_call | solution.py:1217
  150.2 0.0 copy-start
  150.2 7.0 %bitcast_convert_fusion.1 = (f32[1,2048,512]{2,1,0:T(8,128)}, f32[1,2048,512]{2,1,0:T(8,128)}) fusion(bf16[2048,512]{1,0:T(8,128)(2,1)} %get-tuple-element.11, bf16[2048,512]{1,0:T(8,128)(2,1)} %get-tuple-element.10), kind=kLoop, calls=%fused_computation.1 | loop fusion | flops 2097152 | bytes 12582912 | tf_op jit(solution)/shard_map/broadcast_in_dim | solution.py:1281
  157.2 0.0 copy-done
  157.2 0.0 copy-start.2
  157.2 0.0 copy-start.1
  157.2 2.5 %bitcast_convert_fusion = f32[1,512,2048]{2,1,0:T(8,128)} fusion(bf16[512,2048]{1,0:T(8,128)(2,1)S(1)} %copy-done), kind=kLoop, calls=%fused_computation | loop fusion | flops 1048576 | bytes 6291456 | tf_op jit(solution)/shard_map/broadcast_in_dim | solution.py:1281
  159.8 0.0 copy-done.2
  159.8 0.8 copy.18
  160.6 0.0 copy-done.1
  160.6 0.8 copy.19
Async XLA Ops:
  150.2 7.0 %copy-start = (bf16[512,2048]{1,0:T(8,128)(2,1)S(1)}, bf16[512,2048]{1,0:T(8,128)(2,1)}, u32[]{:S(2)}) copy-start(bf16[512,2048]{1,0:T(8,128)(2,1)} %get-tuple-element.12) | copy-start | bytes 6291460
  157.2 2.5 %copy-start.2 = (f32[128,1024]{1,0:T(8,128)S(1)}, f32[128,1024]{1,0:T(8,128)}, u32[]{:S(2)}) copy-start(f32[128,1024]{1,0:T(8,128)} %get-tuple-element.25) | copy-start | bytes 1572868
  157.2 3.3 %copy-start.1 = (bf16[256,1024]{1,0:T(8,128)(2,1)S(1)}, bf16[256,1024]{1,0:T(8,128)(2,1)}, u32[]{:S(2)}) copy-start(bf16[256,1024]{1,0:T(8,128)(2,1)} %get-tuple-element.26) | copy-start | bytes 1572868
